TPU v7x, 128 devices: a whole 4x4x4 slice. The times are simulated.
128 devices in a mesh: ep: 64 (over z, y, x), tp: 2 (over core).
Axes of the slice: x: 4, y: 4, z: 4, core: 2. Of those that a mesh axis runs over, the one named last changes fastest.
Arguments:
- stream: bfloat16 [4096, 2048], P('ep', 'tp'), may hold values from -40 to 40
- conv_state: bfloat16 [4096, 3, 2048], P('ep', None, 'tp'), may hold values from -5 to 5
- recur_state: float32 [4096, 2048], P('ep', 'tp'), may hold values from -5 to 5
- mix_gain: float32 [2048], replicated, may hold values from 0.1 to 1.9
- branch_weight: bfloat16 [2048, 2048], P(None, 'tp'), may hold values from -0.125 to 0.125
- gate_weight: bfloat16 [2048, 2048], P(None, 'tp'), may hold values from -0.125 to 0.125
- conv_taps: float32 [4, 2048], P(None, 'tp'), may hold values from -3 to 3
- recur_map: bfloat16 [16, 128, 128], P('tp'), may hold values from -0.5 to 0.5
- input_map: bfloat16 [16, 128, 128], P('tp'), may hold values from -0.5 to 0.5
- decay_logit: float32 [2048], P('tp'), may hold values from -1 to 6
- out_weight: bfloat16 [2048, 2048], P(None, 'tp'), may hold values from -0.125 to 0.125
- moe_gain: float32 [2048], replicated, may hold values from 0.1 to 1.9
- route_ids: int32 [4096, 6], P('ep'), may hold values from 0 to 63, all different within a row; in each aligned block of 64 rows (0 to 63, 64 to 127, ...) at most 18 rows name the same one
- route_weights: float32 [4096, 6], P('ep'), may hold values from 0.2 to 1
- expert_gate: bfloat16 [64, 2048, 512], P('ep', None, 'tp'), may hold values from -0.125 to 0.125
- expert_up: bfloat16 [64, 2048, 512], P('ep', None, 'tp'), may hold values from -0.125 to 0.125
- expert_down: bfloat16 [64, 512, 2048], P('ep', None, 'tp'), may hold values from -0.25 to 0.25
- dense_gate: bfloat16 [2048, 512], P(None, 'tp'), may hold values from -0.125 to 0.125
- dense_up: bfloat16 [2048, 512], P(None, 'tp'), may hold values from -0.125 to 0.125
- dense_down: bfloat16 [512, 2048], P(None, 'tp'), may hold values from -0.25 to 0.25
- dense_scale: float32 [2048], P('tp'), may hold values from 0.1 to 1.9
Outputs:
- result: bfloat16 [4096, 2048], P('ep', 'tp')
- new_state: float32 [4096, 2048], P('ep', 'tp')
- new_conv: bfloat16 [4096, 3, 2048], P('ep', None, 'tp')
Inputs may be any that keep to these rules, and one draw needn't show every extreme that they name: `route_ids`: each row names 6 different experts; among the rows of one index of ep no expert is named by more than 18 rows, and in every draw some expert is named by exactly 18 rows of some index.
All inputs are finite; a program needn't handle non-finite values.
Results may differ from a plain program's by a relative error of at most 0.014.
Values may be sent and summed in bfloat16 or wider, within the bound.
No kernel may reach another device: no remote copies, remote signals or barrier semaphores. Data moves between devices by JAX's collectives and lax.ppermute only.
A program may use at most 128 MiB of HBM per device.

v0:
```python
import jax
import jax.numpy as jnp
from jax import lax
from jax.sharding import PartitionSpec as P


def laid_out(tiles, dim):
    shape = list(tiles.shape[1:])
    shape[dim] *= tiles.shape[0]
    return jnp.moveaxis(tiles, 0, dim).reshape(shape)


def sent_to_all(shard, axis):
    length = lax.axis_size(axis)
    return lax.all_to_all(
        jnp.broadcast_to(shard[None], (length, *shard.shape)), axis, 0, 0, tiled=True
    )


def gathered_copies(shard, axis, dim):
    return laid_out(sent_to_all(shard, axis), dim)


def accumulate_with(weight, segment):
    return jnp.dot(segment, weight, preferred_element_type=jnp.float32)


def normalize(part_rows, gain_vec):
    whole_rows = gathered_copies(part_rows, "tp", 1).astype(jnp.float32)
    row_mean = jnp.mean(whole_rows, axis=1, keepdims=True)
    row_var = jnp.mean(whole_rows * whole_rows, axis=1, keepdims=True) - row_mean * row_mean
    return ((whole_rows - row_mean) * lax.rsqrt(row_var + 1e-05) * gain_vec).astype(jnp.bfloat16)


def per_device(
    stream,
    conv_state,
    recur_state,
    mix_gain,
    branch_weight,
    gate_weight,
    conv_taps,
    recur_map,
    input_map,
    decay_logit,
    out_weight,
    moe_gain,
    route_ids,
    route_weights,
    expert_gate,
    expert_up,
    expert_down,
    dense_gate,
    dense_up,
    dense_down,
    dense_scale,
):
    seq_count = stream.shape[0]
    out_width = stream.shape[1]
    normed = normalize(stream, mix_gain)
    branch_in = jnp.dot(normed, branch_weight, preferred_element_type=jnp.float32).astype(
        jnp.bfloat16
    )
    gate_pre = jnp.dot(normed, gate_weight, preferred_element_type=jnp.float32).astype(jnp.bfloat16)
    conv_sum = branch_in.astype(jnp.float32) * conv_taps[3]
    for offset in range(3):
        conv_sum = conv_sum + conv_state[:, offset].astype(jnp.float32) * conv_taps[offset]
    conv_out = conv_sum.astype(jnp.bfloat16)
    new_conv = jnp.concatenate([conv_state[:, 1:], branch_in[:, None]], axis=1)
    block_count = recur_map.shape[0]
    block_width = recur_map.shape[1]
    grouped = conv_out.reshape(seq_count, block_count, block_width)
    recur_gate = jax.nn.sigmoid(
        jnp.einsum("nbc,bcd->nbd", grouped, recur_map, preferred_element_type=jnp.float32)
    ).reshape(seq_count, -1)
    input_gate = jax.nn.sigmoid(
        jnp.einsum("nbc,bcd->nbd", grouped, input_map, preferred_element_type=jnp.float32)
    ).reshape(seq_count, -1)
    log_decay = -8.0 * recur_gate * jax.nn.softplus(-decay_logit)
    driven = jnp.sqrt(-jnp.expm1(2.0 * log_decay)) * (input_gate * conv_out.astype(jnp.float32))
    new_state = jnp.exp(log_decay) * recur_state + driven
    mixer_in = (jax.nn.gelu(gate_pre.astype(jnp.float32)) * new_state).astype(jnp.bfloat16)
    mixer_out = accumulate_with(
        out_weight, lax.all_gather(mixer_in, "tp", axis=1, tiled=True)
    ).astype(jnp.bfloat16)
    resid = (stream.astype(jnp.float32) + mixer_out.astype(jnp.float32)).astype(jnp.bfloat16)
    normed_two = normalize(resid, moe_gain)
    top_count = route_ids.shape[1]
    expert_count = lax.axis_size("ep")
    capacity = max(2, min(seq_count, 3 * seq_count * top_count // expert_count))
    flat_ids = route_ids.reshape(-1)
    one_hot = (flat_ids[:, None] == jnp.arange(expert_count, dtype=jnp.int32)[None, :]).astype(
        jnp.int32
    )
    slot_rank = jnp.sum(one_hot * (jnp.cumsum(one_hot, axis=0) - 1), axis=1)
    slot_index = (flat_ids * capacity + slot_rank).reshape(seq_count, top_count)
    dispatch_table = jnp.sum(
        (
            slot_index[:, :, None]
            == jnp.arange(expert_count * capacity, dtype=jnp.int32)[None, None, :]
        ).astype(jnp.bfloat16),
        axis=1,
    )
    own_gate = expert_gate[0]
    own_up = expert_up[0]
    own_down = expert_down[0]
    own_features = lax.dynamic_slice_in_dim(
        normed_two, lax.axis_index("tp") * out_width, out_width, 1
    )
    outgoing = lax.dot_general(
        dispatch_table, own_features, (((0,), (0,)), ((), ())), preferred_element_type=jnp.float32
    )
    outgoing = outgoing.astype(jnp.bfloat16).reshape(expert_count, capacity, -1)
    incoming = lax.all_gather(
        lax.all_to_all(outgoing, "ep", split_axis=0, concat_axis=0, tiled=True),
        "tp",
        axis=2,
        tiled=True,
    )
    source_count, slot_count, feature_count = incoming.shape
    taken_rows = incoming.reshape(source_count * slot_count, feature_count)
    gate_sum = jnp.dot(taken_rows, own_gate, preferred_element_type=jnp.float32)
    up_sum = jnp.dot(taken_rows, own_up, preferred_element_type=jnp.float32)
    hidden = (jax.nn.silu(gate_sum) * up_sum).astype(jnp.bfloat16)
    served_rows = accumulate_with(own_down, gathered_copies(hidden, "tp", 1))
    served = served_rows.astype(jnp.bfloat16).reshape(source_count, slot_count, -1)
    returned = lax.all_to_all(served, "ep", split_axis=0, concat_axis=0, tiled=True).reshape(
        expert_count * capacity, -1
    )
    picked = returned[slot_index]
    routed = jnp.sum(picked.astype(jnp.float32) * route_weights[:, :, None], axis=1)
    dense_gsum = jnp.dot(normed_two, dense_gate, preferred_element_type=jnp.float32)
    dense_usum = jnp.dot(normed_two, dense_up, preferred_element_type=jnp.float32)
    dense_hidden = (jax.nn.silu(dense_gsum) * dense_usum).astype(jnp.bfloat16)
    dense_out = accumulate_with(
        dense_down, lax.all_gather(dense_hidden, "tp", axis=1, tiled=True)
    ).astype(jnp.bfloat16)
    result = (
        resid.astype(jnp.float32) + routed + dense_scale * dense_out.astype(jnp.float32)
    ).astype(jnp.bfloat16)
    return (result, new_state, new_conv)


def solution(mesh):
    in_specs = (
        P("ep", "tp"),
        P("ep", None, "tp"),
        P("ep", "tp"),
        P(),
        P(None, "tp"),
        P(None, "tp"),
        P(None, "tp"),
        P("tp", None, None),
        P("tp", None, None),
        P("tp"),
        P(None, "tp"),
        P(),
        P("ep", None),
        P("ep", None),
        P("ep", None, "tp"),
        P("ep", None, "tp"),
        P("ep", None, "tp"),
        P(None, "tp"),
        P(None, "tp"),
        P(None, "tp"),
        P("tp"),
    )
    out_specs = (P("ep", "tp"), P("ep", "tp"), P("ep", None, "tp"))
    return jax.shard_map(
        per_device, mesh=mesh, in_specs=in_specs, out_specs=out_specs, check_vma=False
    )
```

profile of v0, /device:TPU:0, one launch (start us, length us, event | category | flops | bytes accessed | tf_op | source)
XLA Modules:
  0.0 197.2 jit_solution(7304002262852420736)
XLA Ops:
  7.2 1.7 broadcast_in_dim.10
  8.9 3.4 %all-to-all-start = ((bf16[2,64,1024]{2,1,0:T(8,128)(2,1)}), bf16[2,64,1024]{2,1,0:T(8,128)(2,1)S(1)}, u32[]{:S(2)}, u32[]{:S(2)}) async-start(bf16[2,64,1024]{2,1,0:T(8,128)(2,1)} %broadcast_in_dim.10), calls=%async_computation | async-start | bytes 524288 | tf_op jit(solution)/shard_map/all_to_all | solution.py:15
  12.4 0.9 fusion.51
  13.3 0.7 all-to-all-done
  14.0 0.2 convert_reduce_fusion.1
  14.3 4.0 %fusion.38 = (bf16[64,1024]{1,0:T(8,128)(2,1)S(1)}, bf16[64,1024]{1,0:T(8,128)(2,1)}) fusion(f32[1024]{0:T(1024)S(1)} %bitcast.101, bf16[64,3,1024]{2,0,1:T(8,128)(2,1)S(1)} %copy-done.6, f32[1024]{0:T(1024)S(1)} %bitcast.102, f32[1024]{0:T(1024)S(1)} %bitcast.100, f32[1024]{0:T(1024)S(1)} %bitcast.99, bf16[2048,1024]{1,0:T(8,128)(2,1)} %param.25, ...), kind=kOutput, calls=%fused_computation.64 | convolution fusion | flops 269811712 | bytes 5399040 | tf_op jit(solution)/shard_map/dot_general | solution.py:61
  18.2 0.2 fusion.5
  18.5 0.2 fusion.9
  18.7 0.2 copy-done.19
  18.9 0.3 copy-done.13
  19.2 0.2 fusion.36
  19.5 1.0 fusion.34
  20.5 2.1 %all_gather.9 = bf16[64,2048]{1,0:T(8,128)(2,1)S(1)} all-gather(bf16[64,1024]{1,0:T(8,128)(2,1)S(1)} %fusion.34), channel_id=1, replica_groups=mesh['ep'=64,'tp'=2] {'tp'}, dimensions={1}, use_global_device_ids=true | all-gather | bytes 393216 | tf_op jit(solution)/shard_map/all_gather | solution.py:84
  22.6 0.9 fusion.15
  23.5 0.7 broadcast_in_dim.11
  24.2 3.4 %all-to-all-start.1 = ((bf16[2,64,1024]{2,1,0:T(8,128)(2,1)}), bf16[2,64,1024]{2,1,0:T(8,128)(2,1)S(1)}, u32[]{:S(2)}, u32[]{:S(2)}) async-start(bf16[2,64,1024]{2,1,0:T(8,128)(2,1)} %broadcast_in_dim.11), calls=%async_computation.1 | async-start | bytes 524288 | tf_op jit(solution)/shard_map/all_to_all | solution.py:15
  27.8 0.1 eq.38
  27.9 0.1 eq.42
  28.1 1.1 all-to-all-done.1
  29.3 0.9 reduce-window.6
  30.2 0.2 slice_reduce_fusion
  30.8 1.0 fusion.23
  31.8 0.2 convert_reduce_fusion
  32.2 0.7 copy-done.4
  32.9 1.7 convolution_convert_fusion.1
  34.6 2.4 %reshape.118 = bf16[64,18,1024]{2,1,0:T(8,128)(2,1)} reshape(bf16[1152,1024]{1,0:T(8,128)(2,1)S(1)} %convolution_convert_fusion.1) | data formatting | bytes 4718592 | tf_op jit(solution)/shard_map/reshape | solution.py:113
  37.0 53.3 %all_to_all.25 = bf16[64,18,1024]{2,1,0:T(8,128)(2,1)} all-to-all(bf16[64,18,1024]{2,1,0:T(8,128)(2,1)} %reshape.118), channel_id=1, replica_groups=mesh['ep'=64,'tp'=2] {'ep'}, dimensions={0} | all-to-all | bytes 4718592 | tf_op jit(solution)/shard_map/all_to_all | solution.py:115
  90.3 15.6 %all-gather.2.cloned.1.call-done = bf16[64,18,2048]{2,1,0:T(8,128)(2,1)} async-done(((bf16[64,18,1024]{2,1,0:T(8,128)(2,1)}), bf16[64,18,2048]{2,1,0:T(8,128)(2,1)}) %all-gather.2.cloned.1.call-update) | async-done | bytes 4718608 | tf_op jit(solution)/shard_map/all_gather | solution.py:114
  106.0 7.8 %reshape.119 = bf16[1152,2048]{1,0:T(8,128)(2,1)} reshape(bf16[64,18,2048]{2,1,0:T(8,128)(2,1)} %all-gather.2.cloned.1.call-done) | data formatting | bytes 9437184 | tf_op jit(solution)/shard_map/reshape | solution.py:121
  113.7 3.9 %fusion.21 = f32[1152,256]{1,0:T(8,128)S(1)} fusion(bf16[1152,2048]{1,0:T(8,128)(2,1)} %reshape.119, bf16[1,2048,256]{2,1,0:T(8,128)(2,1)S(1)} %copy-done.20), kind=kOutput, calls=%fused_computation.34 | convolution fusion | flops 1207959552 | bytes 6946816 | tf_op jit(solution)/shard_map/dot_general | solution.py:122
  117.7 0.1 copy-done.21
  117.8 1.6 fusion
  119.4 0.3 copy.78
  119.8 4.7 %all_to_all.26 = bf16[2,1152,256]{1,2,0:T(8,128)(2,1)S(1)} all-to-all(bf16[2,1152,256]{1,2,0:T(8,128)(2,1)S(1)} %broadcast_in_dim.12), channel_id=1, replica_groups=mesh['ep'=64,'tp'=2] {'tp'}, dimensions={0} | all-to-all | bytes 2359296 | tf_op jit(solution)/shard_map/all_to_all | solution.py:15
  124.4 1.4 convolution_convert_fusion
  125.9 2.4 %reshape.121 = bf16[64,18,1024]{2,1,0:T(8,128)(2,1)} reshape(bf16[1152,1024]{1,0:T(8,128)(2,1)S(1)} %convolution_convert_fusion) | data formatting | bytes 4718592 | tf_op jit(solution)/shard_map/reshape | solution.py:126
  128.3 10.8 %all-to-all-start.4 = ((bf16[64,18,1024]{2,1,0:T(8,128)(2,1)}), bf16[64,18,1024]{2,1,0:T(8,128)(2,1)}, u32[]{:S(2)}, u32[]{:S(2)}) async-start(bf16[64,18,1024]{2,1,0:T(8,128)(2,1)} %reshape.121), calls=%async_computation.4 | async-start | bytes 6291456 | tf_op jit(solution)/shard_map/all_to_all | solution.py:127
  139.3 0.7 copy.80
  140.1 0.3 fusion.52
  140.4 1.5 fusion.18
  141.9 2.0 %all_gather.11 = bf16[64,512]{1,0:T(8,128)(2,1)} all-gather(bf16[64,256]{1,0:T(8,128)(2,1)S(1)} %fusion.18), channel_id=1, replica_groups=mesh['ep'=64,'tp'=2] {'tp'}, dimensions={1}, use_global_device_ids=true | all-gather | bytes 98304 | tf_op jit(solution)/shard_map/all_gather | solution.py:136
  143.9 0.8 pad_maximum_fusion
  144.7 36.2 %all-to-all-done.4 = bf16[64,18,1024]{2,1,0:T(8,128)(2,1)} async-done(((bf16[64,18,1024]{2,1,0:T(8,128)(2,1)}), bf16[64,18,1024]{2,1,0:T(8,128)(2,1)}, u32[]{:S(2)}, u32[]{:S(2)}) %all-to-all-start.4) | async-done | bytes 2359328 | tf_op jit(solution)/shard_map/all_to_all | solution.py:127
  180.9 2.9 %reshape.122 = bf16[1152,1024]{1,0:T(8,128)(2,1)S(1)} reshape(bf16[64,18,1024]{2,1,0:T(8,128)(2,1)} %all-to-all-done.4) | data formatting | bytes 4718592 | tf_op jit(solution)/shard_map/reshape | solution.py:127
  183.8 2.7 %gather_fusion = bf16[384,1024]{1,0:T(8,128)(2,1)} fusion(bf16[1152,1024]{1,0:T(8,128)(2,1)S(1)} %reshape.122, s32[1024]{0:T(1024)S(1)} %pad_clamp_fusion), kind=kCustom, calls=%fused_computation | custom fusion | bytes 1574400 | tf_op jit(solution)/shard_map/gather | solution.py:130
  186.5 1.3 reshape.138
  187.8 1.6 multiply_reduce_fusion
  189.4 1.0 fusion.17
  (67 shorter events, 1.3 us)
Async XLA Ops:
  7.2 117.3 %copy-start = (bf16[1,512,1024]{2,1,0:T(8,128)(2,1)S(1)}, bf16[1,512,1024]{2,1,0:T(8,128)(2,1)}, u32[]{:S(2)}) copy-start(bf16[1,512,1024]{2,1,0:T(8,128)(2,1)} %param.37) | copy-start | bytes 3145732
  7.2 7.0 %copy-start.6 = (bf16[64,3,1024]{2,0,1:T(8,128)(2,1)S(1)}, bf16[64,3,1024]{2,0,1:T(8,128)(2,1)}, u32[]{:S(2)}) copy-start(bf16[64,3,1024]{2,0,1:T(8,128)(2,1)} %param.22) | copy-start | bytes 1179652
  7.2 7.0 %copy-start.14 = (f32[2048]{0:T(1024)S(1)}, f32[2048]{0:T(1024)}, u32[]{:S(2)}) copy-start(f32[2048]{0:T(1024)} %param.24) | copy-start | bytes 24580
  8.9 5.0 %all-to-all-start = ((bf16[2,64,1024]{2,1,0:T(8,128)(2,1)}), bf16[2,64,1024]{2,1,0:T(8,128)(2,1)S(1)}, u32[]{:S(2)}, u32[]{:S(2)}) async-start(bf16[2,64,1024]{2,1,0:T(8,128)(2,1)} %broadcast_in_dim.10), calls=%async_computation | async-start | bytes 524288 | tf_op jit(solution)/shard_map/all_to_all | solution.py:15
  14.2 4.0 %copy-start.22 = (bf16[8,128,128]{2,1,0:T(8,128)(2,1)S(1)}, bf16[8,128,128]{2,1,0:T(8,128)(2,1)}, u32[]{:S(2)}) copy-start(bf16[8,128,128]{2,1,0:T(8,128)(2,1)} %param.29) | copy-start | bytes 786436
  14.2 4.2 %copy-start.23 = (bf16[8,128,128]{2,1,0:T(8,128)(2,1)S(1)}, bf16[8,128,128]{2,1,0:T(8,128)(2,1)}, u32[]{:S(2)}) copy-start(bf16[8,128,128]{2,1,0:T(8,128)(2,1)} %param.28) | copy-start | bytes 786436
  14.3 5.2 %copy-start.3 = (bf16[2048,1024]{1,0:T(8,128)(2,1)S(1)}, bf16[2048,1024]{1,0:T(8,128)(2,1)}, u32[]{:S(2)}) copy-start(bf16[2048,1024]{1,0:T(8,128)(2,1)} %param.26) | copy-start | bytes 12582916
  18.2 0.7 copy-start.19
  18.2 1.0 copy-start.13
  19.4 1.0 copy-start.9
  19.4 3.1 %copy-start.2 = (bf16[2048,1024]{1,0:T(8,128)(2,1)S(1)}, bf16[2048,1024]{1,0:T(8,128)(2,1)}, u32[]{:S(2)}) copy-start(bf16[2048,1024]{1,0:T(8,128)(2,1)} %param.31) | copy-start | bytes 12582916
  19.5 3.1 %copy-start.10 = (bf16[64,1024]{1,0:T(8,128)(2,1)S(1)}, bf16[64,1024]{1,0:T(8,128)(2,1)}, u32[]{:S(2)}) copy-start(bf16[64,1024]{1,0:T(8,128)(2,1)} %param.21) | copy-start | bytes 393220
  22.6 5.1 %copy-start.15 = (s32[64,6]{0,1:T(8,128)S(1)}, s32[64,6]{0,1:T(8,128)}, u32[]{:S(2)}) copy-start(s32[64,6]{0,1:T(8,128)} %param.33) | copy-start | bytes 4612
  23.4 8.6 %copy-start.16 = (f32[2048]{0:T(1024)S(1)}, f32[2048]{0:T(1024)}, u32[]{:S(2)}) copy-start(f32[2048]{0:T(1024)} %param.32) | copy-start | bytes 24580
  24.2 5.0 %all-to-all-start.1 = ((bf16[2,64,1024]{2,1,0:T(8,128)(2,1)}), bf16[2,64,1024]{2,1,0:T(8,128)(2,1)S(1)}, u32[]{:S(2)}, u32[]{:S(2)}) async-start(bf16[2,64,1024]{2,1,0:T(8,128)(2,1)} %broadcast_in_dim.11), calls=%async_computation.1 | async-start | bytes 524288 | tf_op jit(solution)/shard_map/all_to_all | solution.py:15
  27.6 78.3 %all-gather.2.cloned.1.call-start = ((), (), s32[]{:S(2)}) async-start(), calls=%async_computation.5 | async-start | bytes 9437184 | tf_op jit(solution)/shard_map/all_gather | solution.py:114
  32.1 0.7 copy-start.4
  90.3 23.4 %copy-start.20 = (bf16[1,2048,256]{2,1,0:T(8,128)(2,1)S(1)}, bf16[1,2048,256]{2,1,0:T(8,128)(2,1)}, u32[]{:S(2)}) copy-start(bf16[1,2048,256]{2,1,0:T(8,128)(2,1)} %param.35) | copy-start | bytes 3145732
  113.7 3.9 %copy-start.1 = (bf16[1152,2048]{1,0:T(8,128)(2,1)S(1)}, bf16[1152,2048]{1,0:T(8,128)(2,1)}, u32[]{:S(2)}) copy-start(bf16[1152,2048]{1,0:T(8,128)(2,1)} %reshape.119) | copy-start | bytes 14155780
  113.7 4.1 %copy-start.21 = (bf16[1,2048,256]{2,1,0:T(8,128)(2,1)S(1)}, bf16[1,2048,256]{2,1,0:T(8,128)(2,1)}, u32[]{:S(2)}) copy-start(bf16[1,2048,256]{2,1,0:T(8,128)(2,1)} %param.36) | copy-start | bytes 3145732
  128.3 11.0 %copy-start.18 = (f32[64,6]{0,1:T(8,128)S(1)}, f32[64,6]{0,1:T(8,128)}, u32[]{:S(2)}) copy-start(f32[64,6]{0,1:T(8,128)} %param.34) | copy-start | bytes 4612
  128.3 11.7 %copy-start.5 = (bf16[64,2048]{1,0:T(8,128)(2,1)S(1)}, bf16[64,2048]{1,0:T(8,128)(2,1)}, u32[]{:S(2)}) copy-start(bf16[64,2048]{1,0:T(8,128)(2,1)} %copy-done.4) | copy-start | bytes 786436
  128.3 11.7 %copy-start.7 = (bf16[2048,256]{1,0:T(8,128)(2,1)S(1)}, bf16[2048,256]{1,0:T(8,128)(2,1)}, u32[]{:S(2)}) copy-start(bf16[2048,256]{1,0:T(8,128)(2,1)} %param.38) | copy-start | bytes 3145732
  128.3 52.5 %all-to-all-start.4 = ((bf16[64,18,1024]{2,1,0:T(8,128)(2,1)}), bf16[64,18,1024]{2,1,0:T(8,128)(2,1)}, u32[]{:S(2)}, u32[]{:S(2)}) async-start(bf16[64,18,1024]{2,1,0:T(8,128)(2,1)} %reshape.121), calls=%async_computation.4 | async-start | bytes 6291456 | tf_op jit(solution)/shard_map/all_to_all | solution.py:127
  139.1 4.8 %slice-start = ((bf16[64,3,1024]{2,0,1:T(8,128)(2,1)}), bf16[64,2,1024]{2,0,1:T(8,128)(2,1)S(1)}, s32[]{:S(2)}) async-start(bf16[64,3,1024]{2,0,1:T(8,128)(2,1)} %param.22), calls=%async_computation.6 | async-start | bytes 524288 | tf_op jit(solution)/shard_map/slice | solution.py:69
  139.1 4.8 %copy-start.11 = (bf16[64,1024]{1,0:T(8,128)(2,1)S(1)}, bf16[64,1024]{1,0:T(8,128)(2,1)}, u32[]{:S(2)}) copy-start(bf16[64,1024]{1,0:T(8,128)(2,1)} %get-tuple-element.18) | copy-start | bytes 393220
  186.5 2.9 %copy-start.17 = (f32[1024]{0:T(1024)S(1)}, f32[1024]{0:T(1024)}, u32[]{:S(2)}) copy-start(f32[1024]{0:T(1024)} %param.41) | copy-start | bytes 12292
  187.8 1.6 copy-start.8
  187.8 1.6 copy-start.12
Sparse Core Ops, SparseCore 0:
  90.4 15.4 all-gather.1
where the time goes:
time: 198 us; the launch traced here: 197 us
  blocking collectives  62.1 us (31%)
  waiting for transfers between devices  53.6 us (27%)
  local copies, waits for them, and re-layouts  26.5 us (13%)
  starting transfers between devices  17.7 us (9%)
  matrix products  17.6 us (9%)
  between operations  14.5 us (7%)
  other arithmetic  5.26 us (3%)
    all_to_all x1, blocking collectives, per_device(): lax.all_to_all(outgoing, 'ep', split_axis=0, concat_axis=0, tiled=True)  53.3 us
    all_to_all x1, waiting for transfers between devices, per_device(): lax.all_to_all(served, 'ep', split_axis=0, concat_axis=0, tiled=True)  36.2 us
    all_gather x1, waiting for transfers between devices, per_device(): lax.all_gather(lax.all_to_all(outgoing, 'ep', split_axis=0, concat_axis=0...  15.6 us
    all_to_all x1, starting transfers between devices, per_device(): lax.all_to_all(served, 'ep', split_axis=0, concat_axis=0, tiled=True)  10.8 us
    reshape x1, local copies, waits for them, and re-layouts, per_device(): taken_rows = incoming.reshape(source_count * slot_count, feature_count)  7.77 us
    all_to_all x2, starting transfers between devices, sent_to_all(): lax.all_to_all(jnp.broadcast_to(shard[None], (length, *shard.shape)), axi...  6.89 us
    all_to_all x1, blocking collectives, sent_to_all(): lax.all_to_all(jnp.broadcast_to(shard[None], (length, *shard.shape)), axi...  4.68 us
  transfers between devices with their start and end apart: 4, of which 4 were waited for; matrix products, arithmetic and copies ran while one was open for 2% of the time, Pallas kernels for 0%

commit v1 on v0

v1 whole, which is shorter than its diff:
```python
import functools

import jax
import jax.numpy as jnp
from jax import lax
from jax.experimental import pallas as pl
from jax.experimental.pallas import tpu as pltpu
from jax.sharding import PartitionSpec as P

BF = jnp.bfloat16
F32 = jnp.float32
SWAP = [(0, 1), (1, 0)]
VMEM_LIMIT = 56 * 1024 * 1024


def swapped(x):
    return lax.ppermute(x, "tp", SWAP)


def in_order(core, own, other):
    return jnp.where(
        core == 0,
        jnp.concatenate([own, other], axis=1),
        jnp.concatenate([other, own], axis=1),
    )


def route_tables(ids, core, slots):
    rows = ids.shape[0]
    experts = rows
    lane = lax.broadcasted_iota(jnp.int32, (rows, experts), 1)
    hits = [(ids[:, k : k + 1] == lane) for k in range(ids.shape[1])]
    chosen = functools.reduce(jnp.logical_or, hits)
    chosen_f = jnp.where(chosen, 1.0, 0.0).astype(F32)
    earlier = (
        lax.broadcasted_iota(jnp.int32, (rows, rows), 0)
        > lax.broadcasted_iota(jnp.int32, (rows, rows), 1)
    )
    rank = jnp.dot(
        jnp.where(earlier, 1.0, 0.0).astype(BF),
        chosen_f.astype(BF),
        preferred_element_type=F32,
    )
    place = jnp.where(chosen, rank - (slots * core).astype(F32), -1.0)
    return hits, place


def spread(experts, width):
    lane = lax.broadcasted_iota(jnp.int32, (experts, experts * width), 1)
    sub = lax.broadcasted_iota(jnp.int32, (experts, experts * width), 0)
    return jnp.where(lane // width == sub, 1.0, 0.0).astype(BF)


LANES = 128


def put_pieces(piece_ref, values, start):
    count = values.shape[0]
    for n in range(values.shape[1] // LANES):
        c, part = divmod(start + n, 2)
        piece_ref[part, pl.ds(c, count, stride=8), :] = values[:, n * LANES : (n + 1) * LANES]


def read_pieces(piece_ref):
    return jnp.concatenate([piece_ref[0].astype(BF), piece_ref[1].astype(BF)], axis=1)


def take_pieces(piece_ref, block_ref, features, rows_ref, start):
    count = block_ref.shape[0] // 8
    piece_ref[0] = block_ref[:, features : features + LANES].astype(F32)
    piece_ref[1] = block_ref[:, features + LANES :].astype(F32)
    for n in range(features // LANES):
        c, part = divmod(n, 2)
        rows_ref[start : start + count, n * LANES : (n + 1) * LANES] = piece_ref[
            part, pl.ds(c, count, stride=8), :
        ].astype(BF)


def pack_body(core_ref, own_ref, other_ref, gain_ref, ids_ref, out_ref, norm_ref, piece_ref):
    core = core_ref[0]
    half = own_ref.shape[1]
    features = 2 * half
    own = own_ref[...].astype(F32)
    other = other_ref[...].astype(F32)
    mean = (jnp.sum(own, 1, keepdims=True) + jnp.sum(other, 1, keepdims=True)) / features
    square = (
        jnp.sum(own * own, 1, keepdims=True) + jnp.sum(other * other, 1, keepdims=True)
    ) / features
    scale = lax.rsqrt(square - mean * mean + 1e-05)
    gain_own = gain_ref[pl.ds(core, 1), :]
    gain_other = gain_ref[pl.ds(1 - core, 1), :]
    norm_ref[:, :half] = ((own - mean) * scale * gain_own).astype(BF)
    norm_ref[:, half:] = ((other - mean) * scale * gain_other).astype(BF)
    rows = norm_ref[...]
    experts = ids_ref.shape[0]
    slots = 9
    _, place = route_tables(ids_ref[...], core, slots)
    wide = jnp.dot(place.astype(BF), spread(experts, 8), preferred_element_type=F32)
    lane = lax.broadcasted_iota(jnp.int32, wide.shape, 1) % 8
    table = jnp.where(wide == lane.astype(F32), 1.0, 0.0)
    table = jnp.transpose(table).astype(BF)
    out_ref[:, :features] = jnp.dot(table, rows, preferred_element_type=F32).astype(BF)
    last = jnp.transpose(jnp.where(place == 8.0, 1.0, 0.0)).astype(BF)
    ninth = jnp.dot(last, rows, preferred_element_type=F32)
    put_pieces(piece_ref, ninth, 0)
    out_ref[:, features:] = read_pieces(piece_ref)


def expert_body(
    core_ref,
    in_ref,
    gate_ref,
    gate2_ref,
    up_ref,
    up2_ref,
    down_ref,
    down2_ref,
    out_ref,
    piece_ref,
    rows_ref,
):
    core = core_ref[0]
    count = in_ref.shape[0]
    features = gate_ref.shape[0]
    half = features // 2
    units = gate_ref.shape[1]
    rows_ref[:count, :] = in_ref[:, :features]
    take_pieces(piece_ref, in_ref, features, rows_ref, count)
    first = pl.multiple_of(core * half, half)
    second = pl.multiple_of((1 - core) * half, half)

    def product(weight):
        return jnp.dot(
            rows_ref[:, :half], weight[pl.ds(first, half), :], preferred_element_type=F32
        ) + jnp.dot(rows_ref[:, half:], weight[pl.ds(second, half), :], preferred_element_type=F32)

    def hidden(gate, up):
        return (jax.nn.silu(product(gate)) * product(up)).astype(BF)

    hid_own = hidden(gate_ref, up_ref)
    hid_other = hidden(gate2_ref, up2_ref)
    unit_own = pl.multiple_of(core * units, units)
    unit_other = pl.multiple_of((1 - core) * units, units)
    for part, down in enumerate((down_ref, down2_ref)):
        served = jnp.dot(
            hid_own, down[pl.ds(unit_own, units), :], preferred_element_type=F32
        ) + jnp.dot(hid_other, down[pl.ds(unit_other, units), :], preferred_element_type=F32)
        out_ref[:, part * half : (part + 1) * half] = served[:count].astype(BF)
        put_pieces(piece_ref, served[count:], part * (half // LANES))
    out_ref[:, features:] = read_pieces(piece_ref)


def combine_body(core_ref, in_ref, ids_ref, weights_ref, own_ref, other_ref, piece_ref, last_ref):
    core = core_ref[0]
    experts = ids_ref.shape[0]
    rows = ids_ref.shape[0]
    features = 2 * own_ref.shape[1]
    half = features // 2
    hits, place = route_tables(ids_ref[...], core, 9)
    weight = functools.reduce(
        jnp.add,
        [jnp.where(hit, weights_ref[:, k : k + 1], 0.0) for k, hit in enumerate(hits)],
    )
    high = weight.astype(BF).astype(F32)
    low = (weight - high).astype(BF).astype(F32)
    expand = spread(experts, 8)
    wide = jnp.dot(place.astype(BF), expand, preferred_element_type=F32)
    lane = lax.broadcasted_iota(jnp.int32, wide.shape, 1) % 8
    match = wide == lane.astype(F32)
    tables = []
    lasts = []
    for part in (high, low):
        spread_part = jnp.dot(part.astype(BF), expand, preferred_element_type=F32)
        tables.append(jnp.where(match, spread_part, 0.0).astype(BF))
        lasts.append(jnp.where(place == 8.0, part, 0.0).astype(BF))
    table = jnp.concatenate(tables, axis=0)
    last = jnp.concatenate(lasts, axis=0)
    take_pieces(piece_ref, in_ref, features, last_ref, 0)
    total = jnp.dot(table, in_ref[:, :features], preferred_element_type=F32) + jnp.dot(
        last, last_ref[...], preferred_element_type=F32
    )
    total = total[:rows] + total[rows:]
    own_ref[...] = total[:, :half]
    other_ref[...] = total[:, half:]


def vmem(count):
    return [pl.BlockSpec(memory_space=pltpu.VMEM)] * count


def smem():
    return [pl.BlockSpec(memory_space=pltpu.SMEM)]


def per_device(
    stream,
    conv_state,
    recur_state,
    mix_gain,
    branch_weight,
    gate_weight,
    conv_taps,
    recur_map,
    input_map,
    decay_logit,
    out_weight,
    moe_gain,
    route_ids,
    route_weights,
    expert_gate,
    expert_up,
    expert_down,
    dense_gate,
    dense_up,
    dense_down,
    dense_scale,
):
    core = lax.axis_index("tp")
    core_arr = core.astype(jnp.int32).reshape(1)
    seq_count, half = stream.shape
    features = 2 * half
    experts = lax.axis_size("ep")
    own_gate, own_up, own_down = expert_gate[0], expert_up[0], expert_down[0]
    stream_other = swapped(stream)
    other_gate, other_up, other_down = swapped(own_gate), swapped(own_up), swapped(own_down)

    whole = in_order(core, stream, stream_other).astype(F32)
    mean = jnp.mean(whole, axis=1, keepdims=True)
    var = jnp.mean(whole * whole, axis=1, keepdims=True) - mean * mean
    normed = ((whole - mean) * lax.rsqrt(var + 1e-05) * mix_gain).astype(BF)
    branch_in = jnp.dot(normed, branch_weight, preferred_element_type=F32).astype(BF)
    gate_pre = jnp.dot(normed, gate_weight, preferred_element_type=F32).astype(BF)
    conv_sum = branch_in.astype(F32) * conv_taps[3]
    for offset in range(3):
        conv_sum = conv_sum + conv_state[:, offset].astype(F32) * conv_taps[offset]
    conv_out = conv_sum.astype(BF)
    new_conv = jnp.concatenate([conv_state[:, 1:], branch_in[:, None]], axis=1)
    block_count, block_width = recur_map.shape[0], recur_map.shape[1]
    grouped = conv_out.reshape(seq_count, block_count, block_width)
    recur_gate = jax.nn.sigmoid(
        jnp.einsum("nbc,bcd->nbd", grouped, recur_map, preferred_element_type=F32)
    ).reshape(seq_count, -1)
    input_gate = jax.nn.sigmoid(
        jnp.einsum("nbc,bcd->nbd", grouped, input_map, preferred_element_type=F32)
    ).reshape(seq_count, -1)
    log_decay = -8.0 * recur_gate * jax.nn.softplus(-decay_logit)
    driven = jnp.sqrt(-jnp.expm1(2.0 * log_decay)) * (input_gate * conv_out.astype(F32))
    new_state = jnp.exp(log_decay) * recur_state + driven
    mixer_in = (jax.nn.gelu(gate_pre.astype(F32)) * new_state).astype(BF)
    mixer_whole = in_order(core, mixer_in, swapped(mixer_in))
    mixer_out = jnp.dot(mixer_whole, out_weight, preferred_element_type=F32).astype(BF)
    resid = (stream.astype(F32) + mixer_out.astype(F32)).astype(BF)
    resid_other = swapped(resid)

    block = features + features // 8
    payload, normed_two = pl.pallas_call(
        pack_body,
        name="pack",
        out_shape=(
            jax.ShapeDtypeStruct((experts * 8, block), BF),
            jax.ShapeDtypeStruct((seq_count, features), BF),
        ),
        in_specs=smem() + vmem(4),
        out_specs=tuple(vmem(2)),
        scratch_shapes=[pltpu.VMEM((2, experts * 8, LANES), F32)],
        compiler_params=pltpu.CompilerParams(vmem_limit_bytes=VMEM_LIMIT),
    )(core_arr, resid, resid_other, moe_gain.reshape(2, half), route_ids)

    incoming = lax.all_to_all(
        payload.reshape(experts, 8, block), "ep", split_axis=0, concat_axis=0, tiled=True
    ).reshape(experts * 8, block)

    own_two, other_two = normed_two[:, :half], normed_two[:, half:]
    whole_two = in_order(core, own_two, other_two)
    dense_hidden = (
        jax.nn.silu(jnp.dot(whole_two, dense_gate, preferred_element_type=F32))
        * jnp.dot(whole_two, dense_up, preferred_element_type=F32)
    ).astype(BF)
    dense_whole = in_order(core, dense_hidden, swapped(dense_hidden))
    dense_out = jnp.dot(dense_whole, dense_down, preferred_element_type=F32).astype(BF)
    base = resid.astype(F32) + dense_scale * dense_out.astype(F32)

    served = pl.pallas_call(
        expert_body,
        name="experts",
        out_shape=jax.ShapeDtypeStruct((experts * 8, block), BF),
        in_specs=smem() + vmem(7),
        out_specs=vmem(1)[0],
        scratch_shapes=[
            pltpu.VMEM((2, experts * 8, LANES), F32),
            pltpu.VMEM((experts * 9, features), BF),
        ],
        compiler_params=pltpu.CompilerParams(vmem_limit_bytes=VMEM_LIMIT),
    )(
        core_arr,
        incoming,
        own_gate,
        other_gate,
        own_up,
        other_up,
        own_down,
        other_down,
    )

    returned = lax.all_to_all(
        served.reshape(experts, 8, block), "ep", split_axis=0, concat_axis=0, tiled=True
    ).reshape(experts * 8, block)

    sum_own, sum_other = pl.pallas_call(
        combine_body,
        name="combine",
        out_shape=(
            jax.ShapeDtypeStruct((seq_count, half), F32),
            jax.ShapeDtypeStruct((seq_count, half), F32),
        ),
        in_specs=smem() + vmem(3),
        out_specs=tuple(vmem(2)),
        scratch_shapes=[
            pltpu.VMEM((2, experts * 8, LANES), F32),
            pltpu.VMEM((experts, features), BF),
        ],
        compiler_params=pltpu.CompilerParams(vmem_limit_bytes=VMEM_LIMIT),
    )(core_arr, returned, route_ids, route_weights)
    result = (base + (sum_own + swapped(sum_other))).astype(BF)
    return (result, new_state, new_conv)


def solution(mesh):
    in_specs = (
        P("ep", "tp"),
        P("ep", None, "tp"),
        P("ep", "tp"),
        P(),
        P(None, "tp"),
        P(None, "tp"),
        P(None, "tp"),
        P("tp", None, None),
        P("tp", None, None),
        P("tp"),
        P(None, "tp"),
        P(),
        P("ep", None),
        P("ep", None),
        P("ep", None, "tp"),
        P("ep", None, "tp"),
        P("ep", None, "tp"),
        P(None, "tp"),
        P(None, "tp"),
        P(None, "tp"),
        P("tp"),
    )
    out_specs = (P("ep", "tp"), P("ep", "tp"), P("ep", None, "tp"))
    return jax.shard_map(
        per_device, mesh=mesh, in_specs=in_specs, out_specs=out_specs, check_vma=False
    )
```

time: 198 us -> 123 us (0.62)
  blocking collectives: 62.1 us -> 0 us
  local copies, waits for them, and re-layouts: 26.5 us -> 9.18 us
  Pallas kernels: 0 us -> 15.7 us
  between operations: 14.5 us -> 0.93 us
  waiting for transfers between devices: 53.6 us -> 60.7 us
  matrix products: 17.6 us -> 12.2 us
  other arithmetic: 5.26 us -> 2.91 us
  starting transfers between devices: 17.7 us -> 19.7 us
    all_to_all x2 -> x0, blocking collectives: 58 us -> none  [the longest x1 53.3 us: per_device(): lax.all_to_all(outgoing, 'ep', split_axis=0, concat_axis=0, tiled=True)]
    all_to_all x3 -> x2, waiting for transfers between devices: 37.9 us -> 55.2 us  [the longest x1 28 us: per_device(): lax.all_to_all(served.reshape(experts, 8, block), 'ep', split_axis=0, con...]
    pallas_call x0 -> x3, Pallas kernels: none -> 15.7 us  [the longest x1 8.76 us: per_device(): pl.pallas_call(expert_body, name='experts', out_shape=jax.ShapeDtypeStruc...]
    all_gather x1 -> x0, waiting for transfers between devices: 15.6 us -> none  [per_device(): lax.all_gather(lax.all_to_all(outgoing, 'ep', split_axis=0, concat_axis=0...]
    reshape x4 -> x1, local copies, waits for them, and re-layouts: 15.6 us -> 0.6 us  [per_device(): moe_gain.reshape(2, half)]
    ppermute x0 -> x8, waiting for transfers between devices: none -> 5.46 us  [swapped(): return lax.ppermute(x, 'tp', SWAP)]
    dot_general x12 -> x8, matrix products: 17.6 us -> 12.2 us  [the longest x1 4.12 us: per_device(): jnp.dot(normed, branch_weight, preferred_element_type=F32).astype(BF)]
    unnamed x50 -> x48, local copies, waits for them, and re-layouts: 2.22 us -> 6.69 us
  transfers between devices with their start and end apart: 4 -> 10, of which waited for: 4 -> 7; matrix products, arithmetic and copies ran while one was open for 2% -> 8% of each run, Pallas kernels for 0% -> 0%
where the time goes in v1:
time: 123 us; the launch traced here: 121 us
  waiting for transfers between devices  60.7 us (49%)
  starting transfers between devices  19.7 us (16%)
  Pallas kernels  15.7 us (13%)
  matrix products  12.2 us (10%)
  local copies, waits for them, and re-layouts  9.18 us (7%)
  other arithmetic  2.91 us (2%)
    all_to_all x1, waiting for transfers between devices, per_device(): lax.all_to_all(served.reshape(experts, 8, block), 'ep', split_axis=0, con...  28 us
    all_to_all x1, waiting for transfers between devices, per_device(): lax.all_to_all(payload.reshape(experts, 8, block), 'ep', split_axis=0, co...  27.2 us
    all_to_all x1, starting transfers between devices, per_device(): lax.all_to_all(payload.reshape(experts, 8, block), 'ep', split_axis=0, co...  11.5 us
    pallas_call x1, Pallas kernels, per_device(): pl.pallas_call(expert_body, name='experts', out_shape=jax.ShapeDtypeStruc...  8.76 us
    unnamed x48, local copies, waits for them, and re-layouts  6.69 us
    all_to_all x1, starting transfers between devices, per_device(): lax.all_to_all(served.reshape(experts, 8, block), 'ep', split_axis=0, con...  5.93 us
    ppermute x8, waiting for transfers between devices, swapped(): return lax.ppermute(x, 'tp', SWAP)  5.46 us
    dot_general x1, matrix products, per_device(): jnp.dot(normed, branch_weight, preferred_element_type=F32).astype(BF)  4.12 us
  transfers between devices with their start and end apart: 10, of which 7 were waited for; matrix products, arithmetic and copies ran while one was open for 8% of the time, Pallas kernels for 0%

profile of v1, /device:TPU:0, one launch (start us, length us, event | category | flops | bytes accessed | tf_op | source)
XLA Modules:
  0.0 121.4 jit_solution(5490047119576107951)
XLA Ops:
  0.6 0.0 copy-start
  0.7 0.1 collective-permute-start
  0.8 0.9 fusion.62
  1.7 0.7 fusion.54
  2.4 1.2 convert_reduce_fusion
  3.6 0.0 copy-start.19
  3.6 0.0 copy-start.22
  3.6 4.1 %fusion.38 = (bf16[64,1024]{1,0:T(8,128)(2,1)S(1)}, bf16[64,1024]{1,0:T(8,128)(2,1)}) fusion(f32[1024]{0:T(1024)S(1)} %bitcast.71, bf16[64,3,1024]{2,0,1:T(8,128)(2,1)} %param.22, f32[1024]{0:T(1024)S(1)} %bitcast.72, f32[1024]{0:T(1024)S(1)} %bitcast.70, f32[1024]{0:T(1024)S(1)} %bitcast.69, bf16[2048,1024]{1,0:T(8,128)(2,1)} %param.25, f32[2048]{0:T(1024)} %param.24, ...), kind=kOutput, calls=%fused_computation.55 | convolution fusion | flops 271122432 | bytes 5136897 | tf_op jit(solution)/shard_map/dot_general | solution.py:231
  7.8 0.2 fusion.3
  8.0 0.2 fusion.7
  8.2 0.2 fusion.31
  8.5 0.0 copy-start.12
  8.5 0.0 copy-start.17
  8.5 1.0 fusion.29
  9.5 0.6 collective-permute-start.1
  10.1 1.0 collective-permute-done.1
  11.1 0.8 fusion.14.own_ref
  12.0 0.4 collective-permute-start.2
  12.4 0.7 copy.28.ids_ref
  13.1 0.6 reshape.64.gain_ref
  13.7 0.6 copy-done.13
  14.4 3.7 %pack.1 = (bf16[512,2304]{1,0:T(8,128)(2,1)}, bf16[64,2048]{1,0:T(8,128)(2,1)}) custom-call(s32[1]{0:T(128)} %bitcast.9.core_ref, bf16[64,1024]{1,0:T(8,128)(2,1)} %copy-done.4, bf16[64,1024]{1,0:T(8,128)(2,1)} %copy-done.13, f32[2,1024]{1,0:T(2,128)} %reshape.64.gain_ref, s32[64,6]{1,0:T(8,128)} %copy.28.ids_ref), custom_call_target="tpu_custom_call" | custom-call | tf_op jit(solution)/shard_map/pack/pallas_call | solution.py:256
  18.1 11.5 %all-to-all-start = ((bf16[64,8,2304]{2,1,0:T(8,128)(2,1)}), bf16[64,8,2304]{2,1,0:T(8,128)(2,1)S(1)}, u32[]{:S(2)}, u32[]{:S(2)}) async-start(bf16[64,8,2304]{2,1,0:T(8,128)(2,1)} %bitcast.61), calls=%async_computation | async-start | bytes 4718592 | tf_op jit(solution)/shard_map/all_to_all | solution.py:269
  29.6 0.1 collective-permute-start.4
  29.7 0.5 collective-permute-start.5
  30.2 0.1 collective-permute-start.6
  30.3 2.3 %collective-permute-done.4.gate2_ref = bf16[2048,256]{1,0:T(8,128)(2,1)S(1)} collective-permute-done((bf16[2048,256]{1,0:T(8,128)(2,1)}, bf16[2048,256]{1,0:T(8,128)(2,1)S(1)}, u32[]{:S(2)}, u32[]{:S(2)}) %collective-permute-start.4) | collective-permute-done | bytes 1048608 | tf_op jit(solution)/shard_map/ppermute | solution.py:17
  32.5 1.5 %collective-permute-done.5.up2_ref = bf16[2048,256]{1,0:T(8,128)(2,1)S(1)} collective-permute-done((bf16[2048,256]{1,0:T(8,128)(2,1)}, bf16[2048,256]{1,0:T(8,128)(2,1)S(1)}, u32[]{:S(2)}, u32[]{:S(2)}) %collective-permute-start.5) | collective-permute-done | bytes 1048608 | tf_op jit(solution)/shard_map/ppermute | solution.py:17
  34.0 1.0 copy-done.7
  35.0 0.6 collective-permute-done.6.down2_ref
  35.7 27.2 %all-to-all-done = bf16[64,8,2304]{2,1,0:T(8,128)(2,1)S(1)} async-done(((bf16[64,8,2304]{2,1,0:T(8,128)(2,1)}), bf16[64,8,2304]{2,1,0:T(8,128)(2,1)S(1)}, u32[]{:S(2)}, u32[]{:S(2)}) %all-to-all-start) | async-done | bytes 2359328 | tf_op jit(solution)/shard_map/all_to_all | solution.py:269
  62.9 1.4 %copy-done.2 = bf16[64,8,2304]{2,1,0:T(8,128)(2,1)} copy-done((bf16[64,8,2304]{2,1,0:T(8,128)(2,1)}, bf16[64,8,2304]{2,1,0:T(8,128)(2,1)S(1)}, u32[]{:S(2)}) %copy-start.2) | copy-done | bytes 2359320
  64.3 8.8 %experts.1 = bf16[512,2304]{1,0:T(8,128)(2,1)} custom-call(s32[1]{0:T(128)} %bitcast.9.core_ref, bf16[512,2304]{1,0:T(8,128)(2,1)} %bitcast.59, bf16[2048,256]{1,0:T(8,128)(2,1)} %bitcast.63, bf16[2048,256]{1,0:T(8,128)(2,1)} %copy-done.6, bf16[2048,256]{1,0:T(8,128)(2,1)} %bitcast.65, bf16[2048,256]{1,0:T(8,128)(2,1)} %copy-done.7, ...), custom_call_target="tpu_custom_call" | custom-call | tf_op jit(solution)/shard_map/experts/pallas_call | solution.py:283
  73.1 5.9 %all-to-all-start.1 = ((bf16[64,8,2304]{2,1,0:T(8,128)(2,1)}), bf16[64,8,2304]{2,1,0:T(8,128)(2,1)S(1)}, u32[]{:S(2)}, u32[]{:S(2)}) async-start(bf16[64,8,2304]{2,1,0:T(8,128)(2,1)} %bitcast.60), calls=%async_computation.1 | async-start | bytes 4718592 | tf_op jit(solution)/shard_map/all_to_all | solution.py:305
  79.1 0.0 copy-start.16
  79.1 0.7 copy.30.weights_ref
  79.8 1.0 fusion.61
  80.8 0.6 copy-done.9
  81.4 0.1 copy-done.10
  81.5 2.2 %fusion.53 = f32[64,256]{1,0:T(8,128)} fusion(bf16[2048,256]{1,0:T(8,128)(2,1)} %param.38, bf16[64,2048]{1,0:T(8,128)(2,1)} %get-tuple-element.7, bf16[64,1024]{1,0:T(8,128)(2,1)S(1)} %get-tuple-element.14, bf16[64,1024]{1,0:T(8,128)(2,1)S(1)} %get-tuple-element.13, pred[]{:T(512)S(6)} %eq.2), kind=kOutput, calls=%fused_computation.75 | convolution fusion | flops 67764224 | bytes 1638401 | tf_op jit(solution)/shard_map/dot_general | solution.py:276
  83.7 28.0 %all-to-all-done.1 = bf16[64,8,2304]{2,1,0:T(8,128)(2,1)S(1)} async-done(((bf16[64,8,2304]{2,1,0:T(8,128)(2,1)}), bf16[64,8,2304]{2,1,0:T(8,128)(2,1)S(1)}, u32[]{:S(2)}, u32[]{:S(2)}) %all-to-all-start.1) | async-done | bytes 2359328 | tf_op jit(solution)/shard_map/all_to_all | solution.py:305
  111.7 1.4 %copy-done.1 = bf16[64,8,2304]{2,1,0:T(8,128)(2,1)} copy-done((bf16[64,8,2304]{2,1,0:T(8,128)(2,1)}, bf16[64,8,2304]{2,1,0:T(8,128)(2,1)S(1)}, u32[]{:S(2)}) %copy-start.1) | copy-done | bytes 2359320
  113.1 3.3 %combine.1 = (f32[64,1024]{1,0:T(8,128)}, f32[64,1024]{1,0:T(8,128)}) custom-call(s32[1]{0:T(128)} %bitcast.9.core_ref, bf16[512,2304]{1,0:T(8,128)(2,1)} %bitcast.58, s32[64,6]{1,0:T(8,128)} %copy.28.ids_ref, f32[64,6]{1,0:T(8,128)} %copy.30.weights_ref), custom_call_target="tpu_custom_call" | custom-call | tf_op jit(solution)/shard_map/combine/pallas_call | solution.py:309
  116.4 1.7 %multiply_convert_fusion = bf16[64,256]{1,0:T(8,128)(2,1)S(1)} fusion(f32[64,256]{1,0:T(8,128)} %fusion.53, bf16[2048,256]{1,0:T(8,128)(2,1)} %param.39, bf16[64,2048]{1,0:T(8,128)(2,1)} %get-tuple-element.7, bf16[64,1024]{1,0:T(8,128)(2,1)} %copy-done.10, bf16[64,1024]{1,0:T(8,128)(2,1)} %copy-done.9, pred[]{:T(512)S(6)} %eq.2), kind=kOutput, calls=%fused_computation.71 | convolution fusion | flops 67862528 | bytes 1671169 | tf_op jit(solution)/shard_map/dot_general | solution.py:277
  118.1 0.5 collective-permute-start.3
  118.6 0.8 pad_maximum_fusion
  119.4 0.1 collective-permute-done.3
  119.5 1.9 %fusion.16 = bf16[64,1024]{1,0:T(8,128)(2,1)} fusion(bf16[512,1024]{1,0:T(8,128)(2,1)S(1)} %copy-done, f32[64,1024]{1,0:T(8,128)} %get-tuple-element.9, f32[64,1024]{1,0:T(8,128)S(1)} %collective-permute-done.7, bf16[64,1024]{1,0:T(8,128)(2,1)S(1)} %copy-done.5, f32[1024]{0:T(1024)S(1)} %copy-done.16, bf16[64,256]{1,0:T(8,128)(2,1)S(1)} %collective-permute-done.3, ...), kind=kOutput, calls=%fused_computation.22 | convolution fusion | flops 67928064 | bytes 1904641 | tf_op jit(solution)/shard_map/dot_general | solution.py:280
  (41 shorter events, 0.1 us)
Async XLA Ops:
  0.6 118.8 %copy-start = (bf16[512,1024]{1,0:T(8,128)(2,1)S(1)}, bf16[512,1024]{1,0:T(8,128)(2,1)}, u32[]{:S(2)}) copy-start(bf16[512,1024]{1,0:T(8,128)(2,1)} %param.40) | copy-start | bytes 3145732
  0.6 7.1 %copy-start.20 = (bf16[8,128,128]{2,1,0:T(8,128)(2,1)S(1)}, bf16[8,128,128]{2,1,0:T(8,128)(2,1)}, u32[]{:S(2)}) copy-start(bf16[8,128,128]{2,1,0:T(8,128)(2,1)} %param.29) | copy-start | bytes 786436
  0.7 7.3 %copy-start.21 = (bf16[8,128,128]{2,1,0:T(8,128)(2,1)S(1)}, bf16[8,128,128]{2,1,0:T(8,128)(2,1)}, u32[]{:S(2)}) copy-start(bf16[8,128,128]{2,1,0:T(8,128)(2,1)} %param.28) | copy-start | bytes 786436
  0.7 7.6 %copy-start.11 = (f32[64,1024]{1,0:T(8,128)S(1)}, f32[64,1024]{1,0:T(8,128)}, u32[]{:S(2)}) copy-start(f32[64,1024]{1,0:T(8,128)} %param.23) | copy-start | bytes 786436
  0.7 1.7 %collective-permute-start = (bf16[64,1024]{1,0:T(8,128)(2,1)}, bf16[64,1024]{1,0:T(8,128)(2,1)S(1)}, u32[]{:S(2)}, u32[]{:S(2)}) collective-permute-start(bf16[64,1024]{1,0:T(8,128)(2,1)} %param.21), channel_id=1, source_target_pairs={{0,1},{1,0},{2,3},{3,2},{4,5},{5,4},{6,7},{7,6},{8,9},{9,8},{10,11... | collective-permute-start | bytes 393224 | tf_op jit(solution)/shard_map/ppermute | solution.py:17
  3.6 4.9 %copy-start.8 = (bf16[64,1024]{1,0:T(8,128)(2,1)S(1)}, bf16[64,1024]{1,0:T(8,128)(2,1)}, u32[]{:S(2)}) copy-start(bf16[64,1024]{1,0:T(8,128)(2,1)} %param.21) | copy-start | bytes 393220
  3.6 4.9 %copy-start.19 = (bf16[2048,1024]{1,0:T(8,128)(2,1)S(1)}, bf16[2048,1024]{1,0:T(8,128)(2,1)}, u32[]{:S(2)}) copy-start(bf16[2048,1024]{1,0:T(8,128)(2,1)} %param.26) | copy-start | bytes 12582916
  3.6 4.9 %copy-start.22 = (f32[2048]{0:T(1024)S(1)}, f32[2048]{0:T(1024)}, u32[]{:S(2)}) copy-start(f32[2048]{0:T(1024)} %param.24) | copy-start | bytes 24580
  7.7 3.3 %copy-start.3 = (bf16[2048,1024]{1,0:T(8,128)(2,1)S(1)}, bf16[2048,1024]{1,0:T(8,128)(2,1)}, u32[]{:S(2)}) copy-start(bf16[2048,1024]{1,0:T(8,128)(2,1)} %param.31) | copy-start | bytes 12582916
  8.5 3.4 %copy-start.12 = (f32[64,1024]{1,0:T(8,128)}, f32[64,1024]{1,0:T(8,128)S(1)}, u32[]{:S(2)}) copy-start(f32[64,1024]{1,0:T(8,128)S(1)} %fusion.31) | copy-start | bytes 786436
  8.5 3.9 %copy-start.17 = (s32[64,6]{0,1:T(8,128)S(1)}, s32[64,6]{0,1:T(8,128)}, u32[]{:S(2)}) copy-start(s32[64,6]{0,1:T(8,128)} %param.33) | copy-start | bytes 4612
  8.5 4.6 %copy-start.15 = (f32[2048]{0:T(1024)S(1)}, f32[2048]{0:T(1024)}, u32[]{:S(2)}) copy-start(f32[2048]{0:T(1024)} %param.32) | copy-start | bytes 24580
  9.5 1.6 %collective-permute-start.1 = (bf16[64,1024]{1,0:T(8,128)(2,1)S(1)}, bf16[64,1024]{1,0:T(8,128)(2,1)S(1)}, u32[]{:S(2)}, u32[]{:S(2)}) collective-permute-start(bf16[64,1024]{1,0:T(8,128)(2,1)S(1)} %fusion.29), channel_id=1, source_target_pairs={{0,1},{1,0},{2,3},{3,2},{4,5},{5,4},{6,7},{7,6},{8,9},{9,8},{10,11... | collective-permute-start | bytes 393224 | tf_op jit(solution)/shard_map/ppermute | solution.py:17
  12.0 1.8 %copy-start.4 = (bf16[64,1024]{1,0:T(8,128)(2,1)}, bf16[64,1024]{1,0:T(8,128)(2,1)S(1)}, u32[]{:S(2)}) copy-start(bf16[64,1024]{1,0:T(8,128)(2,1)S(1)} %fusion.14.own_ref) | copy-start | bytes 393220
  12.0 1.8 %collective-permute-start.2 = (bf16[64,1024]{1,0:T(8,128)(2,1)S(1)}, bf16[64,1024]{1,0:T(8,128)(2,1)S(1)}, u32[]{:S(2)}, u32[]{:S(2)}) collective-permute-start(bf16[64,1024]{1,0:T(8,128)(2,1)S(1)} %fusion.14.own_ref), channel_id=1, source_target_pairs={{0,1},{1,0},{2,3},{3,2},{4,5},{5,4},{6,7},{7,6},{8,9},{9,8},{10,11... | collective-permute-start | bytes 393224 | tf_op jit(solution)/shard_map/ppermute | solution.py:17
  13.7 0.7 copy-start.13
  18.1 44.9 %all-to-all-start = ((bf16[64,8,2304]{2,1,0:T(8,128)(2,1)}), bf16[64,8,2304]{2,1,0:T(8,128)(2,1)S(1)}, u32[]{:S(2)}, u32[]{:S(2)}) async-start(bf16[64,8,2304]{2,1,0:T(8,128)(2,1)} %bitcast.61), calls=%async_computation | async-start | bytes 4718592 | tf_op jit(solution)/shard_map/all_to_all | solution.py:269
  29.6 3.0 %collective-permute-start.4 = (bf16[2048,256]{1,0:T(8,128)(2,1)}, bf16[2048,256]{1,0:T(8,128)(2,1)S(1)}, u32[]{:S(2)}, u32[]{:S(2)}) collective-permute-start(bf16[2048,256]{1,0:T(8,128)(2,1)} %bitcast.62), channel_id=1, source_target_pairs={{0,1},{1,0},{2,3},{3,2},{4,5},{5,4},{6,7},{7,6},{8,9},{9,8},{10,11... | collective-permute-start | bytes 3145736 | tf_op jit(solution)/shard_map/ppermute | solution.py:17
  29.7 4.4 %collective-permute-start.5 = (bf16[2048,256]{1,0:T(8,128)(2,1)}, bf16[2048,256]{1,0:T(8,128)(2,1)S(1)}, u32[]{:S(2)}, u32[]{:S(2)}) collective-permute-start(bf16[2048,256]{1,0:T(8,128)(2,1)} %bitcast.64), channel_id=1, source_target_pairs={{0,1},{1,0},{2,3},{3,2},{4,5},{5,4},{6,7},{7,6},{8,9},{9,8},{10,11... | collective-permute-start | bytes 3145736 | tf_op jit(solution)/shard_map/ppermute | solution.py:17
  30.2 5.5 %collective-permute-start.6 = (bf16[512,1024]{1,0:T(8,128)(2,1)}, bf16[512,1024]{1,0:T(8,128)(2,1)}, u32[]{:S(2)}, u32[]{:S(2)}) collective-permute-start(bf16[512,1024]{1,0:T(8,128)(2,1)} %bitcast.66), channel_id=1, source_target_pairs={{0,1},{1,0},{2,3},{3,2},{4,5},{5,4},{6,7},{7,6},{8,9},{9,8},{10,11... | collective-permute-start | bytes 3145736 | tf_op jit(solution)/shard_map/ppermute | solution.py:17
  32.5 1.5 %copy-start.6 = (bf16[2048,256]{1,0:T(8,128)(2,1)}, bf16[2048,256]{1,0:T(8,128)(2,1)S(1)}, u32[]{:S(2)}) copy-start(bf16[2048,256]{1,0:T(8,128)(2,1)S(1)} %collective-permute-done.4.gate2_ref) | copy-start | bytes 3145732
  34.0 1.0 copy-start.7
  62.9 1.4 %copy-start.2 = (bf16[64,8,2304]{2,1,0:T(8,128)(2,1)}, bf16[64,8,2304]{2,1,0:T(8,128)(2,1)S(1)}, u32[]{:S(2)}) copy-start(bf16[64,8,2304]{2,1,0:T(8,128)(2,1)S(1)} %all-to-all-done) | copy-start | bytes 7077892
  73.1 6.0 %copy-start.18 = (f32[64,6]{0,1:T(8,128)S(1)}, f32[64,6]{0,1:T(8,128)}, u32[]{:S(2)}) copy-start(f32[64,6]{0,1:T(8,128)} %param.34) | copy-start | bytes 4612
  73.1 38.6 %all-to-all-start.1 = ((bf16[64,8,2304]{2,1,0:T(8,128)(2,1)}), bf16[64,8,2304]{2,1,0:T(8,128)(2,1)S(1)}, u32[]{:S(2)}, u32[]{:S(2)}) async-start(bf16[64,8,2304]{2,1,0:T(8,128)(2,1)} %bitcast.60), calls=%async_computation.1 | async-start | bytes 4718592 | tf_op jit(solution)/shard_map/all_to_all | solution.py:305
  79.0 40.4 %copy-start.5 = (bf16[64,1024]{1,0:T(8,128)(2,1)S(1)}, bf16[64,1024]{1,0:T(8,128)(2,1)}, u32[]{:S(2)}) copy-start(bf16[64,1024]{1,0:T(8,128)(2,1)} %copy-done.4) | copy-start | bytes 393220
  79.1 40.4 %copy-start.16 = (f32[1024]{0:T(1024)S(1)}, f32[1024]{0:T(1024)}, u32[]{:S(2)}) copy-start(f32[1024]{0:T(1024)} %param.41) | copy-start | bytes 12292
  80.8 0.6 copy-start.9
  80.8 0.7 copy-start.10
  111.7 1.4 %copy-start.1 = (bf16[64,8,2304]{2,1,0:T(8,128)(2,1)}, bf16[64,8,2304]{2,1,0:T(8,128)(2,1)S(1)}, u32[]{:S(2)}) copy-start(bf16[64,8,2304]{2,1,0:T(8,128)(2,1)S(1)} %all-to-all-done.1) | copy-start | bytes 7077892
  111.7 6.9 %slice-start = ((bf16[64,3,1024]{2,0,1:T(8,128)(2,1)}), bf16[64,2,1024]{2,0,1:T(8,128)(2,1)S(1)}, s32[]{:S(2)}) async-start(bf16[64,3,1024]{2,0,1:T(8,128)(2,1)} %param.22), calls=%async_computation.2 | async-start | bytes 524288 | tf_op jit(solution)/shard_map/slice | solution.py:237
  111.7 6.9 %copy-start.14 = (bf16[64,1024]{1,0:T(8,128)(2,1)S(1)}, bf16[64,1024]{1,0:T(8,128)(2,1)}, u32[]{:S(2)}) copy-start(bf16[64,1024]{1,0:T(8,128)(2,1)} %get-tuple-element.22) | copy-start | bytes 393220
  116.4 3.0 %collective-permute-start.7 = (f32[64,1024]{1,0:T(8,128)}, f32[64,1024]{1,0:T(8,128)S(1)}, u32[]{:S(2)}, u32[]{:S(2)}) collective-permute-start(f32[64,1024]{1,0:T(8,128)} %get-tuple-element.10), channel_id=1, source_target_pairs={{0,1},{1,0},{2,3},{3,2},{4,5},{5,4},{6,7},{7,6},{8,9},{9,8},{10,11... | collective-permute-start | bytes 786440 | tf_op jit(solution)/shard_map/ppermute | solution.py:17
  118.1 1.4 %collective-permute-start.3 = (bf16[64,256]{1,0:T(8,128)(2,1)S(1)}, bf16[64,256]{1,0:T(8,128)(2,1)S(1)}, u32[]{:S(2)}, u32[]{:S(2)}) collective-permute-start(bf16[64,256]{1,0:T(8,128)(2,1)S(1)} %multiply_convert_fusion), channel_id=1, source_target_pairs={{0,1},{1,0},{2,3},{3,2},{4,5},{5,4},{6,7},{7,6},{8,9},{9,8},{10,11... | collective-permute-start | bytes 98312 | tf_op jit(solution)/shard_map/ppermute | solution.py:17

commit v2 on v1

v2 whole, which is shorter than its diff:
```python
import functools

import jax
import jax.numpy as jnp
from jax import lax
from jax.experimental import pallas as pl
from jax.experimental.pallas import tpu as pltpu
from jax.sharding import PartitionSpec as P


BF = jnp.bfloat16
F32 = jnp.float32
SWAP = [(0, 1), (1, 0)]
MIB = 1024 * 1024
LANES = 128
SLOTS = 9
MAIN = 8
CHUNKS = 4


def swapped(x):
    return lax.ppermute(x, "tp", SWAP)


def in_order(core, own, other):
    return jnp.where(
        core == 0,
        jnp.concatenate([own, other], axis=1),
        jnp.concatenate([other, own], axis=1),
    )


def places(ids, core):
    experts = rows = ids.shape[1]
    expert = lax.broadcasted_iota(jnp.int32, (experts, rows), 0)
    hits = [ids[k : k + 1, :] == expert for k in range(ids.shape[0])]
    chosen = functools.reduce(jnp.logical_or, hits)
    earlier = lax.broadcasted_iota(jnp.int32, (rows, rows), 0) < lax.broadcasted_iota(
        jnp.int32, (rows, rows), 1
    )
    rank = jnp.dot(
        jnp.where(chosen, 1.0, 0.0).astype(BF),
        jnp.where(earlier, 1.0, 0.0).astype(BF),
        preferred_element_type=F32,
    )
    return hits, jnp.where(chosen, rank - (SLOTS * core).astype(F32), -1.0)


def each_slot(values):
    experts = values.shape[0]
    shape = (experts * MAIN, experts)
    row = lax.broadcasted_iota(jnp.int32, shape, 0) // MAIN
    spread = jnp.where(row == lax.broadcasted_iota(jnp.int32, shape, 1), 1.0, 0.0).astype(BF)
    return jnp.dot(spread, values.astype(BF), preferred_element_type=F32)


def slot_number(shape):
    return (lax.broadcasted_iota(jnp.int32, shape, 0) % MAIN).astype(F32)


def put_pieces(piece_ref, values, start, base):
    count = values.shape[0]
    for n in range(values.shape[1] // LANES):
        c, part = divmod(start + n, 2)
        piece_ref[part, pl.ds(base + c, count, stride=MAIN), :] = values[
            :, n * LANES : (n + 1) * LANES
        ]


def take_pieces(piece_ref, block_ref, features, rows_ref, start):
    count = block_ref.shape[0] // MAIN
    piece_ref[0] = block_ref[:, features : features + LANES].astype(F32)
    piece_ref[1] = block_ref[:, features + LANES :].astype(F32)
    for n in range(features // LANES):
        c, part = divmod(n, 2)
        rows_ref[start : start + count, n * LANES : (n + 1) * LANES] = piece_ref[
            part, pl.ds(c, count, stride=MAIN), :
        ].astype(BF)


def pack_body(
    core_ref,
    own_ref,
    other_ref,
    gain_ref,
    ids_ref,
    out_ref,
    norm_out_ref,
    norm_ref,
    block_ref,
    piece_ref,
    sems,
):
    core = core_ref[0]
    half = own_ref.shape[1]
    features = 2 * half
    own = own_ref[...].astype(F32)
    other = other_ref[...].astype(F32)
    mean = (jnp.sum(own, 1, keepdims=True) + jnp.sum(other, 1, keepdims=True)) / features
    square = (
        jnp.sum(own * own, 1, keepdims=True) + jnp.sum(other * other, 1, keepdims=True)
    ) / features
    scale = lax.rsqrt(square - mean * mean + 1e-05)
    low, high = gain_ref[:, :half], gain_ref[:, half:]
    gain_own = jnp.where(core == 0, low, high)
    gain_other = jnp.where(core == 0, high, low)
    norm_ref[:, :half] = ((own - mean) * scale * gain_own).astype(BF)
    norm_ref[:, half:] = ((other - mean) * scale * gain_other).astype(BF)
    norm_copy = pltpu.make_async_copy(norm_ref, norm_out_ref, sems.at[CHUNKS])
    norm_copy.start()
    rows = norm_ref[...]
    experts = ids_ref.shape[1]
    _, place = places(ids_ref[...], core)
    wide = each_slot(place)
    table = jnp.where(wide == slot_number(wide.shape), 1.0, 0.0).astype(BF)
    last = jnp.where(place == float(MAIN), 1.0, 0.0).astype(BF)
    ninth = jnp.dot(last, rows, preferred_element_type=F32)
    put_pieces(piece_ref, ninth, 0, 0)
    count = experts * MAIN
    step = count // CHUNKS
    copies = [norm_copy]
    for n in range(CHUNKS):
        span = slice(n * step, (n + 1) * step)
        block_ref[span, :features] = jnp.dot(
            table[span], rows, preferred_element_type=F32
        ).astype(BF)
        block_ref[span, features : features + LANES] = piece_ref[0, span].astype(BF)
        block_ref[span, features + LANES :] = piece_ref[1, span].astype(BF)
        copy = pltpu.make_async_copy(block_ref.at[span], out_ref.at[span], sems.at[n])
        copy.start()
        copies.append(copy)
    for copy in copies:
        copy.wait()


def table_body(core_ref, ids_ref, weights_ref, table_ref, last_ref):
    rows = ids_ref.shape[1]
    hits, place = places(ids_ref[...], core_ref[0])
    weight = functools.reduce(
        jnp.add,
        [jnp.where(hit, weights_ref[k : k + 1, :], 0.0) for k, hit in enumerate(hits)],
    )
    high = weight.astype(BF).astype(F32)
    low = (weight - high).astype(BF).astype(F32)
    wide = each_slot(place)
    match = wide == slot_number(wide.shape)
    for n, part in enumerate((high, low)):
        span = slice(n * rows, (n + 1) * rows)
        table_ref[span, :] = jnp.transpose(jnp.where(match, each_slot(part), 0.0)).astype(BF)
        last_ref[span, :] = jnp.transpose(jnp.where(place == float(MAIN), part, 0.0)).astype(BF)


def expert_body(
    core_ref,
    in_ref,
    gate_ref,
    gate2_ref,
    up_ref,
    up2_ref,
    down_ref,
    down2_ref,
    out_ref,
    gates_ref,
    ups_ref,
    downs_ref,
    block_ref,
    piece_ref,
    take_ref,
    rows_ref,
    sems,
    out_sems,
):
    core = core_ref[0]
    features, units = gate_ref.shape
    half = features // 2
    starts = (pl.multiple_of(core * half, half), pl.multiple_of((1 - core) * half, half))
    unit_starts = (
        pl.multiple_of(core * units, units),
        pl.multiple_of((1 - core) * units, units),
    )
    loads = []
    for whole, parts, size, width, offsets in (
        (gates_ref, (gate_ref, gate2_ref), half, units, starts),
        (ups_ref, (up_ref, up2_ref), half, units, starts),
        (downs_ref, (down_ref, down2_ref), units, half, unit_starts),
    ):
        group = []
        for column, part in enumerate(parts):
            for row, start in enumerate(offsets):
                copy = pltpu.make_async_copy(
                    part.at[pl.ds(start, size), :],
                    whole.at[pl.ds(row * size, size), pl.ds(column * width, width)],
                    sems.at[4 * len(loads) + len(group)],
                )
                copy.start()
                group.append(copy)
        loads.append(group)
    count = in_ref.shape[0]
    step = count // CHUNKS
    take_pieces(take_ref, in_ref, features, rows_ref, 0)
    main, last = in_ref[:, :features], rows_ref[...]

    def product(weight):
        return jnp.concatenate(
            [
                jnp.dot(main, weight, preferred_element_type=F32),
                jnp.dot(last, weight, preferred_element_type=F32),
            ],
            axis=0,
        )

    for copy in loads[0]:
        copy.wait()
    gate = product(gates_ref[...])
    for copy in loads[1]:
        copy.wait()
    hidden = (jax.nn.silu(gate) * product(ups_ref[...])).astype(BF)
    for copy in loads[2]:
        copy.wait()
    served = jnp.dot(hidden[count:], downs_ref[...], preferred_element_type=F32)
    put_pieces(piece_ref, served, 0, 0)
    copies = []
    for n in range(CHUNKS):
        span = slice(n * step, (n + 1) * step)
        block_ref[span, :features] = jnp.dot(
            hidden[span], downs_ref[...], preferred_element_type=F32
        ).astype(BF)
        block_ref[span, features : features + LANES] = piece_ref[0, span].astype(BF)
        block_ref[span, features + LANES :] = piece_ref[1, span].astype(BF)
        copy = pltpu.make_async_copy(block_ref.at[span], out_ref.at[span], out_sems.at[n])
        copy.start()
        copies.append(copy)
    for copy in copies:
        copy.wait()


def combine_body(in_ref, table_ref, lasts_ref, own_ref, other_ref, piece_ref, last_ref):
    rows, half = own_ref.shape
    features = 2 * half
    take_pieces(piece_ref, in_ref, features, last_ref, 0)
    total = jnp.dot(
        table_ref[...], in_ref[:, :features], preferred_element_type=F32
    ) + jnp.dot(lasts_ref[...], last_ref[...], preferred_element_type=F32)
    total = total[:rows] + total[rows:]
    own_ref[...] = total[:, :half]
    other_ref[...] = total[:, half:]


def vmem(count):
    return [pl.BlockSpec(memory_space=pltpu.VMEM)] * count


def hbm(count):
    return [pl.BlockSpec(memory_space=pltpu.HBM)] * count


def smem():
    return [pl.BlockSpec(memory_space=pltpu.SMEM)]


def per_device(
    stream,
    conv_state,
    recur_state,
    mix_gain,
    branch_weight,
    gate_weight,
    conv_taps,
    recur_map,
    input_map,
    decay_logit,
    out_weight,
    moe_gain,
    route_ids,
    route_weights,
    expert_gate,
    expert_up,
    expert_down,
    dense_gate,
    dense_up,
    dense_down,
    dense_scale,
):
    core = lax.axis_index("tp")
    core_arr = core.astype(jnp.int32).reshape(1)
    seq_count, half = stream.shape
    features = 2 * half
    experts = lax.axis_size("ep")
    own_gate, own_up, own_down = expert_gate[0], expert_up[0], expert_down[0]
    stream_other = swapped(stream)

    whole = in_order(core, stream, stream_other).astype(F32)
    mean = jnp.mean(whole, axis=1, keepdims=True)
    var = jnp.mean(whole * whole, axis=1, keepdims=True) - mean * mean
    normed = ((whole - mean) * lax.rsqrt(var + 1e-05) * mix_gain).astype(BF)
    branch_in = jnp.dot(normed, branch_weight, preferred_element_type=F32).astype(BF)
    gate_pre = jnp.dot(normed, gate_weight, preferred_element_type=F32).astype(BF)
    conv_sum = branch_in.astype(F32) * conv_taps[3]
    for offset in range(3):
        conv_sum = conv_sum + conv_state[:, offset].astype(F32) * conv_taps[offset]
    conv_out = conv_sum.astype(BF)
    new_conv = jnp.concatenate([conv_state[:, 1:], branch_in[:, None]], axis=1)
    block_count, block_width = recur_map.shape[0], recur_map.shape[1]
    grouped = conv_out.reshape(seq_count, block_count, block_width)
    recur_gate = jax.nn.sigmoid(
        jnp.einsum("nbc,bcd->nbd", grouped, recur_map, preferred_element_type=F32)
    ).reshape(seq_count, -1)
    input_gate = jax.nn.sigmoid(
        jnp.einsum("nbc,bcd->nbd", grouped, input_map, preferred_element_type=F32)
    ).reshape(seq_count, -1)
    log_decay = -8.0 * recur_gate * jax.nn.softplus(-decay_logit)
    driven = jnp.sqrt(-jnp.expm1(2.0 * log_decay)) * (input_gate * conv_out.astype(F32))
    new_state = jnp.exp(log_decay) * recur_state + driven
    mixer_in = (jax.nn.gelu(gate_pre.astype(F32)) * new_state).astype(BF)
    mixer_whole = in_order(core, mixer_in, swapped(mixer_in))
    mixer_out = jnp.dot(mixer_whole, out_weight, preferred_element_type=F32).astype(BF)
    resid = (stream.astype(F32) + mixer_out.astype(F32)).astype(BF)
    resid_other = swapped(resid)

    block = features + features // MAIN
    count = experts * MAIN
    pieces = pltpu.VMEM((2, count, LANES), F32)
    ids_t, weights_t = route_ids.T, route_weights.T
    payload, normed_two = pl.pallas_call(
        pack_body,
        name="pack",
        out_shape=(pltpu.HBM((count, block), BF), pltpu.HBM((seq_count, features), BF)),
        in_specs=smem() + vmem(4),
        out_specs=tuple(hbm(2)),
        scratch_shapes=[
            pltpu.VMEM((seq_count, features), BF),
            pltpu.VMEM((count, block), BF),
            pieces,
            pltpu.SemaphoreType.DMA((CHUNKS + 1,)),
        ],
        compiler_params=pltpu.CompilerParams(vmem_limit_bytes=14 * MIB),
    )(core_arr, resid, resid_other, moe_gain.reshape(1, features), ids_t)

    own_gate, own_up, own_down, payload = lax.optimization_barrier(
        (own_gate, own_up, own_down, payload)
    )
    other_gate, other_up, other_down = swapped(own_gate), swapped(own_up), swapped(own_down)
    incoming = lax.all_to_all(
        payload.reshape(experts, MAIN, block), "ep", split_axis=0, concat_axis=0, tiled=True
    )
    incoming = incoming.reshape(count, block)
    units = own_gate.shape[1]
    table, last = pl.pallas_call(
        table_body,
        name="table",
        out_shape=(
            jax.ShapeDtypeStruct((2 * seq_count, count), BF),
            jax.ShapeDtypeStruct((2 * seq_count, experts), BF),
        ),
        in_specs=smem() + vmem(2),
        out_specs=tuple(vmem(2)),
        compiler_params=pltpu.CompilerParams(vmem_limit_bytes=8 * MIB),
    )(core_arr, ids_t, weights_t)

    own_two, other_two = normed_two[:, :half], normed_two[:, half:]
    whole_two = in_order(core, own_two, other_two)
    dense_hidden = (
        jax.nn.silu(jnp.dot(whole_two, dense_gate, preferred_element_type=F32))
        * jnp.dot(whole_two, dense_up, preferred_element_type=F32)
    ).astype(BF)
    dense_whole = in_order(core, dense_hidden, swapped(dense_hidden))
    dense_out = jnp.dot(dense_whole, dense_down, preferred_element_type=F32).astype(BF)
    base = resid.astype(F32) + dense_scale * dense_out.astype(F32)

    incoming, base, new_conv, new_state, table, last = lax.optimization_barrier(
        (incoming, base, new_conv, new_state, table, last)
    )
    served = pl.pallas_call(
        expert_body,
        name="experts",
        out_shape=pltpu.HBM((count, block), BF),
        in_specs=smem() + vmem(1) + hbm(6),
        out_specs=hbm(1)[0],
        scratch_shapes=[
            pltpu.VMEM((features, 2 * units), BF),
            pltpu.VMEM((features, 2 * units), BF),
            pltpu.VMEM((2 * units, features), BF),
            pltpu.VMEM((count, block), BF),
            pieces,
            pieces,
            pltpu.VMEM((experts, features), BF),
            pltpu.SemaphoreType.DMA((12,)),
            pltpu.SemaphoreType.DMA((CHUNKS,)),
        ],
        compiler_params=pltpu.CompilerParams(vmem_limit_bytes=28 * MIB),
    )(
        core_arr,
        incoming,
        *(
            pltpu.with_memory_space_constraint(weight, pltpu.HBM)
            for weight in (own_gate, other_gate, own_up, other_up, own_down, other_down)
        ),
    )

    returned = lax.all_to_all(
        served.reshape(experts, MAIN, block), "ep", split_axis=0, concat_axis=0, tiled=True
    )
    returned = returned.reshape(count, block)
    sum_own, sum_other = pl.pallas_call(
        combine_body,
        name="combine",
        out_shape=(
            jax.ShapeDtypeStruct((seq_count, half), F32),
            jax.ShapeDtypeStruct((seq_count, half), F32),
        ),
        in_specs=vmem(3),
        out_specs=tuple(vmem(2)),
        scratch_shapes=[pieces, pltpu.VMEM((experts, features), BF)],
        compiler_params=pltpu.CompilerParams(vmem_limit_bytes=14 * MIB),
    )(returned, table, last)
    result = (base + (sum_own + swapped(sum_other))).astype(BF)
    return (result, new_state, new_conv)


def solution(mesh):
    in_specs = (
        P("ep", "tp"),
        P("ep", None, "tp"),
        P("ep", "tp"),
        P(),
        P(None, "tp"),
        P(None, "tp"),
        P(None, "tp"),
        P("tp", None, None),
        P("tp", None, None),
        P("tp"),
        P(None, "tp"),
        P(),
        P("ep", None),
        P("ep", None),
        P("ep", None, "tp"),
        P("ep", None, "tp"),
        P("ep", None, "tp"),
        P(None, "tp"),
        P(None, "tp"),
        P(None, "tp"),
        P("tp"),
    )
    out_specs = (P("ep", "tp"), P("ep", "tp"), P("ep", None, "tp"))
    return jax.shard_map(
        per_device, mesh=mesh, in_specs=in_specs, out_specs=out_specs, check_vma=False
    )
```

time: 123 us -> 111 us (0.902)
  blocking collectives: 0 us -> 38.6 us
  waiting for transfers between devices: 60.7 us -> 28.4 us
  starting transfers between devices: 19.7 us -> 13.6 us
  local copies, waits for them, and re-layouts: 9.18 us -> 3.23 us
  Pallas kernels: 15.7 us -> 10.5 us
  matrix products: 12.2 us -> 10.7 us
    all_to_all x0 -> x1, blocking collectives: none -> 38.6 us  [per_device(): lax.all_to_all(served.reshape(experts, MAIN, block), 'ep', split_axis=0,...]
    all_to_all x2 -> x1, waiting for transfers between devices: 55.2 us -> 24.8 us  [per_device(): lax.all_to_all(payload.reshape(experts, MAIN, block), 'ep', split_axis=0,...]
    all_to_all x2 -> x1, starting transfers between devices: 17.5 us -> 11.5 us  [per_device(): lax.all_to_all(payload.reshape(experts, MAIN, block), 'ep', split_axis=0,...]
    unnamed x48 -> x38, local copies, waits for them, and re-layouts: 6.69 us -> 1.34 us
    pallas_call x1, Pallas kernels: 3.27 us -> 0.61 us  [per_device(): pl.pallas_call(combine_body, name='combine', out_shape=(jax.ShapeDtypeStr...]
    pallas_call x2 -> x3, Pallas kernels: 12.4 us -> 9.85 us  [the longest x1 7.33 us: per_device(): pl.pallas_call(expert_body, name='experts', out_shape=pltpu.HBM((count, b...]
    ppermute x8, waiting for transfers between devices: 5.46 us -> 3.67 us  [swapped(): return lax.ppermute(x, 'tp', SWAP)]
  transfers between devices with their start and end apart: 10 -> 9, of which waited for: 7 -> 5; matrix products, arithmetic and copies ran while one was open for 8% -> 7% of each run, Pallas kernels for 0% -> 0%
where the time goes in v2:
time: 111 us; the launch traced here: 110 us
  blocking collectives  38.6 us (35%)
  waiting for transfers between devices  28.4 us (26%)
  starting transfers between devices  13.6 us (12%)
  matrix products  10.7 us (10%)
  Pallas kernels  10.5 us (9%)
  other arithmetic  3.62 us (3%)
  local copies, waits for them, and re-layouts  3.23 us (3%)
    all_to_all x1, blocking collectives, per_device(): lax.all_to_all(served.reshape(experts, MAIN, block), 'ep', split_axis=0,...  38.6 us
    all_to_all x1, waiting for transfers between devices, per_device(): lax.all_to_all(payload.reshape(experts, MAIN, block), 'ep', split_axis=0,...  24.8 us
    all_to_all x1, starting transfers between devices, per_device(): lax.all_to_all(payload.reshape(experts, MAIN, block), 'ep', split_axis=0,...  11.5 us
    pallas_call x1, Pallas kernels, per_device(): pl.pallas_call(expert_body, name='experts', out_shape=pltpu.HBM((count, b...  7.33 us
    dot_general x1, matrix products, per_device(): jnp.dot(normed, branch_weight, preferred_element_type=F32).astype(BF)  4.12 us
    ppermute x8, waiting for transfers between devices, swapped(): return lax.ppermute(x, 'tp', SWAP)  3.67 us
  transfers between devices with their start and end apart: 9, of which 5 were waited for; matrix products, arithmetic and copies ran while one was open for 7% of the time, Pallas kernels for 0%

profile of v2, /device:TPU:0, one launch (start us, length us, event | category | flops | bytes accessed | tf_op | source)
XLA Modules:
  0.0 109.7 jit_solution(10281228957974721979)
XLA Ops:
  0.6 0.0 copy-start
  0.7 0.1 collective-permute-start
  0.8 0.9 fusion.60
  1.7 0.7 fusion.52
  2.4 0.0 collective-permute-done
  2.4 1.2 %convert_reduce_fusion = (f32[64]{0:T(128)S(1)}, f32[64]{0:T(128)S(1)}) fusion(bf16[64,1024]{1,0:T(8,128)(2,1)} %param.21, bf16[64,1024]{1,0:T(8,128)(2,1)S(1)} %collective-permute-done, pred[]{:T(512)S(6)} %eq.2), kind=kLoop, calls=%fused_computation.23 | loop fusion | flops 1703808 | bytes 262657 | tf_op jit(solution)/shard_map/reduce_sum | solution.py:293
  3.6 0.0 copy-start.10
  3.6 0.0 copy-start.15
  3.6 0.0 copy-start.18
  3.6 4.1 %fusion.36 = (bf16[64,1024]{1,0:T(8,128)(2,1)S(1)}, bf16[64,1024]{1,0:T(8,128)(2,1)}) fusion(f32[1024]{0:T(1024)S(1)} %bitcast.78, bf16[64,3,1024]{2,0,1:T(8,128)(2,1)} %param.22, f32[1024]{0:T(1024)S(1)} %bitcast.79, f32[1024]{0:T(1024)S(1)} %bitcast.77, f32[1024]{0:T(1024)S(1)} %bitcast.76, bf16[2048,1024]{1,0:T(8,128)(2,1)} %param.25, f32[2048]{0:T(1024)} %param.24, ...), kind=kOutput, calls=%fused_computation.53 | convolution fusion | flops 271122432 | bytes 5136897 | tf_op jit(solution)/shard_map/dot_general | solution.py:296
  7.8 0.2 fusion.3
  8.0 0.2 fusion.7
  8.2 0.2 fusion.29
  8.5 0.0 copy-start.12
  8.5 0.0 copy-start.5
  8.5 0.0 copy-start.6
  8.5 1.0 fusion.27
  9.5 0.0 copy-start.7
  9.6 0.6 collective-permute-start.1
  10.1 1.0 collective-permute-done.1
  11.1 0.9 fusion.13.own_ref
  12.0 0.4 collective-permute-start.2
  12.4 1.0 collective-permute-done.2.other_ref
  13.4 2.0 %pack.1 = (bf16[512,2304]{1,0:T(8,128)(2,1)}, bf16[64,2048]{1,0:T(8,128)(2,1)}) custom-call(s32[1]{0:T(128)} %bitcast.3.core_ref, bf16[64,1024]{1,0:T(8,128)(2,1)S(1)} %fusion.13.own_ref, bf16[64,1024]{1,0:T(8,128)(2,1)S(1)} %collective-permute-done.2.other_ref, f32[1,2048]{1,0:T(1,128)S(1)} %bitcast.65, s32[6,64]{1,0:T(8,128)S(1)} %bitcast.63), custom_call_target="tpu_custom_call" | custom-call | tf_op jit(solution)/shard_map/pack/pallas_call | solution.py:324
  15.5 0.0 copy-start.14
  15.5 11.5 %all-to-all-start = ((bf16[64,8,2304]{2,1,0:T(8,128)(2,1)}), bf16[64,8,2304]{2,1,0:T(8,128)(2,1)S(1)}, u32[]{:S(2)}, u32[]{:S(2)}) async-start(bf16[64,8,2304]{2,1,0:T(8,128)(2,1)} %bitcast.68), calls=%async_computation | async-start | bytes 4718592 | tf_op jit(solution)/shard_map/all_to_all | solution.py:343
  27.0 0.0 slice-start
  27.0 0.0 copy-start.13
  27.1 0.5 table.1
  27.6 0.6 copy-done.1
  28.2 0.6 copy-done.3
  28.8 0.1 collective-permute-start.4
  28.9 0.4 collective-permute-start.5
  29.3 0.1 collective-permute-start.6
  29.4 1.0 fusion.59
  30.4 1.6 %fusion.51 = f32[64,256]{1,0:T(8,128)S(1)} fusion(bf16[2048,256]{1,0:T(8,128)(2,1)} %param.38, bf16[64,2048]{1,0:T(8,128)(2,1)} %get-tuple-element.21, bf16[64,1024]{1,0:T(8,128)(2,1)S(1)} %get-tuple-element.38, bf16[64,1024]{1,0:T(8,128)(2,1)S(1)} %get-tuple-element.37, pred[]{:T(512)S(6)} %eq.2), kind=kOutput, calls=%fused_computation.74 | convolution fusion | flops 67764224 | bytes 1638401 | tf_op jit(solution)/shard_map/dot_general | solution.py:363
  32.0 1.6 %multiply_convert_fusion = bf16[64,256]{1,0:T(8,128)(2,1)S(1)} fusion(f32[64,256]{1,0:T(8,128)S(1)} %fusion.51, bf16[2048,256]{1,0:T(8,128)(2,1)} %param.39, bf16[64,2048]{1,0:T(8,128)(2,1)} %get-tuple-element.21, bf16[64,1024]{1,0:T(8,128)(2,1)S(1)} %get-tuple-element.38, bf16[64,1024]{1,0:T(8,128)(2,1)S(1)} %get-tuple-element.37, pred[]{:T(512)S(6)} %eq.2), kind=kOutput, calls=%fused_computation.70 | convolution fusion | flops 67862528 | bytes 1671169 | tf_op jit(solution)/shard_map/dot_general | solution.py:364
  33.6 0.3 collective-permute-start.3
  34.0 0.8 pad_maximum_fusion
  34.7 0.2 collective-permute-done.3
  34.9 1.0 fusion.10
  35.9 24.8 %all-to-all-done = bf16[64,8,2304]{2,1,0:T(8,128)(2,1)S(1)} async-done(((bf16[64,8,2304]{2,1,0:T(8,128)(2,1)}), bf16[64,8,2304]{2,1,0:T(8,128)(2,1)S(1)}, u32[]{:S(2)}, u32[]{:S(2)}) %all-to-all-start) | async-done | bytes 2359328 | tf_op jit(solution)/shard_map/all_to_all | solution.py:343
  60.7 7.3 %experts.1 = bf16[512,2304]{1,0:T(8,128)(2,1)} custom-call(s32[1]{0:T(128)} %bitcast.3.core_ref, bf16[512,2304]{1,0:T(8,128)(2,1)S(1)} %bitcast.62, bf16[2048,256]{1,0:T(8,128)(2,1)} %bitcast.70, bf16[2048,256]{1,0:T(8,128)(2,1)} %collective-permute-done.4.gate2_ref, bf16[2048,256]{1,0:T(8,128)(2,1)} %bitcast.72, ...), custom_call_target="tpu_custom_call" | custom-call | tf_op jit(solution)/shard_map/experts/pallas_call | solution.py:373
  68.1 38.6 %all_to_all.10 = bf16[64,8,2304]{2,1,0:T(8,128)(2,1)S(1)} all-to-all(bf16[64,8,2304]{2,1,0:T(8,128)(2,1)} %bitcast.67), channel_id=1, replica_groups=mesh['ep'=64,'tp'=2] {'ep'}, dimensions={0} | all-to-all | bytes 4718592 | tf_op jit(solution)/shard_map/all_to_all | solution.py:400
  106.7 0.6 combine.1
  107.3 0.1 collective-permute-start.7
  107.4 1.5 %collective-permute-done.7 = f32[64,1024]{1,0:T(8,128)S(1)} collective-permute-done((f32[64,1024]{1,0:T(8,128)S(1)}, f32[64,1024]{1,0:T(8,128)S(1)}, u32[]{:S(2)}, u32[]{:S(2)}) %collective-permute-start.7) | collective-permute-done | bytes 262176 | tf_op jit(solution)/shard_map/ppermute | solution.py:22
  109.0 0.7 add_convert_fusion
  (31 shorter events, 0.1 us)
Async XLA Ops:
  0.6 34.3 %copy-start = (bf16[512,1024]{1,0:T(8,128)(2,1)S(1)}, bf16[512,1024]{1,0:T(8,128)(2,1)}, u32[]{:S(2)}) copy-start(bf16[512,1024]{1,0:T(8,128)(2,1)} %param.40) | copy-start | bytes 3145732
  0.6 7.1 %copy-start.16 = (bf16[8,128,128]{2,1,0:T(8,128)(2,1)S(1)}, bf16[8,128,128]{2,1,0:T(8,128)(2,1)}, u32[]{:S(2)}) copy-start(bf16[8,128,128]{2,1,0:T(8,128)(2,1)} %param.29) | copy-start | bytes 786436
  0.7 7.3 %copy-start.17 = (bf16[8,128,128]{2,1,0:T(8,128)(2,1)S(1)}, bf16[8,128,128]{2,1,0:T(8,128)(2,1)}, u32[]{:S(2)}) copy-start(bf16[8,128,128]{2,1,0:T(8,128)(2,1)} %param.28) | copy-start | bytes 786436
  0.7 7.6 %copy-start.11 = (f32[64,1024]{1,0:T(8,128)S(1)}, f32[64,1024]{1,0:T(8,128)}, u32[]{:S(2)}) copy-start(f32[64,1024]{1,0:T(8,128)} %param.23) | copy-start | bytes 786436
  0.7 1.7 %collective-permute-start = (bf16[64,1024]{1,0:T(8,128)(2,1)}, bf16[64,1024]{1,0:T(8,128)(2,1)S(1)}, u32[]{:S(2)}, u32[]{:S(2)}) collective-permute-start(bf16[64,1024]{1,0:T(8,128)(2,1)} %param.21), channel_id=1, source_target_pairs={{0,1},{1,0},{2,3},{3,2},{4,5},{5,4},{6,7},{7,6},{8,9},{9,8},{10,11... | collective-permute-start | bytes 393224 | tf_op jit(solution)/shard_map/ppermute | solution.py:22
  3.6 4.9 %copy-start.10 = (bf16[64,1024]{1,0:T(8,128)(2,1)S(1)}, bf16[64,1024]{1,0:T(8,128)(2,1)}, u32[]{:S(2)}) copy-start(bf16[64,1024]{1,0:T(8,128)(2,1)} %param.21) | copy-start | bytes 393220
  3.6 4.9 %copy-start.15 = (bf16[2048,1024]{1,0:T(8,128)(2,1)S(1)}, bf16[2048,1024]{1,0:T(8,128)(2,1)}, u32[]{:S(2)}) copy-start(bf16[2048,1024]{1,0:T(8,128)(2,1)} %param.26) | copy-start | bytes 12582916
  3.6 4.9 %copy-start.18 = (f32[2048]{0:T(1024)S(1)}, f32[2048]{0:T(1024)}, u32[]{:S(2)}) copy-start(f32[2048]{0:T(1024)} %param.24) | copy-start | bytes 24580
  7.7 3.4 %copy-start.8 = (bf16[2048,1024]{1,0:T(8,128)(2,1)S(1)}, bf16[2048,1024]{1,0:T(8,128)(2,1)}, u32[]{:S(2)}) copy-start(bf16[2048,1024]{1,0:T(8,128)(2,1)} %param.31) | copy-start | bytes 12582916
  8.5 3.5 %copy-start.12 = (f32[64,1024]{1,0:T(8,128)}, f32[64,1024]{1,0:T(8,128)S(1)}, u32[]{:S(2)}) copy-start(f32[64,1024]{1,0:T(8,128)S(1)} %fusion.29) | copy-start | bytes 786436
  8.5 4.9 %copy-start.5 = (s32[64,6]{0,1:T(8,128)S(1)}, s32[64,6]{0,1:T(8,128)}, u32[]{:S(2)}) copy-start(s32[64,6]{0,1:T(8,128)} %param.33) | copy-start | bytes 4612
  8.5 4.9 %copy-start.6 = (f32[2048]{0:T(1024)S(1)}, f32[2048]{0:T(1024)}, u32[]{:S(2)}) copy-start(f32[2048]{0:T(1024)} %param.32) | copy-start | bytes 24580
  9.5 17.5 %copy-start.7 = (f32[64,6]{0,1:T(8,128)S(1)}, f32[64,6]{0,1:T(8,128)}, u32[]{:S(2)}) copy-start(f32[64,6]{0,1:T(8,128)} %param.34) | copy-start | bytes 4612
  9.6 1.6 %collective-permute-start.1 = (bf16[64,1024]{1,0:T(8,128)(2,1)S(1)}, bf16[64,1024]{1,0:T(8,128)(2,1)S(1)}, u32[]{:S(2)}, u32[]{:S(2)}) collective-permute-start(bf16[64,1024]{1,0:T(8,128)(2,1)S(1)} %fusion.27), channel_id=1, source_target_pairs={{0,1},{1,0},{2,3},{3,2},{4,5},{5,4},{6,7},{7,6},{8,9},{9,8},{10,11... | collective-permute-start | bytes 393224 | tf_op jit(solution)/shard_map/ppermute | solution.py:22
  12.0 1.4 %collective-permute-start.2 = (bf16[64,1024]{1,0:T(8,128)(2,1)S(1)}, bf16[64,1024]{1,0:T(8,128)(2,1)S(1)}, u32[]{:S(2)}, u32[]{:S(2)}) collective-permute-start(bf16[64,1024]{1,0:T(8,128)(2,1)S(1)} %fusion.13.own_ref), channel_id=1, source_target_pairs={{0,1},{1,0},{2,3},{3,2},{4,5},{5,4},{6,7},{7,6},{8,9},{9,8},{10,11... | collective-permute-start | bytes 393224 | tf_op jit(solution)/shard_map/ppermute | solution.py:22
  15.5 19.4 %copy-start.14 = (f32[1024]{0:T(1024)S(1)}, f32[1024]{0:T(1024)}, u32[]{:S(2)}) copy-start(f32[1024]{0:T(1024)} %param.41) | copy-start | bytes 12292
  15.5 45.2 %all-to-all-start = ((bf16[64,8,2304]{2,1,0:T(8,128)(2,1)}), bf16[64,8,2304]{2,1,0:T(8,128)(2,1)S(1)}, u32[]{:S(2)}, u32[]{:S(2)}) async-start(bf16[64,8,2304]{2,1,0:T(8,128)(2,1)} %bitcast.68), calls=%async_computation | async-start | bytes 4718592 | tf_op jit(solution)/shard_map/all_to_all | solution.py:343
  27.0 6.9 %slice-start = ((bf16[64,3,1024]{2,0,1:T(8,128)(2,1)}), bf16[64,2,1024]{2,0,1:T(8,128)(2,1)S(1)}, s32[]{:S(2)}) async-start(bf16[64,3,1024]{2,0,1:T(8,128)(2,1)} %param.22), calls=%async_computation.2 | async-start | bytes 524288 | tf_op jit(solution)/shard_map/slice | solution.py:302
  27.0 6.9 %copy-start.13 = (bf16[64,1024]{1,0:T(8,128)(2,1)S(1)}, bf16[64,1024]{1,0:T(8,128)(2,1)}, u32[]{:S(2)}) copy-start(bf16[64,1024]{1,0:T(8,128)(2,1)} %get-tuple-element.46) | copy-start | bytes 393220
  27.6 0.7 copy-start.1
  28.2 0.6 copy-start.3
  28.8 31.9 %collective-permute-start.4 = (bf16[2048,256]{1,0:T(8,128)(2,1)}, bf16[2048,256]{1,0:T(8,128)(2,1)}, u32[]{:S(2)}, u32[]{:S(2)}) collective-permute-start(bf16[2048,256]{1,0:T(8,128)(2,1)} %bitcast.69), channel_id=1, source_target_pairs={{0,1},{1,0},{2,3},{3,2},{4,5},{5,4},{6,7},{7,6},{8,9},{9,8},{10,11... | collective-permute-start | bytes 3145736 | tf_op jit(solution)/shard_map/ppermute | solution.py:22
  28.9 31.8 %collective-permute-start.5 = (bf16[2048,256]{1,0:T(8,128)(2,1)}, bf16[2048,256]{1,0:T(8,128)(2,1)}, u32[]{:S(2)}, u32[]{:S(2)}) collective-permute-start(bf16[2048,256]{1,0:T(8,128)(2,1)} %bitcast.71), channel_id=1, source_target_pairs={{0,1},{1,0},{2,3},{3,2},{4,5},{5,4},{6,7},{7,6},{8,9},{9,8},{10,11... | collective-permute-start | bytes 3145736 | tf_op jit(solution)/shard_map/ppermute | solution.py:22
  29.3 31.4 %collective-permute-start.6 = (bf16[512,1024]{1,0:T(8,128)(2,1)}, bf16[512,1024]{1,0:T(8,128)(2,1)}, u32[]{:S(2)}, u32[]{:S(2)}) collective-permute-start(bf16[512,1024]{1,0:T(8,128)(2,1)} %bitcast.73), channel_id=1, source_target_pairs={{0,1},{1,0},{2,3},{3,2},{4,5},{5,4},{6,7},{7,6},{8,9},{9,8},{10,11... | collective-permute-start | bytes 3145736 | tf_op jit(solution)/shard_map/ppermute | solution.py:22
  33.6 1.3 %collective-permute-start.3 = (bf16[64,256]{1,0:T(8,128)(2,1)S(1)}, bf16[64,256]{1,0:T(8,128)(2,1)S(1)}, u32[]{:S(2)}, u32[]{:S(2)}) collective-permute-start(bf16[64,256]{1,0:T(8,128)(2,1)S(1)} %multiply_convert_fusion), channel_id=1, source_target_pairs={{0,1},{1,0},{2,3},{3,2},{4,5},{5,4},{6,7},{7,6},{8,9},{9,8},{10,11... | collective-permute-start | bytes 98312 | tf_op jit(solution)/shard_map/ppermute | solution.py:22
  68.1 38.7 %copy-start.2 = (bf16[128,512]{1,0:T(8,128)(2,1)S(1)}, bf16[128,512]{1,0:T(8,128)(2,1)}, u32[]{:S(2)}) copy-start(bf16[128,512]{1,0:T(8,128)(2,1)} %copy-done.1) | copy-start | bytes 393220
  68.1 38.7 %copy-start.4 = (bf16[128,64]{1,0:T(8,128)(2,1)S(1)}, bf16[128,64]{1,0:T(8,128)(2,1)}, u32[]{:S(2)}) copy-start(bf16[128,64]{1,0:T(8,128)(2,1)} %copy-done.3) | copy-start | bytes 49156
  68.1 40.9 %copy-start.9 = (f32[64,1024]{1,0:T(8,128)S(1)}, f32[64,1024]{1,0:T(8,128)}, u32[]{:S(2)}) copy-start(f32[64,1024]{1,0:T(8,128)} %fusion.10) | copy-start | bytes 786436
  107.3 1.6 %collective-permute-start.7 = (f32[64,1024]{1,0:T(8,128)S(1)}, f32[64,1024]{1,0:T(8,128)S(1)}, u32[]{:S(2)}, u32[]{:S(2)}) collective-permute-start(f32[64,1024]{1,0:T(8,128)S(1)} %get-tuple-element.32), channel_id=1, source_target_pairs={{0,1},{1,0},{2,3},{3,2},{4,5},{5,4},{6,7},{7,6},{8,9},{9,8},{10,11... | collective-permute-start | bytes 786440 | tf_op jit(solution)/shard_map/ppermute | solution.py:22

commit v3 on v2

v3 whole, which is shorter than its diff:
```python
import functools

import jax
import jax.numpy as jnp
from jax import lax
from jax.experimental import pallas as pl
from jax.experimental.pallas import tpu as pltpu
from jax.sharding import PartitionSpec as P


BF = jnp.bfloat16
F32 = jnp.float32
SWAP = [(0, 1), (1, 0)]
MIB = 1024 * 1024
LANES = 128
SLOTS = 9
MAIN = 8


def swapped(x):
    return lax.ppermute(x, "tp", SWAP)


def in_order(core, own, other):
    return jnp.where(
        core == 0,
        jnp.concatenate([own, other], axis=1),
        jnp.concatenate([other, own], axis=1),
    )


def places(ids, core):
    experts = rows = ids.shape[1]
    expert = lax.broadcasted_iota(jnp.int32, (experts, rows), 0)
    hits = [ids[k : k + 1, :] == expert for k in range(ids.shape[0])]
    chosen = functools.reduce(jnp.logical_or, hits)
    earlier = lax.broadcasted_iota(jnp.int32, (rows, rows), 0) < lax.broadcasted_iota(
        jnp.int32, (rows, rows), 1
    )
    rank = jnp.dot(
        jnp.where(chosen, 1.0, 0.0).astype(BF),
        jnp.where(earlier, 1.0, 0.0).astype(BF),
        preferred_element_type=F32,
    )
    return hits, jnp.where(chosen, rank - (SLOTS * core).astype(F32), -1.0)


def each_slot(values):
    experts = values.shape[0]
    shape = (experts * MAIN, experts)
    row = lax.broadcasted_iota(jnp.int32, shape, 0) // MAIN
    spread = jnp.where(row == lax.broadcasted_iota(jnp.int32, shape, 1), 1.0, 0.0).astype(BF)
    return jnp.dot(spread, values.astype(BF), preferred_element_type=F32)


def slot_number(shape):
    return (lax.broadcasted_iota(jnp.int32, shape, 0) % MAIN).astype(F32)


def put_pieces(piece_ref, values, start, base):
    count = values.shape[0]
    for n in range(values.shape[1] // LANES):
        c, part = divmod(start + n, 2)
        piece_ref[part, pl.ds(base + c, count, stride=MAIN), :] = values[
            :, n * LANES : (n + 1) * LANES
        ]


def take_pieces(piece_ref, block_ref, features, rows_ref, start):
    count = block_ref.shape[0] // MAIN
    piece_ref[0] = block_ref[:, features : features + LANES].astype(F32)
    piece_ref[1] = block_ref[:, features + LANES :].astype(F32)
    for n in range(features // LANES):
        c, part = divmod(n, 2)
        rows_ref[start : start + count, n * LANES : (n + 1) * LANES] = piece_ref[
            part, pl.ds(c, count, stride=MAIN), :
        ].astype(BF)


def pack_body(
    core_ref,
    own_ref,
    other_ref,
    gain_ref,
    ids_ref,
    out_ref,
    norm_out_ref,
    norm_ref,
    piece_ref,
    sem,
):
    core = core_ref[0]
    half = own_ref.shape[1]
    features = 2 * half
    own = own_ref[...].astype(F32)
    other = other_ref[...].astype(F32)
    mean = (jnp.sum(own, 1, keepdims=True) + jnp.sum(other, 1, keepdims=True)) / features
    square = (
        jnp.sum(own * own, 1, keepdims=True) + jnp.sum(other * other, 1, keepdims=True)
    ) / features
    scale = lax.rsqrt(square - mean * mean + 1e-05)
    low, high = gain_ref[:, :half], gain_ref[:, half:]
    gain_own = jnp.where(core == 0, low, high)
    gain_other = jnp.where(core == 0, high, low)
    norm_ref[:, :half] = ((own - mean) * scale * gain_own).astype(BF)
    norm_ref[:, half:] = ((other - mean) * scale * gain_other).astype(BF)
    norm_copy = pltpu.make_async_copy(norm_ref, norm_out_ref, sem)
    norm_copy.start()
    rows = norm_ref[...]
    _, place = places(ids_ref[...], core)
    wide = each_slot(place)
    table = jnp.where(wide == slot_number(wide.shape), 1.0, 0.0).astype(BF)
    last = jnp.where(place == float(MAIN), 1.0, 0.0).astype(BF)
    out_ref[:, :features] = jnp.dot(table, rows, preferred_element_type=F32).astype(BF)
    put_pieces(piece_ref, jnp.dot(last, rows, preferred_element_type=F32), 0, 0)
    out_ref[:, features : features + LANES] = piece_ref[0].astype(BF)
    out_ref[:, features + LANES :] = piece_ref[1].astype(BF)
    norm_copy.wait()


def start_all(pairs, sems):
    copies = [
        pltpu.make_async_copy(source, target, sems.at[n])
        for n, (source, target) in enumerate(pairs)
    ]
    for copy in copies:
        copy.start()
    return copies


def wait_all(copies):
    for copy in copies:
        copy.wait()


def warm_body(
    weight_hbm,
    state_hbm,
    taps_hbm,
    logit_hbm,
    weight_ref,
    conv_ref,
    decay_ref,
    state_ref,
    taps_ref,
    logit_ref,
    sems,
):
    copies = start_all(
        (
            (state_hbm, state_ref),
            (taps_hbm, taps_ref),
            (logit_hbm, logit_ref),
            (weight_hbm, weight_ref),
        ),
        sems,
    )
    wait_all(copies[:3])
    conv = state_ref[0].astype(F32) * taps_ref[0:1, :]
    for offset in range(1, 3):
        conv = conv + state_ref[offset].astype(F32) * taps_ref[offset : offset + 1, :]
    conv_ref[...] = conv
    decay_ref[...] = -8.0 * jax.nn.softplus(-logit_ref[...])
    wait_all(copies[3:])


def near_body(core_ref, mixed_ref, weight_ref, weight_hbm, part_ref, other_ref, sem):
    half = mixed_ref.shape[1]
    second = pl.ds(pl.multiple_of((1 - core_ref[0]) * half, half), half)
    copy = pltpu.make_async_copy(weight_hbm.at[second, :], other_ref, sem)
    copy.start()
    part_ref[...] = jnp.dot(mixed_ref[...], weight_ref[...], preferred_element_type=F32)
    copy.wait()


def resid_body(part_ref, mixed_ref, weight_ref, stream_ref, out_ref):
    mixer_out = part_ref[...] + jnp.dot(
        mixed_ref[...], weight_ref[...], preferred_element_type=F32
    )
    out_ref[...] = (stream_ref[...].astype(F32) + mixer_out.astype(BF).astype(F32)).astype(BF)


def mixer_body(
    core_ref,
    own_ref,
    other_ref,
    gain_ref,
    branch_ref,
    conv_ref,
    taps_ref,
    decay_ref,
    recur_ref,
    input_ref,
    state_ref,
    gate_hbm,
    out_hbm,
    branch_out_hbm,
    state_out_hbm,
    mixed_ref,
    weight_ref,
    gate_ref,
    branch_out_ref,
    state_out_ref,
    sems,
):
    core = core_ref[0]
    half = own_ref.shape[1]
    features = 2 * half
    first = pl.ds(pl.multiple_of(core * half, half), half)
    second = pl.ds(pl.multiple_of((1 - core) * half, half), half)
    copies = start_all(((gate_hbm, gate_ref), (out_hbm.at[first, :], weight_ref)), sems)
    own = own_ref[...].astype(F32)
    other = other_ref[...].astype(F32)
    mean = (jnp.sum(own, 1, keepdims=True) + jnp.sum(other, 1, keepdims=True)) / features
    square = (
        jnp.sum(own * own, 1, keepdims=True) + jnp.sum(other * other, 1, keepdims=True)
    ) / features
    scale = lax.rsqrt(square - mean * mean + 1e-05)
    low, high = gain_ref[:, :half], gain_ref[:, half:]
    own = ((own - mean) * scale * jnp.where(core == 0, low, high)).astype(BF)
    other = ((other - mean) * scale * jnp.where(core == 0, high, low)).astype(BF)

    def product(weight):
        return (
            jnp.dot(own, weight[first, :], preferred_element_type=F32)
            + jnp.dot(other, weight[second, :], preferred_element_type=F32)
        ).astype(BF)

    branch = product(branch_ref)
    branch_out_ref[...] = branch
    conv = (conv_ref[...] + branch.astype(F32) * taps_ref[3:4, :]).astype(BF)
    width = recur_ref.shape[1]
    recur, drive = (
        jnp.concatenate(
            [
                jnp.dot(
                    conv[:, n * width : (n + 1) * width], maps[n], preferred_element_type=F32
                )
                for n in range(maps.shape[0])
            ],
            axis=1,
        )
        for maps in (recur_ref, input_ref)
    )
    log_decay = jax.nn.sigmoid(recur) * decay_ref[...]
    turn = jnp.tanh(log_decay)
    kept = jnp.sqrt(-2.0 * turn / (1.0 - turn))
    driven = kept * (jax.nn.sigmoid(drive) * conv.astype(F32))
    state = jnp.exp(log_decay) * state_ref[...] + driven
    state_out_ref[...] = state
    branch_copy = pltpu.make_async_copy(branch_out_ref, branch_out_hbm, sems.at[2])
    branch_copy.start()
    state_copy = pltpu.make_async_copy(state_out_ref, state_out_hbm, sems.at[3])
    state_copy.start()
    wait_all(copies[:1])
    mixed_ref[...] = (jax.nn.gelu(product(gate_ref).astype(F32)) * state).astype(BF)
    wait_all([*copies[1:], branch_copy, state_copy])


def table_body(core_ref, ids_ref, weights_ref, table_ref, last_ref):
    rows = ids_ref.shape[1]
    hits, place = places(ids_ref[...], core_ref[0])
    weight = functools.reduce(
        jnp.add,
        [jnp.where(hit, weights_ref[k : k + 1, :], 0.0) for k, hit in enumerate(hits)],
    )
    high = weight.astype(BF).astype(F32)
    low = (weight - high).astype(BF).astype(F32)
    wide = each_slot(place)
    match = wide == slot_number(wide.shape)
    for n, part in enumerate((high, low)):
        span = slice(n * rows, (n + 1) * rows)
        table_ref[span, :] = jnp.transpose(jnp.where(match, each_slot(part), 0.0)).astype(BF)
        last_ref[span, :] = jnp.transpose(jnp.where(place == float(MAIN), part, 0.0)).astype(BF)


def expert_body(
    core_ref,
    in_ref,
    gate_ref,
    gate2_ref,
    up_ref,
    up2_ref,
    down_ref,
    down2_ref,
    out_ref,
    block_ref,
    piece_ref,
    take_ref,
    rows_ref,
    out_sems,
):
    core = core_ref[0]
    features, units = gate_ref.shape
    half = features // 2
    first = pl.ds(pl.multiple_of(core * half, half), half)
    second = pl.ds(pl.multiple_of((1 - core) * half, half), half)
    unit_own = pl.ds(pl.multiple_of(core * units, units), units)
    unit_other = pl.ds(pl.multiple_of((1 - core) * units, units), units)
    count = in_ref.shape[0]
    extra = count // MAIN
    take_pieces(take_ref, in_ref, features, rows_ref, 0)
    rows_ref[extra:, :] = in_ref[:, :features]

    def product(weight):
        return jnp.dot(
            rows_ref[:, :half], weight[first, :], preferred_element_type=F32
        ) + jnp.dot(rows_ref[:, half:], weight[second, :], preferred_element_type=F32)

    def hidden(gate, up):
        return (jax.nn.silu(product(gate)) * product(up)).astype(BF)

    hid_own = hidden(gate_ref, up_ref)
    hid_other = hidden(gate2_ref, up2_ref)
    copies = []
    for part, down in enumerate((down_ref, down2_ref)):
        served = jnp.dot(hid_own, down[unit_own, :], preferred_element_type=F32) + jnp.dot(
            hid_other, down[unit_other, :], preferred_element_type=F32
        )
        put_pieces(piece_ref, served[:extra], part * (half // LANES), 0)
        cols = slice(part * half, (part + 1) * half)
        block_ref[:, cols] = served[extra:].astype(BF)
        if part:
            cols = slice(half, block_ref.shape[1])
            block_ref[:, features : features + LANES] = piece_ref[0].astype(BF)
            block_ref[:, features + LANES :] = piece_ref[1].astype(BF)
        copy = pltpu.make_async_copy(block_ref.at[:, cols], out_ref.at[:, cols], out_sems.at[part])
        copy.start()
        copies.append(copy)
    for copy in copies:
        copy.wait()


def combine_body(
    in_ref,
    table_hbm,
    lasts_hbm,
    base_hbm,
    own_ref,
    other_ref,
    piece_ref,
    last_ref,
    table_ref,
    lasts_ref,
    base_ref,
    sems,
):
    loads = []
    for n, (source, target) in enumerate(
        ((table_hbm, table_ref), (lasts_hbm, lasts_ref), (base_hbm, base_ref))
    ):
        copy = pltpu.make_async_copy(source, target, sems.at[n])
        copy.start()
        loads.append(copy)
    rows, half = own_ref.shape
    features = 2 * half
    take_pieces(piece_ref, in_ref, features, last_ref, 0)
    for copy in loads:
        copy.wait()
    total = jnp.dot(
        table_ref[...], in_ref[:, :features], preferred_element_type=F32
    ) + jnp.dot(lasts_ref[...], last_ref[...], preferred_element_type=F32)
    total = total[:rows] + total[rows:]
    own_ref[...] = total[:, :half] + base_ref[...]
    other_ref[...] = total[:, half:]


def vmem(count):
    return [pl.BlockSpec(memory_space=pltpu.VMEM)] * count


def hbm(count):
    return [pl.BlockSpec(memory_space=pltpu.HBM)] * count


def in_hbm(x):
    return pltpu.with_memory_space_constraint(x, pltpu.HBM)


def smem():
    return [pl.BlockSpec(memory_space=pltpu.SMEM)]


def per_device(
    stream,
    conv_state,
    recur_state,
    mix_gain,
    branch_weight,
    gate_weight,
    conv_taps,
    recur_map,
    input_map,
    decay_logit,
    out_weight,
    moe_gain,
    route_ids,
    route_weights,
    expert_gate,
    expert_up,
    expert_down,
    dense_gate,
    dense_up,
    dense_down,
    dense_scale,
):
    core = lax.axis_index("tp")
    core_arr = core.astype(jnp.int32).reshape(1)
    seq_count, half = stream.shape
    features = 2 * half
    experts = lax.axis_size("ep")
    own_gate, own_up, own_down = expert_gate[0], expert_up[0], expert_down[0]
    stream_other = swapped(stream)
    branch_near, conv_part, decay = pl.pallas_call(
        warm_body,
        name="warm",
        out_shape=(
            jax.ShapeDtypeStruct((features, half), BF),
            jax.ShapeDtypeStruct((seq_count, half), F32),
            jax.ShapeDtypeStruct((1, half), F32),
        ),
        in_specs=hbm(4),
        out_specs=tuple(vmem(3)),
        scratch_shapes=[
            pltpu.VMEM((3, seq_count, half), BF),
            pltpu.VMEM((4, half), F32),
            pltpu.VMEM((1, half), F32),
            pltpu.SemaphoreType.DMA((4,)),
        ],
        compiler_params=pltpu.CompilerParams(vmem_limit_bytes=8 * MIB),
    )(
        *(
            in_hbm(x)
            for x in (
                branch_weight,
                conv_state.transpose(1, 0, 2),
                conv_taps,
                decay_logit.reshape(1, half),
            )
        )
    )
    branch_in, new_state, mixer_in, out_own = pl.pallas_call(
        mixer_body,
        name="mixer",
        out_shape=(
            pltpu.HBM((seq_count, half), BF),
            pltpu.HBM((seq_count, half), F32),
            jax.ShapeDtypeStruct((seq_count, half), BF),
            jax.ShapeDtypeStruct((half, half), BF),
        ),
        in_specs=smem() + vmem(10) + hbm(2),
        out_specs=tuple(hbm(2) + vmem(2)),
        scratch_shapes=[
            pltpu.VMEM((features, half), BF),
            pltpu.VMEM((seq_count, half), BF),
            pltpu.VMEM((seq_count, half), F32),
            pltpu.SemaphoreType.DMA((4,)),
        ],
        compiler_params=pltpu.CompilerParams(vmem_limit_bytes=14 * MIB),
        cost_estimate=pl.CostEstimate(
            flops=4 * seq_count * features * half,
            transcendentals=6 * seq_count * half,
            bytes_accessed=4 * features * half,
        ),
    )(
        core_arr,
        stream,
        stream_other,
        mix_gain.reshape(1, features),
        branch_near,
        conv_part,
        conv_taps,
        decay,
        recur_map,
        input_map,
        recur_state,
        in_hbm(gate_weight),
        in_hbm(out_weight),
    )
    own_gate, own_up, own_down, mixer_in = lax.optimization_barrier(
        (own_gate, own_up, own_down, mixer_in)
    )
    mixer_other = swapped(mixer_in)
    other_gate, other_up, other_down = swapped(own_gate), swapped(own_up), swapped(own_down)
    part, out_other = pl.pallas_call(
        near_body,
        name="near",
        out_shape=(
            jax.ShapeDtypeStruct((seq_count, half), F32),
            jax.ShapeDtypeStruct((half, half), BF),
        ),
        in_specs=smem() + vmem(2) + hbm(1),
        out_specs=tuple(vmem(2)),
        scratch_shapes=[pltpu.SemaphoreType.DMA],
        compiler_params=pltpu.CompilerParams(vmem_limit_bytes=8 * MIB),
    )(core_arr, mixer_in, out_own, in_hbm(out_weight))
    resid = pl.pallas_call(
        resid_body,
        name="resid",
        out_shape=jax.ShapeDtypeStruct((seq_count, half), BF),
        in_specs=vmem(4),
        out_specs=vmem(1)[0],
        compiler_params=pltpu.CompilerParams(vmem_limit_bytes=8 * MIB),
    )(part, mixer_other, out_other, stream)
    resid_other = swapped(resid)

    block = features + features // MAIN
    count = experts * MAIN
    pieces = pltpu.VMEM((2, count, LANES), F32)
    ids_t, weights_t = route_ids.T, route_weights.T
    payload, normed_two = pl.pallas_call(
        pack_body,
        name="pack",
        out_shape=(
            jax.ShapeDtypeStruct((count, block), BF),
            pltpu.HBM((seq_count, features), BF),
        ),
        in_specs=smem() + vmem(4),
        out_specs=(vmem(1)[0], hbm(1)[0]),
        scratch_shapes=[
            pltpu.VMEM((seq_count, features), BF),
            pieces,
            pltpu.SemaphoreType.DMA,
        ],
        compiler_params=pltpu.CompilerParams(vmem_limit_bytes=14 * MIB),
    )(core_arr, resid, resid_other, moe_gain.reshape(1, features), ids_t)

    incoming = lax.all_to_all(
        payload.reshape(experts, MAIN, block), "ep", split_axis=0, concat_axis=0, tiled=True
    )
    incoming, normed_two, ids_late, weights_late, branch_in, conv_late = lax.optimization_barrier(
        (incoming, normed_two, ids_t, weights_t, branch_in, conv_state)
    )
    new_conv = jnp.concatenate([conv_late[:, 1:], branch_in[:, None]], axis=1)
    incoming = incoming.reshape(count, block)
    table, last = pl.pallas_call(
        table_body,
        name="table",
        out_shape=(
            jax.ShapeDtypeStruct((2 * seq_count, count), BF),
            jax.ShapeDtypeStruct((2 * seq_count, experts), BF),
        ),
        in_specs=smem() + vmem(2),
        out_specs=tuple(vmem(2)),
        compiler_params=pltpu.CompilerParams(vmem_limit_bytes=8 * MIB),
    )(core_arr, ids_late, weights_late)

    own_two, other_two = normed_two[:, :half], normed_two[:, half:]
    whole_two = in_order(core, own_two, other_two)
    dense_hidden = (
        jax.nn.silu(jnp.dot(whole_two, dense_gate, preferred_element_type=F32))
        * jnp.dot(whole_two, dense_up, preferred_element_type=F32)
    ).astype(BF)
    dense_whole = in_order(core, dense_hidden, swapped(dense_hidden))
    dense_out = jnp.dot(dense_whole, dense_down, preferred_element_type=F32).astype(BF)
    base = resid.astype(F32) + dense_scale * dense_out.astype(F32)

    served = pl.pallas_call(
        expert_body,
        name="experts",
        out_shape=pltpu.HBM((count, block), BF),
        in_specs=smem() + vmem(7),
        out_specs=hbm(1)[0],
        scratch_shapes=[
            pltpu.VMEM((count, block), BF),
            pieces,
            pieces,
            pltpu.VMEM((experts * SLOTS, features), BF),
            pltpu.SemaphoreType.DMA((2,)),
        ],
        compiler_params=pltpu.CompilerParams(vmem_limit_bytes=24 * MIB),
    )(
        core_arr,
        incoming,
        own_gate,
        other_gate,
        own_up,
        other_up,
        own_down,
        other_down,
    )

    returned = lax.all_to_all(
        served.reshape(experts, MAIN, block), "ep", split_axis=0, concat_axis=0, tiled=True
    )
    returned, base, new_conv, new_state, table, last = lax.optimization_barrier(
        (returned, base, new_conv, new_state, table, last)
    )
    returned = returned.reshape(count, block)
    sum_own, sum_other = pl.pallas_call(
        combine_body,
        name="combine",
        out_shape=(
            jax.ShapeDtypeStruct((seq_count, half), F32),
            jax.ShapeDtypeStruct((seq_count, half), F32),
        ),
        in_specs=vmem(1) + hbm(3),
        out_specs=tuple(vmem(2)),
        scratch_shapes=[
            pieces,
            pltpu.VMEM((experts, features), BF),
            pltpu.VMEM((2 * seq_count, count), BF),
            pltpu.VMEM((2 * seq_count, experts), BF),
            pltpu.VMEM((seq_count, half), F32),
            pltpu.SemaphoreType.DMA((3,)),
        ],
        compiler_params=pltpu.CompilerParams(vmem_limit_bytes=14 * MIB),
    )(returned, *(in_hbm(x) for x in (table, last, base)))
    result = (sum_own + swapped(sum_other)).astype(BF)
    return (result, new_state, new_conv)


def solution(mesh):
    in_specs = (
        P("ep", "tp"),
        P("ep", None, "tp"),
        P("ep", "tp"),
        P(),
        P(None, "tp"),
        P(None, "tp"),
        P(None, "tp"),
        P("tp", None, None),
        P("tp", None, None),
        P("tp"),
        P(None, "tp"),
        P(),
        P("ep", None),
        P("ep", None),
        P("ep", None, "tp"),
        P("ep", None, "tp"),
        P("ep", None, "tp"),
        P(None, "tp"),
        P(None, "tp"),
        P(None, "tp"),
        P("tp"),
    )
    out_specs = (P("ep", "tp"), P("ep", "tp"), P("ep", None, "tp"))
    return jax.shard_map(
        per_device, mesh=mesh, in_specs=in_specs, out_specs=out_specs, check_vma=False
    )
```

time: 111 us -> 113 us (1.018)
  blocking collectives: 38.6 us -> 0 us
  waiting for transfers between devices: 28.4 us -> 60 us
  Pallas kernels: 10.5 us -> 18 us
  matrix products: 10.7 us -> 4.24 us
  starting transfers between devices: 13.6 us -> 18.9 us
  local copies, waits for them, and re-layouts: 3.23 us -> 7.46 us
  other arithmetic: 3.62 us -> 1.47 us
    all_to_all x1 -> x0, blocking collectives: 38.6 us -> none  [per_device(): lax.all_to_all(served.reshape(experts, MAIN, block), 'ep', split_axis=0,...]
    all_to_all x0 -> x1, waiting for transfers between devices: none -> 24.6 us  [per_device(): lax.all_to_all(served.reshape(experts, MAIN, block), 'ep', split_axis=0,...]
    all_to_all x1, waiting for transfers between devices: 24.8 us -> 32.6 us  [per_device(): lax.all_to_all(payload.reshape(experts, MAIN, block), 'ep', split_axis=0,...]
    pallas_call x1 -> x5, Pallas kernels: 2.03 us -> 8.98 us  [the longest x1 3.27 us: per_device(): pl.pallas_call(mixer_body, name='mixer', out_shape=(pltpu.HBM((seq_count,...]
    dot_general x5 -> x0, matrix products: 6.45 us -> none  [the longest x1 4.12 us: per_device(): jnp.dot(normed, branch_weight, preferred_element_type=F32).astype(BF)]
    all_to_all x0 -> x1, starting transfers between devices: none -> 5.81 us  [per_device(): lax.all_to_all(served.reshape(experts, MAIN, block), 'ep', split_axis=0,...]
    unnamed x38, local copies, waits for them, and re-layouts: 1.34 us -> 6.39 us
    reduce_sum x1 -> x0, other arithmetic: 1.19 us -> none  [per_device(): mean = jnp.mean(whole, axis=1, keepdims=True)]
  transfers between devices with their start and end apart: 9 -> 10, of which waited for: 5 -> 4; matrix products, arithmetic and copies ran while one was open for 7% -> 5% of each run, Pallas kernels for 0% -> 4%
where the time goes in v3:
time: 113 us; the launch traced here: 111 us
  waiting for transfers between devices  60 us (53%)
  starting transfers between devices  18.9 us (17%)
  Pallas kernels  18 us (16%)
  local copies, waits for them, and re-layouts  7.46 us (7%)
  matrix products  4.24 us (4%)
  other arithmetic  1.47 us (1%)
    all_to_all x1, waiting for transfers between devices, per_device(): lax.all_to_all(payload.reshape(experts, MAIN, block), 'ep', split_axis=0,...  32.6 us
    all_to_all x1, waiting for transfers between devices, per_device(): lax.all_to_all(served.reshape(experts, MAIN, block), 'ep', split_axis=0,...  24.6 us
    all_to_all x1, starting transfers between devices, per_device(): lax.all_to_all(payload.reshape(experts, MAIN, block), 'ep', split_axis=0,...  11.5 us
    pallas_call x1, Pallas kernels, per_device(): pl.pallas_call(expert_body, name='experts', out_shape=pltpu.HBM((count, b...  6.9 us
    unnamed x38, local copies, waits for them, and re-layouts  6.39 us
    all_to_all x1, starting transfers between devices, per_device(): lax.all_to_all(served.reshape(experts, MAIN, block), 'ep', split_axis=0,...  5.81 us
    pallas_call x1, Pallas kernels, per_device(): pl.pallas_call(mixer_body, name='mixer', out_shape=(pltpu.HBM((seq_count,...  3.27 us
    ppermute x8, waiting for transfers between devices, swapped(): return lax.ppermute(x, 'tp', SWAP)  2.76 us
  transfers between devices with their start and end apart: 10, of which 4 were waited for; matrix products, arithmetic and copies ran while one was open for 5% of the time, Pallas kernels for 4%

profile of v3, /device:TPU:0, one launch (start us, length us, event | category | flops | bytes accessed | tf_op | source)
XLA Modules:
  0.0 111.1 jit_solution(17305553945806539793)
XLA Ops:
  0.6 0.0 copy-start
  0.7 0.1 collective-permute-start
  0.8 2.5 %warm.1 = (bf16[2048,1024]{1,0:T(8,128)(2,1)S(1)}, f32[64,1024]{1,0:T(8,128)S(1)}, f32[1,1024]{1,0:T(1,128)S(1)}) custom-call(bf16[2048,1024]{1,0:T(8,128)(2,1)} %weight_hbm.2, bf16[3,64,1024]{2,1,0:T(8,128)(2,1)} %bitcast.33, f32[4,1024]{1,0:T(4,128)} %taps_ref.1, f32[1,1024]{1,0:T(1,128)} %bitcast.35), custom_call_target="tpu_custom_call" | custom-call | tf_op jit(solution)/shard_map/warm/pallas_call | solution.py:414
  3.3 0.0 collective-permute-done.other_ref
  3.4 3.3 %mixer.1 = (bf16[64,1024]{1,0:T(8,128)(2,1)}, f32[64,1024]{1,0:T(8,128)}, bf16[64,1024]{1,0:T(8,128)(2,1)S(1)}, bf16[1024,1024]{1,0:T(8,128)(2,1)S(1)}) custom-call(s32[1]{0:T(128)} %bitcast.core_ref, bf16[64,1024]{1,0:T(8,128)(2,1)S(1)} %copy-done.5, bf16[64,1024]{1,0:T(8,128)(2,1)S(1)} %collective-permute-done.other_ref, f32[1,2048]{1,0:T(1,128)S(1)} %bitcast.30, ...), custom_call_target="tpu_custom_call" | custom-call | flops 536870912 | bytes 8388608 | tf_op jit(solution)/shard_map/mixer/pallas_call | solution.py:442
  6.7 0.5 collective-permute-start.1
  7.1 1.6 %near.1 = (f32[64,1024]{1,0:T(8,128)S(1)}, bf16[1024,1024]{1,0:T(8,128)(2,1)S(1)}) custom-call(s32[1]{0:T(128)} %bitcast.core_ref, bf16[64,1024]{1,0:T(8,128)(2,1)S(1)} %get-tuple-element.38.mixed_ref, bf16[1024,1024]{1,0:T(8,128)(2,1)S(1)} %get-tuple-element.39.weight_ref, bf16[2048,1024]{1,0:T(8,128)(2,1)} %weight_hbm.3), custom_call_target="tpu_custom_call" | custom-call | tf_op jit(solution)/shard_map/near/pallas_call | solution.py:485
  8.7 0.0 copy-start.12
  8.7 0.0 copy-start.13
  8.8 0.0 collective-permute-done.1.mixed_ref
  8.8 0.5 resid.1.own_ref
  9.3 0.2 collective-permute-start.2
  9.5 1.2 %collective-permute-done.2.other_ref = bf16[64,1024]{1,0:T(8,128)(2,1)S(1)} collective-permute-done((bf16[64,1024]{1,0:T(8,128)(2,1)S(1)}, bf16[64,1024]{1,0:T(8,128)(2,1)S(1)}, u32[]{:S(2)}, u32[]{:S(2)}) %collective-permute-start.2) | collective-permute-done | bytes 131104 | tf_op jit(solution)/shard_map/ppermute | solution.py:21
  10.7 1.1 %pack.1 = (bf16[512,2304]{1,0:T(8,128)(2,1)S(1)}, bf16[64,2048]{1,0:T(8,128)(2,1)}) custom-call(s32[1]{0:T(128)} %bitcast.core_ref, bf16[64,1024]{1,0:T(8,128)(2,1)S(1)} %resid.1.own_ref, bf16[64,1024]{1,0:T(8,128)(2,1)S(1)} %collective-permute-done.2.other_ref, f32[1,2048]{1,0:T(1,128)S(1)} %bitcast.29, s32[6,64]{1,0:T(8,128)S(1)} %bitcast.27), custom_call_target="tpu_custom_call" | custom-call | tf_op jit(solution)/shard_map/pack/pallas_call | solution.py:511
  11.8 1.4 %copy-done.1 = bf16[512,2304]{1,0:T(8,128)(2,1)} copy-done((bf16[512,2304]{1,0:T(8,128)(2,1)}, bf16[512,2304]{1,0:T(8,128)(2,1)S(1)}, u32[]{:S(2)}) %copy-start.1) | copy-done | bytes 2359320
  13.2 11.5 %all-to-all-start = ((bf16[64,8,2304]{2,1,0:T(8,128)(2,1)}), bf16[64,8,2304]{2,1,0:T(8,128)(2,1)S(1)}, u32[]{:S(2)}, u32[]{:S(2)}) async-start(bf16[64,8,2304]{2,1,0:T(8,128)(2,1)} %bitcast.20), calls=%async_computation | async-start | bytes 4718592 | tf_op jit(solution)/shard_map/all_to_all | solution.py:528
  24.8 0.1 collective-permute-start.3
  24.9 0.5 collective-permute-start.4
  25.4 0.1 collective-permute-start.5
  25.5 32.6 %all-to-all-done = bf16[64,8,2304]{2,1,0:T(8,128)(2,1)S(1)} async-done(((bf16[64,8,2304]{2,1,0:T(8,128)(2,1)}), bf16[64,8,2304]{2,1,0:T(8,128)(2,1)S(1)}, u32[]{:S(2)}, u32[]{:S(2)}) %all-to-all-start) | async-done | bytes 2359328 | tf_op jit(solution)/shard_map/all_to_all | solution.py:528
  58.1 0.0 collective-permute-done.3.gate2_ref
  58.1 0.0 collective-permute-done.4.up2_ref
  58.1 0.0 collective-permute-done.5.down2_ref
  58.1 0.0 copy-start.2
  58.1 1.2 %copy-done.2 = bf16[1,2048,256]{2,1,0:T(8,128)(2,1)S(1)} copy-done((bf16[1,2048,256]{2,1,0:T(8,128)(2,1)S(1)}, bf16[1,2048,256]{2,1,0:T(8,128)(2,1)}, u32[]{:S(2)}) %copy-start.2) | copy-done | bytes 1048600
  59.3 1.2 %copy-done.3 = bf16[1,2048,256]{2,1,0:T(8,128)(2,1)S(1)} copy-done((bf16[1,2048,256]{2,1,0:T(8,128)(2,1)S(1)}, bf16[1,2048,256]{2,1,0:T(8,128)(2,1)}, u32[]{:S(2)}) %copy-start.3) | copy-done | bytes 1048600
  60.6 1.2 %copy-done.4 = bf16[1,512,1024]{2,1,0:T(8,128)(2,1)S(1)} copy-done((bf16[1,512,1024]{2,1,0:T(8,128)(2,1)S(1)}, bf16[1,512,1024]{2,1,0:T(8,128)(2,1)}, u32[]{:S(2)}) %copy-start.4) | copy-done | bytes 1048600
  61.8 6.9 %experts.1 = bf16[512,2304]{1,0:T(8,128)(2,1)} custom-call(s32[1]{0:T(128)} %bitcast.core_ref, bf16[512,2304]{1,0:T(8,128)(2,1)S(1)} %bitcast.19, bf16[2048,256]{1,0:T(8,128)(2,1)S(1)} %bitcast.22, bf16[2048,256]{1,0:T(8,128)(2,1)} %collective-permute-done.3.gate2_ref, bf16[2048,256]{1,0:T(8,128)(2,1)S(1)} %bitcast.24, ...), custom_call_target="tpu_custom_call" | custom-call | tf_op jit(solution)/shard_map/experts/pallas_call | solution.py:558
  68.7 5.8 %all-to-all-start.1 = ((bf16[64,8,2304]{2,1,0:T(8,128)(2,1)}), bf16[64,8,2304]{2,1,0:T(8,128)(2,1)S(1)}, u32[]{:S(2)}, u32[]{:S(2)}) async-start(bf16[64,8,2304]{2,1,0:T(8,128)(2,1)} %bitcast.32), calls=%async_computation.1 | async-start | bytes 4718592 | tf_op jit(solution)/shard_map/all_to_all | solution.py:583
  74.5 0.0 copy-start.16
  74.5 0.0 copy-start.17
  74.5 1.0 fusion.13
  75.6 0.0 copy-start.15
  75.6 0.0 copy-start.18
  75.6 1.6 %fusion.9 = f32[64,256]{1,0:T(8,128)S(1)} fusion(bf16[2048,256]{1,0:T(8,128)(2,1)} %param.38, bf16[64,2048]{1,0:T(8,128)(2,1)} %get-tuple-element.49, bf16[64,1024]{1,0:T(8,128)(2,1)S(1)} %get-tuple-element.66, bf16[64,1024]{1,0:T(8,128)(2,1)S(1)} %get-tuple-element.65, pred[]{:T(512)S(6)} %eq.4), kind=kOutput, calls=%fused_computation.16 | convolution fusion | flops 67764224 | bytes 1638401 | tf_op jit(solution)/shard_map/dot_general | solution.py:551
  77.2 1.6 %fusion.2 = bf16[64,256]{1,0:T(8,128)(2,1)S(1)} fusion(bf16[2048,256]{1,0:T(8,128)(2,1)} %param.39, f32[64,256]{1,0:T(8,128)S(1)} %fusion.9, bf16[64,2048]{1,0:T(8,128)(2,1)} %get-tuple-element.49, bf16[64,1024]{1,0:T(8,128)(2,1)S(1)} %get-tuple-element.66, bf16[64,1024]{1,0:T(8,128)(2,1)S(1)} %get-tuple-element.65, pred[]{:T(512)S(6)} %eq.4), kind=kOutput, calls=%fused_computation.4 | convolution fusion | flops 67862528 | bytes 1671169 | tf_op jit(solution)/shard_map/dot_general | solution.py:552
  78.8 0.1 collective-permute-start.6
  79.0 0.8 pad_maximum_fusion
  79.8 0.5 table.1
  80.3 0.0 copy-start.9
  80.3 0.6 copy-done.9
  80.9 0.6 copy-done.11
  81.5 1.0 convert_add_fusion.base_hbm
  82.5 24.6 %all-to-all-done.1 = bf16[64,8,2304]{2,1,0:T(8,128)(2,1)S(1)} async-done(((bf16[64,8,2304]{2,1,0:T(8,128)(2,1)}), bf16[64,8,2304]{2,1,0:T(8,128)(2,1)S(1)}, u32[]{:S(2)}, u32[]{:S(2)}) %all-to-all-start.1) | async-done | bytes 2359328 | tf_op jit(solution)/shard_map/all_to_all | solution.py:583
  107.2 1.6 %combine.1 = (f32[64,1024]{1,0:T(8,128)S(1)}, f32[64,1024]{1,0:T(8,128)S(1)}) custom-call(bf16[512,2304]{1,0:T(8,128)(2,1)S(1)} %bitcast.18, bf16[128,512]{1,0:T(8,128)(2,1)} %copy-done.9, bf16[128,64]{1,0:T(8,128)(2,1)} %copy-done.11, f32[64,1024]{1,0:T(8,128)} %convert_add_fusion.base_hbm), custom_call_target="tpu_custom_call" | custom-call | tf_op jit(solution)/shard_map/combine/pallas_call | solution.py:590
  108.8 0.1 collective-permute-start.7
  108.9 1.5 %collective-permute-done.7 = f32[64,1024]{1,0:T(8,128)S(1)} collective-permute-done((f32[64,1024]{1,0:T(8,128)S(1)}, f32[64,1024]{1,0:T(8,128)S(1)}, u32[]{:S(2)}, u32[]{:S(2)}) %collective-permute-start.7) | collective-permute-done | bytes 262176 | tf_op jit(solution)/shard_map/ppermute | solution.py:21
  110.4 0.7 add_convert_fusion
  (25 shorter events, 0.1 us)
Async XLA Ops:
  0.6 80.9 %copy-start = (bf16[512,1024]{1,0:T(8,128)(2,1)S(1)}, bf16[512,1024]{1,0:T(8,128)(2,1)}, u32[]{:S(2)}) copy-start(bf16[512,1024]{1,0:T(8,128)(2,1)} %param.40) | copy-start | bytes 3145732
  0.6 2.7 %copy-start.5 = (bf16[64,1024]{1,0:T(8,128)(2,1)S(1)}, bf16[64,1024]{1,0:T(8,128)(2,1)}, u32[]{:S(2)}) copy-start(bf16[64,1024]{1,0:T(8,128)(2,1)} %stream_ref.1) | copy-start | bytes 393220
  0.7 2.7 %copy-start.10 = (f32[4,1024]{1,0:T(4,128)S(1)}, f32[4,1024]{1,0:T(4,128)}, u32[]{:S(2)}) copy-start(f32[4,1024]{1,0:T(4,128)} %taps_ref.1) | copy-start | bytes 49156
  0.7 2.7 %copy-start.14 = (f32[2048]{0:T(1024)S(1)}, f32[2048]{0:T(1024)}, u32[]{:S(2)}) copy-start(f32[2048]{0:T(1024)} %param.24) | copy-start | bytes 24580
  0.7 2.7 %copy-start.6 = (bf16[8,128,128]{2,1,0:T(8,128)(2,1)S(1)}, bf16[8,128,128]{2,1,0:T(8,128)(2,1)}, u32[]{:S(2)}) copy-start(bf16[8,128,128]{2,1,0:T(8,128)(2,1)} %recur_ref.1) | copy-start | bytes 786436
  0.7 2.7 %copy-start.7 = (bf16[8,128,128]{2,1,0:T(8,128)(2,1)S(1)}, bf16[8,128,128]{2,1,0:T(8,128)(2,1)}, u32[]{:S(2)}) copy-start(bf16[8,128,128]{2,1,0:T(8,128)(2,1)} %input_ref.1) | copy-start | bytes 786436
  0.7 2.7 %copy-start.8 = (f32[64,1024]{1,0:T(8,128)S(1)}, f32[64,1024]{1,0:T(8,128)}, u32[]{:S(2)}) copy-start(f32[64,1024]{1,0:T(8,128)} %state_ref.1) | copy-start | bytes 786436
  0.7 2.6 %collective-permute-start = (bf16[64,1024]{1,0:T(8,128)(2,1)}, bf16[64,1024]{1,0:T(8,128)(2,1)S(1)}, u32[]{:S(2)}, u32[]{:S(2)}) collective-permute-start(bf16[64,1024]{1,0:T(8,128)(2,1)} %stream_ref.1), channel_id=1, source_target_pairs={{0,1},{1,0},{2,3},{3,2},{4,5},{5,4},{6,7},{7,6},{8,9},{9,8},{10,11... | collective-permute-start | bytes 393224 | tf_op jit(solution)/shard_map/ppermute | solution.py:21
  6.7 2.1 %collective-permute-start.1 = (bf16[64,1024]{1,0:T(8,128)(2,1)S(1)}, bf16[64,1024]{1,0:T(8,128)(2,1)S(1)}, u32[]{:S(2)}, u32[]{:S(2)}) collective-permute-start(bf16[64,1024]{1,0:T(8,128)(2,1)S(1)} %get-tuple-element.38.mixed_ref), channel_id=1, source_target_pairs={{0,1},{1,0},{2,3},{3,2},{4,5},{5,4},{6,7},{7,6},{8,9},{9,8},{10,11... | collective-permute-start | bytes 393224 | tf_op jit(solution)/shard_map/ppermute | solution.py:21
  8.7 2.0 %copy-start.12 = (s32[64,6]{0,1:T(8,128)S(1)}, s32[64,6]{0,1:T(8,128)}, u32[]{:S(2)}) copy-start(s32[64,6]{0,1:T(8,128)} %param.33) | copy-start | bytes 4612
  8.7 2.0 %copy-start.13 = (f32[2048]{0:T(1024)S(1)}, f32[2048]{0:T(1024)}, u32[]{:S(2)}) copy-start(f32[2048]{0:T(1024)} %param.32) | copy-start | bytes 24580
  9.3 1.4 %collective-permute-start.2 = (bf16[64,1024]{1,0:T(8,128)(2,1)S(1)}, bf16[64,1024]{1,0:T(8,128)(2,1)S(1)}, u32[]{:S(2)}, u32[]{:S(2)}) collective-permute-start(bf16[64,1024]{1,0:T(8,128)(2,1)S(1)} %resid.1.own_ref), channel_id=1, source_target_pairs={{0,1},{1,0},{2,3},{3,2},{4,5},{5,4},{6,7},{7,6},{8,9},{9,8},{10,11... | collective-permute-start | bytes 393224 | tf_op jit(solution)/shard_map/ppermute | solution.py:21
  11.8 1.4 %copy-start.1 = (bf16[512,2304]{1,0:T(8,128)(2,1)}, bf16[512,2304]{1,0:T(8,128)(2,1)S(1)}, u32[]{:S(2)}) copy-start(bf16[512,2304]{1,0:T(8,128)(2,1)S(1)} %get-tuple-element.42) | copy-start | bytes 7077892
  13.2 44.9 %all-to-all-start = ((bf16[64,8,2304]{2,1,0:T(8,128)(2,1)}), bf16[64,8,2304]{2,1,0:T(8,128)(2,1)S(1)}, u32[]{:S(2)}, u32[]{:S(2)}) async-start(bf16[64,8,2304]{2,1,0:T(8,128)(2,1)} %bitcast.20), calls=%async_computation | async-start | bytes 4718592 | tf_op jit(solution)/shard_map/all_to_all | solution.py:528
  24.8 33.3 %collective-permute-start.3 = (bf16[2048,256]{1,0:T(8,128)(2,1)}, bf16[2048,256]{1,0:T(8,128)(2,1)}, u32[]{:S(2)}, u32[]{:S(2)}) collective-permute-start(bf16[2048,256]{1,0:T(8,128)(2,1)} %bitcast.21), channel_id=1, source_target_pairs={{0,1},{1,0},{2,3},{3,2},{4,5},{5,4},{6,7},{7,6},{8,9},{9,8},{10,11... | collective-permute-start | bytes 3145736 | tf_op jit(solution)/shard_map/ppermute | solution.py:21
  24.9 33.2 %collective-permute-start.4 = (bf16[2048,256]{1,0:T(8,128)(2,1)}, bf16[2048,256]{1,0:T(8,128)(2,1)}, u32[]{:S(2)}, u32[]{:S(2)}) collective-permute-start(bf16[2048,256]{1,0:T(8,128)(2,1)} %bitcast.23), channel_id=1, source_target_pairs={{0,1},{1,0},{2,3},{3,2},{4,5},{5,4},{6,7},{7,6},{8,9},{9,8},{10,11... | collective-permute-start | bytes 3145736 | tf_op jit(solution)/shard_map/ppermute | solution.py:21
  25.4 32.7 %collective-permute-start.5 = (bf16[512,1024]{1,0:T(8,128)(2,1)}, bf16[512,1024]{1,0:T(8,128)(2,1)}, u32[]{:S(2)}, u32[]{:S(2)}) collective-permute-start(bf16[512,1024]{1,0:T(8,128)(2,1)} %bitcast.25), channel_id=1, source_target_pairs={{0,1},{1,0},{2,3},{3,2},{4,5},{5,4},{6,7},{7,6},{8,9},{9,8},{10,11... | collective-permute-start | bytes 3145736 | tf_op jit(solution)/shard_map/ppermute | solution.py:21
  58.1 1.2 %copy-start.2 = (bf16[1,2048,256]{2,1,0:T(8,128)(2,1)S(1)}, bf16[1,2048,256]{2,1,0:T(8,128)(2,1)}, u32[]{:S(2)}) copy-start(bf16[1,2048,256]{2,1,0:T(8,128)(2,1)} %param.35) | copy-start | bytes 3145732
  59.3 1.2 %copy-start.3 = (bf16[1,2048,256]{2,1,0:T(8,128)(2,1)S(1)}, bf16[1,2048,256]{2,1,0:T(8,128)(2,1)}, u32[]{:S(2)}) copy-start(bf16[1,2048,256]{2,1,0:T(8,128)(2,1)} %param.36) | copy-start | bytes 3145732
  60.6 1.2 %copy-start.4 = (bf16[1,512,1024]{2,1,0:T(8,128)(2,1)S(1)}, bf16[1,512,1024]{2,1,0:T(8,128)(2,1)}, u32[]{:S(2)}) copy-start(bf16[1,512,1024]{2,1,0:T(8,128)(2,1)} %param.37) | copy-start | bytes 3145732
  68.7 38.5 %all-to-all-start.1 = ((bf16[64,8,2304]{2,1,0:T(8,128)(2,1)}), bf16[64,8,2304]{2,1,0:T(8,128)(2,1)S(1)}, u32[]{:S(2)}, u32[]{:S(2)}) async-start(bf16[64,8,2304]{2,1,0:T(8,128)(2,1)} %bitcast.32), calls=%async_computation.1 | async-start | bytes 4718592 | tf_op jit(solution)/shard_map/all_to_all | solution.py:583
  74.5 4.4 %copy-start.16 = (bf16[64,3,1024]{2,0,1:T(8,128)(2,1)S(1)}, bf16[64,3,1024]{2,0,1:T(8,128)(2,1)}, u32[]{:S(2)}) copy-start(bf16[64,3,1024]{2,0,1:T(8,128)(2,1)} %param.22) | copy-start | bytes 1179652
  74.5 4.5 %copy-start.17 = (bf16[64,1024]{1,0:T(8,128)(2,1)S(1)}, bf16[64,1024]{1,0:T(8,128)(2,1)}, u32[]{:S(2)}) copy-start(bf16[64,1024]{1,0:T(8,128)(2,1)} %get-tuple-element.51) | copy-start | bytes 393220
  75.6 4.2 %copy-start.15 = (f32[64,6]{0,1:T(8,128)S(1)}, f32[64,6]{0,1:T(8,128)}, u32[]{:S(2)}) copy-start(f32[64,6]{0,1:T(8,128)} %param.34) | copy-start | bytes 4612
  75.6 5.9 %copy-start.18 = (f32[1024]{0:T(1024)S(1)}, f32[1024]{0:T(1024)}, u32[]{:S(2)}) copy-start(f32[1024]{0:T(1024)} %param.41) | copy-start | bytes 12292
  78.8 2.7 %collective-permute-start.6 = (bf16[64,256]{1,0:T(8,128)(2,1)S(1)}, bf16[64,256]{1,0:T(8,128)(2,1)S(1)}, u32[]{:S(2)}, u32[]{:S(2)}) collective-permute-start(bf16[64,256]{1,0:T(8,128)(2,1)S(1)} %fusion.2), channel_id=1, source_target_pairs={{0,1},{1,0},{2,3},{3,2},{4,5},{5,4},{6,7},{7,6},{8,9},{9,8},{10,11... | collective-permute-start | bytes 98312 | tf_op jit(solution)/shard_map/ppermute | solution.py:21
  80.3 0.7 copy-start.9
  80.9 0.6 copy-start.11
  108.8 1.6 %collective-permute-start.7 = (f32[64,1024]{1,0:T(8,128)S(1)}, f32[64,1024]{1,0:T(8,128)S(1)}, u32[]{:S(2)}, u32[]{:S(2)}) collective-permute-start(f32[64,1024]{1,0:T(8,128)S(1)} %get-tuple-element.62), channel_id=1, source_target_pairs={{0,1},{1,0},{2,3},{3,2},{4,5},{5,4},{6,7},{7,6},{8,9},{9,8},{10,11... | collective-permute-start | bytes 786440 | tf_op jit(solution)/shard_map/ppermute | solution.py:21

commit v4 on v3

--- a/solution.py
+++ b/solution.py
@@ -15,6 +15,7 @@
 LANES = 128
 SLOTS = 9
 MAIN = 8
+CHUNKS = 4
 
 
 def swapped(x):
@@ -66,15 +67,23 @@
         ]
 
 
-def take_pieces(piece_ref, block_ref, features, rows_ref, start):
+def take_pieces(piece_ref, block_ref, features, rows_ref, low=0, high=None):
     count = block_ref.shape[0] // MAIN
     piece_ref[0] = block_ref[:, features : features + LANES].astype(F32)
     piece_ref[1] = block_ref[:, features + LANES :].astype(F32)
-    for n in range(features // LANES):
+    for n in range(low // LANES, (high or features) // LANES):
         c, part = divmod(n, 2)
-        rows_ref[start : start + count, n * LANES : (n + 1) * LANES] = piece_ref[
+        column = n * LANES - low
+        rows_ref[:count, column : column + LANES] = piece_ref[
             part, pl.ds(c, count, stride=MAIN), :
         ].astype(BF)
+
+
+def route_body(core_ref, ids_ref, table_ref, last_ref):
+    _, place = places(ids_ref[...], core_ref[0])
+    wide = each_slot(place)
+    table_ref[...] = jnp.where(wide == slot_number(wide.shape), 1.0, 0.0).astype(BF)
+    last_ref[...] = jnp.where(place == float(MAIN), 1.0, 0.0).astype(BF)
 
 
 def pack_body(
@@ -82,7 +91,8 @@
     own_ref,
     other_ref,
     gain_ref,
-    ids_ref,
+    table_ref,
+    last_ref,
     out_ref,
     norm_out_ref,
     norm_ref,
@@ -107,12 +117,8 @@
     norm_copy = pltpu.make_async_copy(norm_ref, norm_out_ref, sem)
     norm_copy.start()
     rows = norm_ref[...]
-    _, place = places(ids_ref[...], core)
-    wide = each_slot(place)
-    table = jnp.where(wide == slot_number(wide.shape), 1.0, 0.0).astype(BF)
-    last = jnp.where(place == float(MAIN), 1.0, 0.0).astype(BF)
-    out_ref[:, :features] = jnp.dot(table, rows, preferred_element_type=F32).astype(BF)
-    put_pieces(piece_ref, jnp.dot(last, rows, preferred_element_type=F32), 0, 0)
+    put_pieces(piece_ref, jnp.dot(last_ref[...], rows, preferred_element_type=F32), 0, 0)
+    out_ref[:, :features] = jnp.dot(table_ref[...], rows, preferred_element_type=F32).astype(BF)
     out_ref[:, features : features + LANES] = piece_ref[0].astype(BF)
     out_ref[:, features + LANES :] = piece_ref[1].astype(BF)
     norm_copy.wait()
@@ -299,7 +305,7 @@
     unit_other = pl.ds(pl.multiple_of((1 - core) * units, units), units)
     count = in_ref.shape[0]
     extra = count // MAIN
-    take_pieces(take_ref, in_ref, features, rows_ref, 0)
+    take_pieces(take_ref, in_ref, features, rows_ref)
     rows_ref[extra:, :] = in_ref[:, :features]
 
     def product(weight):
@@ -312,57 +318,67 @@
 
     hid_own = hidden(gate_ref, up_ref)
     hid_other = hidden(gate2_ref, up2_ref)
-    copies = []
-    for part, down in enumerate((down_ref, down2_ref)):
-        served = jnp.dot(hid_own, down[unit_own, :], preferred_element_type=F32) + jnp.dot(
-            hid_other, down[unit_other, :], preferred_element_type=F32
+
+    def served(down, span):
+        return jnp.dot(hid_own[span], down[unit_own, :], preferred_element_type=F32) + jnp.dot(
+            hid_other[span], down[unit_other, :], preferred_element_type=F32
         )
-        put_pieces(piece_ref, served[:extra], part * (half // LANES), 0)
-        cols = slice(part * half, (part + 1) * half)
-        block_ref[:, cols] = served[extra:].astype(BF)
-        if part:
-            cols = slice(half, block_ref.shape[1])
-            block_ref[:, features : features + LANES] = piece_ref[0].astype(BF)
-            block_ref[:, features + LANES :] = piece_ref[1].astype(BF)
-        copy = pltpu.make_async_copy(block_ref.at[:, cols], out_ref.at[:, cols], out_sems.at[part])
+
+    own = served(down_ref, slice(None))
+    put_pieces(piece_ref, own[:extra], 0, 0)
+    block_ref[:, :half] = own[extra:].astype(BF)
+    copies = [
+        pltpu.make_async_copy(block_ref.at[:, :half], out_ref.at[:, :half], out_sems.at[CHUNKS])
+    ]
+    copies[0].start()
+    step = count // CHUNKS
+    for n in range(CHUNKS):
+        low = extra + n * step if n else 0
+        other = served(down2_ref, slice(low, extra + (n + 1) * step))
+        if n == 0:
+            put_pieces(piece_ref, other[:extra], half // LANES, 0)
+            other = other[extra:]
+        span = slice(n * step, (n + 1) * step)
+        block_ref[span, half:features] = other.astype(BF)
+        block_ref[span, features : features + LANES] = piece_ref[0, span].astype(BF)
+        block_ref[span, features + LANES :] = piece_ref[1, span].astype(BF)
+        copy = pltpu.make_async_copy(
+            block_ref.at[span, half:], out_ref.at[span, half:], out_sems.at[n]
+        )
         copy.start()
         copies.append(copy)
-    for copy in copies:
-        copy.wait()
+    wait_all(copies)
+
+
+def half_sum(in_ref, table_ref, lasts_ref, piece_ref, last_ref, low, high, features, copies=()):
+    take_pieces(piece_ref, in_ref, features, last_ref, low, high)
+    wait_all(copies)
+    total = jnp.dot(
+        table_ref[...], in_ref[:, low:high], preferred_element_type=F32
+    ) + jnp.dot(lasts_ref[...], last_ref[...], preferred_element_type=F32)
+    rows = total.shape[0] // 2
+    return total[:rows] + total[rows:]
 
 
 def combine_body(
-    in_ref,
-    table_hbm,
-    lasts_hbm,
-    base_hbm,
-    own_ref,
-    other_ref,
-    piece_ref,
-    last_ref,
-    table_ref,
-    lasts_ref,
-    base_ref,
-    sems,
+    in_ref, table_hbm, lasts_hbm, other_ref, table_ref, lasts_ref, piece_ref, last_ref, sems
 ):
-    loads = []
-    for n, (source, target) in enumerate(
-        ((table_hbm, table_ref), (lasts_hbm, lasts_ref), (base_hbm, base_ref))
-    ):
-        copy = pltpu.make_async_copy(source, target, sems.at[n])
-        copy.start()
-        loads.append(copy)
-    rows, half = own_ref.shape
-    features = 2 * half
-    take_pieces(piece_ref, in_ref, features, last_ref, 0)
-    for copy in loads:
-        copy.wait()
-    total = jnp.dot(
-        table_ref[...], in_ref[:, :features], preferred_element_type=F32
-    ) + jnp.dot(lasts_ref[...], last_ref[...], preferred_element_type=F32)
-    total = total[:rows] + total[rows:]
-    own_ref[...] = total[:, :half] + base_ref[...]
-    other_ref[...] = total[:, half:]
+    copies = start_all(((table_hbm, table_ref), (lasts_hbm, lasts_ref)), sems)
+    half = other_ref.shape[1]
+    other_ref[...] = half_sum(
+        in_ref, table_ref, lasts_ref, piece_ref, last_ref, half, 2 * half, 2 * half, copies
+    ).astype(BF)
+
+
+def finish_body(
+    in_ref, table_ref, lasts_ref, base_hbm, own_ref, piece_ref, last_ref, base_ref, sem
+):
+    copy = pltpu.make_async_copy(base_hbm, base_ref, sem)
+    copy.start()
+    half = own_ref.shape[1]
+    total = half_sum(in_ref, table_ref, lasts_ref, piece_ref, last_ref, 0, half, 2 * half)
+    copy.wait()
+    own_ref[...] = total + base_ref[...]
 
 
 def vmem(count):
@@ -502,12 +518,23 @@
         out_specs=vmem(1)[0],
         compiler_params=pltpu.CompilerParams(vmem_limit_bytes=8 * MIB),
     )(part, mixer_other, out_other, stream)
+    ids_t, weights_t = route_ids.T, route_weights.T
+    count = experts * MAIN
     resid_other = swapped(resid)
+    send_table, send_last = pl.pallas_call(
+        route_body,
+        name="route",
+        out_shape=(
+            jax.ShapeDtypeStruct((count, seq_count), BF),
+            jax.ShapeDtypeStruct((experts, seq_count), BF),
+        ),
+        in_specs=smem() + vmem(1),
+        out_specs=tuple(vmem(2)),
+        compiler_params=pltpu.CompilerParams(vmem_limit_bytes=6 * MIB),
+    )(core_arr, ids_t)
 
     block = features + features // MAIN
-    count = experts * MAIN
     pieces = pltpu.VMEM((2, count, LANES), F32)
-    ids_t, weights_t = route_ids.T, route_weights.T
     payload, normed_two = pl.pallas_call(
         pack_body,
         name="pack",
@@ -515,7 +542,7 @@
             jax.ShapeDtypeStruct((count, block), BF),
             pltpu.HBM((seq_count, features), BF),
         ),
-        in_specs=smem() + vmem(4),
+        in_specs=smem() + vmem(5),
         out_specs=(vmem(1)[0], hbm(1)[0]),
         scratch_shapes=[
             pltpu.VMEM((seq_count, features), BF),
@@ -523,7 +550,7 @@
             pltpu.SemaphoreType.DMA,
         ],
         compiler_params=pltpu.CompilerParams(vmem_limit_bytes=14 * MIB),
-    )(core_arr, resid, resid_other, moe_gain.reshape(1, features), ids_t)
+    )(core_arr, resid, resid_other, moe_gain.reshape(1, features), send_table, send_last)
 
     incoming = lax.all_to_all(
         payload.reshape(experts, MAIN, block), "ep", split_axis=0, concat_axis=0, tiled=True
@@ -566,7 +593,7 @@
             pieces,
             pieces,
             pltpu.VMEM((experts * SLOTS, features), BF),
-            pltpu.SemaphoreType.DMA((2,)),
+            pltpu.SemaphoreType.DMA((CHUNKS + 1,)),
         ],
         compiler_params=pltpu.CompilerParams(vmem_limit_bytes=24 * MIB),
     )(
@@ -587,26 +614,39 @@
         (returned, base, new_conv, new_state, table, last)
     )
     returned = returned.reshape(count, block)
-    sum_own, sum_other = pl.pallas_call(
+    sum_other, table, last = pl.pallas_call(
         combine_body,
         name="combine",
         out_shape=(
-            jax.ShapeDtypeStruct((seq_count, half), F32),
-            jax.ShapeDtypeStruct((seq_count, half), F32),
-        ),
-        in_specs=vmem(1) + hbm(3),
-        out_specs=tuple(vmem(2)),
+            jax.ShapeDtypeStruct((seq_count, half), BF),
+            jax.ShapeDtypeStruct(table.shape, BF),
+            jax.ShapeDtypeStruct(last.shape, BF),
+        ),
+        in_specs=vmem(1) + hbm(2),
+        out_specs=tuple(vmem(3)),
         scratch_shapes=[
             pieces,
-            pltpu.VMEM((experts, features), BF),
-            pltpu.VMEM((2 * seq_count, count), BF),
-            pltpu.VMEM((2 * seq_count, experts), BF),
+            pltpu.VMEM((experts, half), BF),
+            pltpu.SemaphoreType.DMA((2,)),
+        ],
+        compiler_params=pltpu.CompilerParams(vmem_limit_bytes=10 * MIB),
+    )(returned, in_hbm(table), in_hbm(last))
+    sum_received = swapped(sum_other)
+    sum_own = pl.pallas_call(
+        finish_body,
+        name="finish",
+        out_shape=jax.ShapeDtypeStruct((seq_count, half), F32),
+        in_specs=vmem(3) + hbm(1),
+        out_specs=vmem(1)[0],
+        scratch_shapes=[
+            pieces,
+            pltpu.VMEM((experts, half), BF),
             pltpu.VMEM((seq_count, half), F32),
-            pltpu.SemaphoreType.DMA((3,)),
+            pltpu.SemaphoreType.DMA,
         ],
-        compiler_params=pltpu.CompilerParams(vmem_limit_bytes=14 * MIB),
-    )(returned, *(in_hbm(x) for x in (table, last, base)))
-    result = (sum_own + swapped(sum_other)).astype(BF)
+        compiler_params=pltpu.CompilerParams(vmem_limit_bytes=10 * MIB),
+    )(returned, table, last, in_hbm(base))
+    result = (sum_own + sum_received.astype(F32)).astype(BF)
     return (result, new_state, new_conv)
 
 

time: 113 us -> 112 us (level)
  waiting for transfers between devices: 60 us -> 58.2 us
    ppermute x8, waiting for transfers between devices: 2.76 us -> 1.01 us  [swapped(): return lax.ppermute(x, 'tp', SWAP)]
    pallas_call x0 -> x2, Pallas kernels: none -> 1.55 us  [the longest x1 1.24 us: per_device(): pl.pallas_call(finish_body, name='finish', out_shape=jax.ShapeDtypeStruct...]
  transfers between devices with their start and end apart: 10 -> 10, of which waited for: 4 -> 4; matrix products, arithmetic and copies ran while one was open for 5% -> 6% of each run, Pallas kernels for 4% -> 6%
where the time goes in v4:
time: 112 us; the launch traced here: 110 us
  waiting for transfers between devices  58.2 us (52%)
  starting transfers between devices  18.9 us (17%)
  Pallas kernels  18.8 us (17%)
  local copies, waits for them, and re-layouts  7.47 us (7%)
  matrix products  4.26 us (4%)
  other arithmetic  1.46 us (1%)
    all_to_all x1, waiting for transfers between devices, per_device(): lax.all_to_all(payload.reshape(experts, MAIN, block), 'ep', split_axis=0,...  32.6 us
    all_to_all x1, waiting for transfers between devices, per_device(): lax.all_to_all(served.reshape(experts, MAIN, block), 'ep', split_axis=0,...  24.6 us
    all_to_all x1, starting transfers between devices, per_device(): lax.all_to_all(payload.reshape(experts, MAIN, block), 'ep', split_axis=0,...  11.5 us
    pallas_call x1, Pallas kernels, per_device(): pl.pallas_call(expert_body, name='experts', out_shape=pltpu.HBM((count, b...  6.6 us
    unnamed x38, local copies, waits for them, and re-layouts  6.41 us
    all_to_all x1, starting transfers between devices, per_device(): lax.all_to_all(served.reshape(experts, MAIN, block), 'ep', split_axis=0,...  5.81 us
    pallas_call x1, Pallas kernels, per_device(): pl.pallas_call(mixer_body, name='mixer', out_shape=(pltpu.HBM((seq_count,...  3.27 us
    pallas_call x1, Pallas kernels, per_device(): pl.pallas_call(warm_body, name='warm', out_shape=(jax.ShapeDtypeStruct((f...  2.49 us
  transfers between devices with their start and end apart: 10, of which 4 were waited for; matrix products, arithmetic and copies ran while one was open for 6% of the time, Pallas kernels for 6%

profile of v4, /device:TPU:0, one launch (start us, length us, event | category | flops | bytes accessed | tf_op | source)
XLA Modules:
  0.0 110.2 jit_solution(7648141753373466432)
XLA Ops:
  0.6 0.0 copy-start
  0.7 0.1 collective-permute-start
  0.8 2.5 %warm.1 = (bf16[2048,1024]{1,0:T(8,128)(2,1)S(1)}, f32[64,1024]{1,0:T(8,128)S(1)}, f32[1,1024]{1,0:T(1,128)S(1)}) custom-call(bf16[2048,1024]{1,0:T(8,128)(2,1)} %weight_hbm.2, bf16[3,64,1024]{2,1,0:T(8,128)(2,1)} %bitcast.34, f32[4,1024]{1,0:T(4,128)} %taps_ref.1, f32[1,1024]{1,0:T(1,128)} %bitcast.36), custom_call_target="tpu_custom_call" | custom-call | tf_op jit(solution)/shard_map/warm/pallas_call | solution.py:430
  3.3 0.0 collective-permute-done.other_ref
  3.4 3.3 %mixer.1 = (bf16[64,1024]{1,0:T(8,128)(2,1)}, f32[64,1024]{1,0:T(8,128)}, bf16[64,1024]{1,0:T(8,128)(2,1)S(1)}, bf16[1024,1024]{1,0:T(8,128)(2,1)S(1)}) custom-call(s32[1]{0:T(128)} %bitcast.core_ref, bf16[64,1024]{1,0:T(8,128)(2,1)S(1)} %copy-done.5, bf16[64,1024]{1,0:T(8,128)(2,1)S(1)} %collective-permute-done.other_ref, f32[1,2048]{1,0:T(1,128)S(1)} %bitcast.31, ...), custom_call_target="tpu_custom_call" | custom-call | flops 536870912 | bytes 8388608 | tf_op jit(solution)/shard_map/mixer/pallas_call | solution.py:458
  6.7 0.5 collective-permute-start.1
  7.1 1.6 %near.1 = (f32[64,1024]{1,0:T(8,128)S(1)}, bf16[1024,1024]{1,0:T(8,128)(2,1)S(1)}) custom-call(s32[1]{0:T(128)} %bitcast.core_ref, bf16[64,1024]{1,0:T(8,128)(2,1)S(1)} %get-tuple-element.41.mixed_ref, bf16[1024,1024]{1,0:T(8,128)(2,1)S(1)} %get-tuple-element.42.weight_ref, bf16[2048,1024]{1,0:T(8,128)(2,1)} %weight_hbm.3), custom_call_target="tpu_custom_call" | custom-call | tf_op jit(solution)/shard_map/near/pallas_call | solution.py:501
  8.7 0.0 copy-start.12
  8.7 0.0 copy-start.13
  8.8 0.0 collective-permute-done.1.mixed_ref
  8.8 0.5 resid.1.own_ref
  9.3 0.2 collective-permute-start.2
  9.5 0.3 route.1
  9.8 0.9 collective-permute-done.2.other_ref
  10.7 1.0 pack.1
  11.7 1.4 %copy-done.1 = bf16[512,2304]{1,0:T(8,128)(2,1)} copy-done((bf16[512,2304]{1,0:T(8,128)(2,1)}, bf16[512,2304]{1,0:T(8,128)(2,1)S(1)}, u32[]{:S(2)}) %copy-start.1) | copy-done | bytes 2359320
  13.1 11.5 %all-to-all-start = ((bf16[64,8,2304]{2,1,0:T(8,128)(2,1)}), bf16[64,8,2304]{2,1,0:T(8,128)(2,1)S(1)}, u32[]{:S(2)}, u32[]{:S(2)}) async-start(bf16[64,8,2304]{2,1,0:T(8,128)(2,1)} %bitcast.21), calls=%async_computation | async-start | bytes 4718592 | tf_op jit(solution)/shard_map/all_to_all | solution.py:555
  24.7 0.1 collective-permute-start.3
  24.8 0.5 collective-permute-start.4
  25.3 0.1 collective-permute-start.5
  25.4 32.6 %all-to-all-done = bf16[64,8,2304]{2,1,0:T(8,128)(2,1)S(1)} async-done(((bf16[64,8,2304]{2,1,0:T(8,128)(2,1)}), bf16[64,8,2304]{2,1,0:T(8,128)(2,1)S(1)}, u32[]{:S(2)}, u32[]{:S(2)}) %all-to-all-start) | async-done | bytes 2359328 | tf_op jit(solution)/shard_map/all_to_all | solution.py:555
  58.0 0.0 collective-permute-done.3.gate2_ref
  58.0 0.0 copy-start.2
  58.0 1.2 %copy-done.2 = bf16[1,2048,256]{2,1,0:T(8,128)(2,1)S(1)} copy-done((bf16[1,2048,256]{2,1,0:T(8,128)(2,1)S(1)}, bf16[1,2048,256]{2,1,0:T(8,128)(2,1)}, u32[]{:S(2)}) %copy-start.2) | copy-done | bytes 1048600
  59.2 1.2 %copy-done.3 = bf16[1,2048,256]{2,1,0:T(8,128)(2,1)S(1)} copy-done((bf16[1,2048,256]{2,1,0:T(8,128)(2,1)S(1)}, bf16[1,2048,256]{2,1,0:T(8,128)(2,1)}, u32[]{:S(2)}) %copy-start.3) | copy-done | bytes 1048600
  60.5 1.2 %copy-done.4 = bf16[1,512,1024]{2,1,0:T(8,128)(2,1)S(1)} copy-done((bf16[1,512,1024]{2,1,0:T(8,128)(2,1)S(1)}, bf16[1,512,1024]{2,1,0:T(8,128)(2,1)}, u32[]{:S(2)}) %copy-start.4) | copy-done | bytes 1048600
  61.7 6.6 %experts.1 = bf16[512,2304]{1,0:T(8,128)(2,1)} custom-call(s32[1]{0:T(128)} %bitcast.core_ref, bf16[512,2304]{1,0:T(8,128)(2,1)S(1)} %bitcast.20, bf16[2048,256]{1,0:T(8,128)(2,1)S(1)} %bitcast.23, bf16[2048,256]{1,0:T(8,128)(2,1)} %collective-permute-done.3.gate2_ref, bf16[2048,256]{1,0:T(8,128)(2,1)S(1)} %bitcast.25, ...), custom_call_target="tpu_custom_call" | custom-call | tf_op jit(solution)/shard_map/experts/pallas_call | solution.py:585
  68.3 5.8 %all-to-all-start.1 = ((bf16[64,8,2304]{2,1,0:T(8,128)(2,1)}), bf16[64,8,2304]{2,1,0:T(8,128)(2,1)S(1)}, u32[]{:S(2)}, u32[]{:S(2)}) async-start(bf16[64,8,2304]{2,1,0:T(8,128)(2,1)} %bitcast.33), calls=%async_computation.1 | async-start | bytes 4718592 | tf_op jit(solution)/shard_map/all_to_all | solution.py:610
  74.1 0.0 copy-start.16
  74.1 0.0 copy-start.17
  74.1 1.0 fusion.13
  75.2 0.0 copy-start.15
  75.2 0.0 copy-start.18
  75.2 1.6 %fusion.9 = f32[64,256]{1,0:T(8,128)S(1)} fusion(bf16[2048,256]{1,0:T(8,128)(2,1)} %param.38, bf16[64,2048]{1,0:T(8,128)(2,1)} %get-tuple-element.54, bf16[64,1024]{1,0:T(8,128)(2,1)S(1)} %get-tuple-element.72, bf16[64,1024]{1,0:T(8,128)(2,1)S(1)} %get-tuple-element.71, pred[]{:T(512)S(6)} %eq.4), kind=kOutput, calls=%fused_computation.16 | convolution fusion | flops 67764224 | bytes 1638401 | tf_op jit(solution)/shard_map/dot_general | solution.py:578
  76.8 1.6 %fusion.2 = bf16[64,256]{1,0:T(8,128)(2,1)S(1)} fusion(bf16[2048,256]{1,0:T(8,128)(2,1)} %param.39, f32[64,256]{1,0:T(8,128)S(1)} %fusion.9, bf16[64,2048]{1,0:T(8,128)(2,1)} %get-tuple-element.54, bf16[64,1024]{1,0:T(8,128)(2,1)S(1)} %get-tuple-element.72, bf16[64,1024]{1,0:T(8,128)(2,1)S(1)} %get-tuple-element.71, pred[]{:T(512)S(6)} %eq.4), kind=kOutput, calls=%fused_computation.4 | convolution fusion | flops 67862528 | bytes 1671169 | tf_op jit(solution)/shard_map/dot_general | solution.py:579
  78.4 0.1 collective-permute-start.6
  78.6 0.8 pad_maximum_fusion
  79.4 0.5 table.1
  79.9 0.0 copy-start.9
  79.9 0.6 copy-done.9
  80.5 0.6 copy-done.11
  81.1 1.0 convert_add_fusion.base_hbm
  82.2 24.6 %all-to-all-done.1 = bf16[64,8,2304]{2,1,0:T(8,128)(2,1)S(1)} async-done(((bf16[64,8,2304]{2,1,0:T(8,128)(2,1)}), bf16[64,8,2304]{2,1,0:T(8,128)(2,1)S(1)}, u32[]{:S(2)}, u32[]{:S(2)}) %all-to-all-start.1) | async-done | bytes 2359328 | tf_op jit(solution)/shard_map/all_to_all | solution.py:610
  106.8 1.3 %combine.1 = (bf16[64,1024]{1,0:T(8,128)(2,1)S(1)}, bf16[128,512]{1,0:T(8,128)(2,1)S(1)}, bf16[128,64]{1,0:T(8,128)(2,1)S(1)}) custom-call(bf16[512,2304]{1,0:T(8,128)(2,1)S(1)} %bitcast.18, bf16[128,512]{1,0:T(8,128)(2,1)} %copy-done.9, bf16[128,64]{1,0:T(8,128)(2,1)} %copy-done.11), custom_call_target="tpu_custom_call" | custom-call | tf_op jit(solution)/shard_map/combine/pallas_call | solution.py:617
  108.1 0.1 collective-permute-start.7
  108.1 1.2 %finish.1 = f32[64,1024]{1,0:T(8,128)S(1)} custom-call(bf16[512,2304]{1,0:T(8,128)(2,1)S(1)} %bitcast.19, bf16[128,512]{1,0:T(8,128)(2,1)S(1)} %get-tuple-element.65.table_ref, bf16[128,64]{1,0:T(8,128)(2,1)S(1)} %get-tuple-element.66.lasts_ref, f32[64,1024]{1,0:T(8,128)} %convert_add_fusion.base_hbm), custom_call_target="tpu_custom_call" | custom-call | tf_op jit(solution)/shard_map/finish/pallas_call | solution.py:635
  109.4 0.1 collective-permute-done.7
  109.5 0.7 add_convert_fusion
  (27 shorter events, 0.1 us)
Async XLA Ops:
  0.6 80.5 %copy-start = (bf16[512,1024]{1,0:T(8,128)(2,1)S(1)}, bf16[512,1024]{1,0:T(8,128)(2,1)}, u32[]{:S(2)}) copy-start(bf16[512,1024]{1,0:T(8,128)(2,1)} %param.40) | copy-start | bytes 3145732
  0.6 2.7 %copy-start.5 = (bf16[64,1024]{1,0:T(8,128)(2,1)S(1)}, bf16[64,1024]{1,0:T(8,128)(2,1)}, u32[]{:S(2)}) copy-start(bf16[64,1024]{1,0:T(8,128)(2,1)} %stream_ref.1) | copy-start | bytes 393220
  0.7 2.7 %copy-start.10 = (f32[4,1024]{1,0:T(4,128)S(1)}, f32[4,1024]{1,0:T(4,128)}, u32[]{:S(2)}) copy-start(f32[4,1024]{1,0:T(4,128)} %taps_ref.1) | copy-start | bytes 49156
  0.7 2.7 %copy-start.14 = (f32[2048]{0:T(1024)S(1)}, f32[2048]{0:T(1024)}, u32[]{:S(2)}) copy-start(f32[2048]{0:T(1024)} %param.24) | copy-start | bytes 24580
  0.7 2.7 %copy-start.6 = (bf16[8,128,128]{2,1,0:T(8,128)(2,1)S(1)}, bf16[8,128,128]{2,1,0:T(8,128)(2,1)}, u32[]{:S(2)}) copy-start(bf16[8,128,128]{2,1,0:T(8,128)(2,1)} %recur_ref.1) | copy-start | bytes 786436
  0.7 2.7 %copy-start.7 = (bf16[8,128,128]{2,1,0:T(8,128)(2,1)S(1)}, bf16[8,128,128]{2,1,0:T(8,128)(2,1)}, u32[]{:S(2)}) copy-start(bf16[8,128,128]{2,1,0:T(8,128)(2,1)} %input_ref.1) | copy-start | bytes 786436
  0.7 2.7 %copy-start.8 = (f32[64,1024]{1,0:T(8,128)S(1)}, f32[64,1024]{1,0:T(8,128)}, u32[]{:S(2)}) copy-start(f32[64,1024]{1,0:T(8,128)} %state_ref.1) | copy-start | bytes 786436
  0.7 2.6 %collective-permute-start = (bf16[64,1024]{1,0:T(8,128)(2,1)}, bf16[64,1024]{1,0:T(8,128)(2,1)S(1)}, u32[]{:S(2)}, u32[]{:S(2)}) collective-permute-start(bf16[64,1024]{1,0:T(8,128)(2,1)} %stream_ref.1), channel_id=1, source_target_pairs={{0,1},{1,0},{2,3},{3,2},{4,5},{5,4},{6,7},{7,6},{8,9},{9,8},{10,11... | collective-permute-start | bytes 393224 | tf_op jit(solution)/shard_map/ppermute | solution.py:22
  6.7 2.1 %collective-permute-start.1 = (bf16[64,1024]{1,0:T(8,128)(2,1)S(1)}, bf16[64,1024]{1,0:T(8,128)(2,1)S(1)}, u32[]{:S(2)}, u32[]{:S(2)}) collective-permute-start(bf16[64,1024]{1,0:T(8,128)(2,1)S(1)} %get-tuple-element.41.mixed_ref), channel_id=1, source_target_pairs={{0,1},{1,0},{2,3},{3,2},{4,5},{5,4},{6,7},{7,6},{8,9},{9,8},{10,11... | collective-permute-start | bytes 393224 | tf_op jit(solution)/shard_map/ppermute | solution.py:22
  8.7 0.7 copy-start.12
  8.7 2.0 %copy-start.13 = (f32[2048]{0:T(1024)S(1)}, f32[2048]{0:T(1024)}, u32[]{:S(2)}) copy-start(f32[2048]{0:T(1024)} %param.32) | copy-start | bytes 24580
  9.3 1.4 %collective-permute-start.2 = (bf16[64,1024]{1,0:T(8,128)(2,1)S(1)}, bf16[64,1024]{1,0:T(8,128)(2,1)S(1)}, u32[]{:S(2)}, u32[]{:S(2)}) collective-permute-start(bf16[64,1024]{1,0:T(8,128)(2,1)S(1)} %resid.1.own_ref), channel_id=1, source_target_pairs={{0,1},{1,0},{2,3},{3,2},{4,5},{5,4},{6,7},{7,6},{8,9},{9,8},{10,11... | collective-permute-start | bytes 393224 | tf_op jit(solution)/shard_map/ppermute | solution.py:22
  11.7 1.4 %copy-start.1 = (bf16[512,2304]{1,0:T(8,128)(2,1)}, bf16[512,2304]{1,0:T(8,128)(2,1)S(1)}, u32[]{:S(2)}) copy-start(bf16[512,2304]{1,0:T(8,128)(2,1)S(1)} %get-tuple-element.47) | copy-start | bytes 7077892
  13.1 44.8 %all-to-all-start = ((bf16[64,8,2304]{2,1,0:T(8,128)(2,1)}), bf16[64,8,2304]{2,1,0:T(8,128)(2,1)S(1)}, u32[]{:S(2)}, u32[]{:S(2)}) async-start(bf16[64,8,2304]{2,1,0:T(8,128)(2,1)} %bitcast.21), calls=%async_computation | async-start | bytes 4718592 | tf_op jit(solution)/shard_map/all_to_all | solution.py:555
  24.7 33.3 %collective-permute-start.3 = (bf16[2048,256]{1,0:T(8,128)(2,1)}, bf16[2048,256]{1,0:T(8,128)(2,1)}, u32[]{:S(2)}, u32[]{:S(2)}) collective-permute-start(bf16[2048,256]{1,0:T(8,128)(2,1)} %bitcast.22), channel_id=1, source_target_pairs={{0,1},{1,0},{2,3},{3,2},{4,5},{5,4},{6,7},{7,6},{8,9},{9,8},{10,11... | collective-permute-start | bytes 3145736 | tf_op jit(solution)/shard_map/ppermute | solution.py:22
  24.8 33.2 %collective-permute-start.4 = (bf16[2048,256]{1,0:T(8,128)(2,1)}, bf16[2048,256]{1,0:T(8,128)(2,1)}, u32[]{:S(2)}, u32[]{:S(2)}) collective-permute-start(bf16[2048,256]{1,0:T(8,128)(2,1)} %bitcast.24), channel_id=1, source_target_pairs={{0,1},{1,0},{2,3},{3,2},{4,5},{5,4},{6,7},{7,6},{8,9},{9,8},{10,11... | collective-permute-start | bytes 3145736 | tf_op jit(solution)/shard_map/ppermute | solution.py:22
  25.3 32.7 %collective-permute-start.5 = (bf16[512,1024]{1,0:T(8,128)(2,1)}, bf16[512,1024]{1,0:T(8,128)(2,1)}, u32[]{:S(2)}, u32[]{:S(2)}) collective-permute-start(bf16[512,1024]{1,0:T(8,128)(2,1)} %bitcast.26), channel_id=1, source_target_pairs={{0,1},{1,0},{2,3},{3,2},{4,5},{5,4},{6,7},{7,6},{8,9},{9,8},{10,11... | collective-permute-start | bytes 3145736 | tf_op jit(solution)/shard_map/ppermute | solution.py:22
  58.0 1.2 %copy-start.2 = (bf16[1,2048,256]{2,1,0:T(8,128)(2,1)S(1)}, bf16[1,2048,256]{2,1,0:T(8,128)(2,1)}, u32[]{:S(2)}) copy-start(bf16[1,2048,256]{2,1,0:T(8,128)(2,1)} %param.35) | copy-start | bytes 3145732
  59.2 1.2 %copy-start.3 = (bf16[1,2048,256]{2,1,0:T(8,128)(2,1)S(1)}, bf16[1,2048,256]{2,1,0:T(8,128)(2,1)}, u32[]{:S(2)}) copy-start(bf16[1,2048,256]{2,1,0:T(8,128)(2,1)} %param.36) | copy-start | bytes 3145732
  60.5 1.2 %copy-start.4 = (bf16[1,512,1024]{2,1,0:T(8,128)(2,1)S(1)}, bf16[1,512,1024]{2,1,0:T(8,128)(2,1)}, u32[]{:S(2)}) copy-start(bf16[1,512,1024]{2,1,0:T(8,128)(2,1)} %param.37) | copy-start | bytes 3145732
  68.3 38.5 %all-to-all-start.1 = ((bf16[64,8,2304]{2,1,0:T(8,128)(2,1)}), bf16[64,8,2304]{2,1,0:T(8,128)(2,1)S(1)}, u32[]{:S(2)}, u32[]{:S(2)}) async-start(bf16[64,8,2304]{2,1,0:T(8,128)(2,1)} %bitcast.33), calls=%async_computation.1 | async-start | bytes 4718592 | tf_op jit(solution)/shard_map/all_to_all | solution.py:610
  74.1 4.4 %copy-start.16 = (bf16[64,3,1024]{2,0,1:T(8,128)(2,1)S(1)}, bf16[64,3,1024]{2,0,1:T(8,128)(2,1)}, u32[]{:S(2)}) copy-start(bf16[64,3,1024]{2,0,1:T(8,128)(2,1)} %param.22) | copy-start | bytes 1179652
  74.1 4.5 %copy-start.17 = (bf16[64,1024]{1,0:T(8,128)(2,1)S(1)}, bf16[64,1024]{1,0:T(8,128)(2,1)}, u32[]{:S(2)}) copy-start(bf16[64,1024]{1,0:T(8,128)(2,1)} %get-tuple-element.56) | copy-start | bytes 393220
  75.2 4.2 %copy-start.15 = (f32[64,6]{0,1:T(8,128)S(1)}, f32[64,6]{0,1:T(8,128)}, u32[]{:S(2)}) copy-start(f32[64,6]{0,1:T(8,128)} %param.34) | copy-start | bytes 4612
  75.2 5.9 %copy-start.18 = (f32[1024]{0:T(1024)S(1)}, f32[1024]{0:T(1024)}, u32[]{:S(2)}) copy-start(f32[1024]{0:T(1024)} %param.41) | copy-start | bytes 12292
  78.4 2.7 %collective-permute-start.6 = (bf16[64,256]{1,0:T(8,128)(2,1)S(1)}, bf16[64,256]{1,0:T(8,128)(2,1)S(1)}, u32[]{:S(2)}, u32[]{:S(2)}) collective-permute-start(bf16[64,256]{1,0:T(8,128)(2,1)S(1)} %fusion.2), channel_id=1, source_target_pairs={{0,1},{1,0},{2,3},{3,2},{4,5},{5,4},{6,7},{7,6},{8,9},{9,8},{10,11... | collective-permute-start | bytes 98312 | tf_op jit(solution)/shard_map/ppermute | solution.py:22
  79.9 0.7 copy-start.9
  80.5 0.6 copy-start.11
  108.1 1.4 %collective-permute-start.7 = (bf16[64,1024]{1,0:T(8,128)(2,1)S(1)}, bf16[64,1024]{1,0:T(8,128)(2,1)S(1)}, u32[]{:S(2)}, u32[]{:S(2)}) collective-permute-start(bf16[64,1024]{1,0:T(8,128)(2,1)S(1)} %get-tuple-element.68), channel_id=1, source_target_pairs={{0,1},{1,0},{2,3},{3,2},{4,5},{5,4},{6,7},{7,6},{8,9},{9,8},{10,11... | collective-permute-start | bytes 393224 | tf_op jit(solution)/shard_map/ppermute | solution.py:22

commit v5 on v4

--- a/solution.py
+++ b/solution.py
@@ -15,19 +15,10 @@
 LANES = 128
 SLOTS = 9
 MAIN = 8
-CHUNKS = 4
 
 
 def swapped(x):
     return lax.ppermute(x, "tp", SWAP)
-
-
-def in_order(core, own, other):
-    return jnp.where(
-        core == 0,
-        jnp.concatenate([own, other], axis=1),
-        jnp.concatenate([other, own], axis=1),
-    )
 
 
 def places(ids, core):
@@ -79,11 +70,27 @@
         ].astype(BF)
 
 
-def route_body(core_ref, ids_ref, table_ref, last_ref):
-    _, place = places(ids_ref[...], core_ref[0])
+def route_body(
+    core_ref, ids_ref, weights_ref, table_ref, last_ref, back_table_ref, back_last_ref
+):
+    rows = ids_ref.shape[1]
+    hits, place = places(ids_ref[...], core_ref[0])
     wide = each_slot(place)
-    table_ref[...] = jnp.where(wide == slot_number(wide.shape), 1.0, 0.0).astype(BF)
+    match = wide == slot_number(wide.shape)
+    table_ref[...] = jnp.where(match, 1.0, 0.0).astype(BF)
     last_ref[...] = jnp.where(place == float(MAIN), 1.0, 0.0).astype(BF)
+    weight = functools.reduce(
+        jnp.add,
+        [jnp.where(hit, weights_ref[k : k + 1, :], 0.0) for k, hit in enumerate(hits)],
+    )
+    high = weight.astype(BF).astype(F32)
+    low = (weight - high).astype(BF).astype(F32)
+    for n, part in enumerate((high, low)):
+        span = slice(n * rows, (n + 1) * rows)
+        back_table_ref[span, :] = jnp.transpose(jnp.where(match, each_slot(part), 0.0)).astype(BF)
+        back_last_ref[span, :] = jnp.transpose(
+            jnp.where(place == float(MAIN), part, 0.0)
+        ).astype(BF)
 
 
 def pack_body(
@@ -94,10 +101,8 @@
     table_ref,
     last_ref,
     out_ref,
-    norm_out_ref,
     norm_ref,
     piece_ref,
-    sem,
 ):
     core = core_ref[0]
     half = own_ref.shape[1]
@@ -114,14 +119,11 @@
     gain_other = jnp.where(core == 0, high, low)
     norm_ref[:, :half] = ((own - mean) * scale * gain_own).astype(BF)
     norm_ref[:, half:] = ((other - mean) * scale * gain_other).astype(BF)
-    norm_copy = pltpu.make_async_copy(norm_ref, norm_out_ref, sem)
-    norm_copy.start()
     rows = norm_ref[...]
     put_pieces(piece_ref, jnp.dot(last_ref[...], rows, preferred_element_type=F32), 0, 0)
     out_ref[:, :features] = jnp.dot(table_ref[...], rows, preferred_element_type=F32).astype(BF)
     out_ref[:, features : features + LANES] = piece_ref[0].astype(BF)
     out_ref[:, features + LANES :] = piece_ref[1].astype(BF)
-    norm_copy.wait()
 
 
 def start_all(pairs, sems):
@@ -200,8 +202,8 @@
     state_ref,
     gate_hbm,
     out_hbm,
-    branch_out_hbm,
-    state_out_hbm,
+    new_conv_hbm,
+    new_state_hbm,
     mixed_ref,
     weight_ref,
     gate_ref,
@@ -214,7 +216,13 @@
     features = 2 * half
     first = pl.ds(pl.multiple_of(core * half, half), half)
     second = pl.ds(pl.multiple_of((1 - core) * half, half), half)
-    copies = start_all(((gate_hbm, gate_ref), (out_hbm.at[first, :], weight_ref)), sems)
+    copies = start_all(
+        (
+            (gate_hbm, gate_ref),
+            (out_hbm.at[first, :], weight_ref),
+        ),
+        sems,
+    )
     own = own_ref[...].astype(F32)
     other = other_ref[...].astype(F32)
     mean = (jnp.sum(own, 1, keepdims=True) + jnp.sum(other, 1, keepdims=True)) / features
@@ -254,30 +262,13 @@
     driven = kept * (jax.nn.sigmoid(drive) * conv.astype(F32))
     state = jnp.exp(log_decay) * state_ref[...] + driven
     state_out_ref[...] = state
-    branch_copy = pltpu.make_async_copy(branch_out_ref, branch_out_hbm, sems.at[2])
+    branch_copy = pltpu.make_async_copy(branch_out_ref, new_conv_hbm.at[2], sems.at[2])
     branch_copy.start()
-    state_copy = pltpu.make_async_copy(state_out_ref, state_out_hbm, sems.at[3])
+    state_copy = pltpu.make_async_copy(state_out_ref, new_state_hbm, sems.at[3])
     state_copy.start()
     wait_all(copies[:1])
     mixed_ref[...] = (jax.nn.gelu(product(gate_ref).astype(F32)) * state).astype(BF)
     wait_all([*copies[1:], branch_copy, state_copy])
-
-
-def table_body(core_ref, ids_ref, weights_ref, table_ref, last_ref):
-    rows = ids_ref.shape[1]
-    hits, place = places(ids_ref[...], core_ref[0])
-    weight = functools.reduce(
-        jnp.add,
-        [jnp.where(hit, weights_ref[k : k + 1, :], 0.0) for k, hit in enumerate(hits)],
-    )
-    high = weight.astype(BF).astype(F32)
-    low = (weight - high).astype(BF).astype(F32)
-    wide = each_slot(place)
-    match = wide == slot_number(wide.shape)
-    for n, part in enumerate((high, low)):
-        span = slice(n * rows, (n + 1) * rows)
-        table_ref[span, :] = jnp.transpose(jnp.where(match, each_slot(part), 0.0)).astype(BF)
-        last_ref[span, :] = jnp.transpose(jnp.where(place == float(MAIN), part, 0.0)).astype(BF)
 
 
 def expert_body(
@@ -289,13 +280,31 @@
     up2_ref,
     down_ref,
     down2_ref,
+    normed_ref,
+    dense_gate_ref,
+    dense_up_ref,
+    old_conv_ref,
+    dense_down_hbm,
+    dense_scale_hbm,
+    conv_begun_hbm,
     out_ref,
-    block_ref,
+    dense_ref,
+    dense_down_ref,
+    dense_scale_ref,
+    new_conv_hbm,
     piece_ref,
     take_ref,
     rows_ref,
-    out_sems,
+    sems,
 ):
+    copies = start_all(
+        (
+            (dense_down_hbm, dense_down_ref),
+            (dense_scale_hbm, dense_scale_ref),
+            (old_conv_ref.at[pl.ds(1, 2)], new_conv_hbm.at[pl.ds(0, 2)]),
+        ),
+        sems,
+    )
     core = core_ref[0]
     features, units = gate_ref.shape
     half = features // 2
@@ -308,51 +317,34 @@
     take_pieces(take_ref, in_ref, features, rows_ref)
     rows_ref[extra:, :] = in_ref[:, :features]
 
-    def product(weight):
-        return jnp.dot(
-            rows_ref[:, :half], weight[first, :], preferred_element_type=F32
-        ) + jnp.dot(rows_ref[:, half:], weight[second, :], preferred_element_type=F32)
-
-    def hidden(gate, up):
-        return (jax.nn.silu(product(gate)) * product(up)).astype(BF)
-
-    hid_own = hidden(gate_ref, up_ref)
-    hid_other = hidden(gate2_ref, up2_ref)
+    def hidden(rows, gate, up):
+        gated, raised = (
+            jnp.dot(rows[:, :half], weight[first, :], preferred_element_type=F32)
+            + jnp.dot(rows[:, half:], weight[second, :], preferred_element_type=F32)
+            for weight in (gate, up)
+        )
+        return (jax.nn.silu(gated) * raised).astype(BF)
+
+    dense_ref[...] = hidden(normed_ref, dense_gate_ref, dense_up_ref)
+    hid_own = hidden(rows_ref, gate_ref, up_ref)
+    hid_other = hidden(rows_ref, gate2_ref, up2_ref)
 
     def served(down, span):
         return jnp.dot(hid_own[span], down[unit_own, :], preferred_element_type=F32) + jnp.dot(
             hid_other[span], down[unit_other, :], preferred_element_type=F32
         )
 
-    own = served(down_ref, slice(None))
-    put_pieces(piece_ref, own[:extra], 0, 0)
-    block_ref[:, :half] = own[extra:].astype(BF)
-    copies = [
-        pltpu.make_async_copy(block_ref.at[:, :half], out_ref.at[:, :half], out_sems.at[CHUNKS])
-    ]
-    copies[0].start()
-    step = count // CHUNKS
-    for n in range(CHUNKS):
-        low = extra + n * step if n else 0
-        other = served(down2_ref, slice(low, extra + (n + 1) * step))
-        if n == 0:
-            put_pieces(piece_ref, other[:extra], half // LANES, 0)
-            other = other[extra:]
-        span = slice(n * step, (n + 1) * step)
-        block_ref[span, half:features] = other.astype(BF)
-        block_ref[span, features : features + LANES] = piece_ref[0, span].astype(BF)
-        block_ref[span, features + LANES :] = piece_ref[1, span].astype(BF)
-        copy = pltpu.make_async_copy(
-            block_ref.at[span, half:], out_ref.at[span, half:], out_sems.at[n]
-        )
-        copy.start()
-        copies.append(copy)
+    for part, down in enumerate((down_ref, down2_ref)):
+        values = served(down, slice(None))
+        put_pieces(piece_ref, values[:extra], part * (half // LANES), 0)
+        out_ref[:, part * half : (part + 1) * half] = values[extra:].astype(BF)
+    out_ref[:, features : features + LANES] = piece_ref[0].astype(BF)
+    out_ref[:, features + LANES :] = piece_ref[1].astype(BF)
     wait_all(copies)
 
 
-def half_sum(in_ref, table_ref, lasts_ref, piece_ref, last_ref, low, high, features, copies=()):
+def half_sum(in_ref, table_ref, lasts_ref, piece_ref, last_ref, low, high, features):
     take_pieces(piece_ref, in_ref, features, last_ref, low, high)
-    wait_all(copies)
     total = jnp.dot(
         table_ref[...], in_ref[:, low:high], preferred_element_type=F32
     ) + jnp.dot(lasts_ref[...], last_ref[...], preferred_element_type=F32)
@@ -360,25 +352,39 @@
     return total[:rows] + total[rows:]
 
 
-def combine_body(
-    in_ref, table_hbm, lasts_hbm, other_ref, table_ref, lasts_ref, piece_ref, last_ref, sems
-):
-    copies = start_all(((table_hbm, table_ref), (lasts_hbm, lasts_ref)), sems)
+def combine_body(in_ref, table_ref, lasts_ref, other_ref, piece_ref, last_ref):
     half = other_ref.shape[1]
     other_ref[...] = half_sum(
-        in_ref, table_ref, lasts_ref, piece_ref, last_ref, half, 2 * half, 2 * half, copies
+        in_ref, table_ref, lasts_ref, piece_ref, last_ref, half, 2 * half, 2 * half
     ).astype(BF)
 
 
 def finish_body(
-    in_ref, table_ref, lasts_ref, base_hbm, own_ref, piece_ref, last_ref, base_ref, sem
+    core_ref,
+    in_ref,
+    table_ref,
+    lasts_ref,
+    resid_ref,
+    own_hid_ref,
+    other_hid_ref,
+    down_ref,
+    scale_ref,
+    own_ref,
+    piece_ref,
+    last_ref,
 ):
-    copy = pltpu.make_async_copy(base_hbm, base_ref, sem)
-    copy.start()
+    core = core_ref[0]
     half = own_ref.shape[1]
-    total = half_sum(in_ref, table_ref, lasts_ref, piece_ref, last_ref, 0, half, 2 * half)
-    copy.wait()
-    own_ref[...] = total + base_ref[...]
+    units = own_hid_ref.shape[1]
+    unit_own = pl.ds(pl.multiple_of(core * units, units), units)
+    unit_other = pl.ds(pl.multiple_of((1 - core) * units, units), units)
+    dense = jnp.dot(own_hid_ref[...], down_ref[unit_own, :], preferred_element_type=F32) + jnp.dot(
+        other_hid_ref[...], down_ref[unit_other, :], preferred_element_type=F32
+    )
+    base = resid_ref[...].astype(F32) + scale_ref[...] * dense.astype(BF).astype(F32)
+    own_ref[...] = base + half_sum(
+        in_ref, table_ref, lasts_ref, piece_ref, last_ref, 0, half, 2 * half
+    )
 
 
 def vmem(count):
@@ -427,18 +433,18 @@
     experts = lax.axis_size("ep")
     own_gate, own_up, own_down = expert_gate[0], expert_up[0], expert_down[0]
     stream_other = swapped(stream)
-    branch_near, conv_part, decay = pl.pallas_call(
+    branch_near, conv_part, decay, old_conv = pl.pallas_call(
         warm_body,
         name="warm",
         out_shape=(
             jax.ShapeDtypeStruct((features, half), BF),
             jax.ShapeDtypeStruct((seq_count, half), F32),
             jax.ShapeDtypeStruct((1, half), F32),
+            jax.ShapeDtypeStruct((3, seq_count, half), BF),
         ),
         in_specs=hbm(4),
-        out_specs=tuple(vmem(3)),
+        out_specs=tuple(vmem(4)),
         scratch_shapes=[
-            pltpu.VMEM((3, seq_count, half), BF),
             pltpu.VMEM((4, half), F32),
             pltpu.VMEM((1, half), F32),
             pltpu.SemaphoreType.DMA((4,)),
@@ -455,11 +461,11 @@
             )
         )
     )
-    branch_in, new_state, mixer_in, out_own = pl.pallas_call(
+    conv_begun, new_state, mixer_in, out_own = pl.pallas_call(
         mixer_body,
         name="mixer",
         out_shape=(
-            pltpu.HBM((seq_count, half), BF),
+            pltpu.HBM((3, seq_count, half), BF),
             pltpu.HBM((seq_count, half), F32),
             jax.ShapeDtypeStruct((seq_count, half), BF),
             jax.ShapeDtypeStruct((half, half), BF),
@@ -521,17 +527,19 @@
     ids_t, weights_t = route_ids.T, route_weights.T
     count = experts * MAIN
     resid_other = swapped(resid)
-    send_table, send_last = pl.pallas_call(
+    send_table, send_last, table, last = pl.pallas_call(
         route_body,
         name="route",
         out_shape=(
             jax.ShapeDtypeStruct((count, seq_count), BF),
             jax.ShapeDtypeStruct((experts, seq_count), BF),
-        ),
-        in_specs=smem() + vmem(1),
-        out_specs=tuple(vmem(2)),
-        compiler_params=pltpu.CompilerParams(vmem_limit_bytes=6 * MIB),
-    )(core_arr, ids_t)
+            jax.ShapeDtypeStruct((2 * seq_count, count), BF),
+            jax.ShapeDtypeStruct((2 * seq_count, experts), BF),
+        ),
+        in_specs=smem() + vmem(2),
+        out_specs=tuple(vmem(4)),
+        compiler_params=pltpu.CompilerParams(vmem_limit_bytes=8 * MIB),
+    )(core_arr, ids_t, weights_t)
 
     block = features + features // MAIN
     pieces = pltpu.VMEM((2, count, LANES), F32)
@@ -540,62 +548,39 @@
         name="pack",
         out_shape=(
             jax.ShapeDtypeStruct((count, block), BF),
-            pltpu.HBM((seq_count, features), BF),
+            jax.ShapeDtypeStruct((seq_count, features), BF),
         ),
         in_specs=smem() + vmem(5),
-        out_specs=(vmem(1)[0], hbm(1)[0]),
-        scratch_shapes=[
-            pltpu.VMEM((seq_count, features), BF),
-            pieces,
-            pltpu.SemaphoreType.DMA,
-        ],
+        out_specs=tuple(vmem(2)),
+        scratch_shapes=[pieces],
         compiler_params=pltpu.CompilerParams(vmem_limit_bytes=14 * MIB),
     )(core_arr, resid, resid_other, moe_gain.reshape(1, features), send_table, send_last)
 
     incoming = lax.all_to_all(
         payload.reshape(experts, MAIN, block), "ep", split_axis=0, concat_axis=0, tiled=True
     )
-    incoming, normed_two, ids_late, weights_late, branch_in, conv_late = lax.optimization_barrier(
-        (incoming, normed_two, ids_t, weights_t, branch_in, conv_state)
-    )
-    new_conv = jnp.concatenate([conv_late[:, 1:], branch_in[:, None]], axis=1)
+    incoming, normed_two = lax.optimization_barrier((incoming, normed_two))
     incoming = incoming.reshape(count, block)
-    table, last = pl.pallas_call(
-        table_body,
-        name="table",
-        out_shape=(
-            jax.ShapeDtypeStruct((2 * seq_count, count), BF),
-            jax.ShapeDtypeStruct((2 * seq_count, experts), BF),
-        ),
-        in_specs=smem() + vmem(2),
-        out_specs=tuple(vmem(2)),
-        compiler_params=pltpu.CompilerParams(vmem_limit_bytes=8 * MIB),
-    )(core_arr, ids_late, weights_late)
-
-    own_two, other_two = normed_two[:, :half], normed_two[:, half:]
-    whole_two = in_order(core, own_two, other_two)
-    dense_hidden = (
-        jax.nn.silu(jnp.dot(whole_two, dense_gate, preferred_element_type=F32))
-        * jnp.dot(whole_two, dense_up, preferred_element_type=F32)
-    ).astype(BF)
-    dense_whole = in_order(core, dense_hidden, swapped(dense_hidden))
-    dense_out = jnp.dot(dense_whole, dense_down, preferred_element_type=F32).astype(BF)
-    base = resid.astype(F32) + dense_scale * dense_out.astype(F32)
-
-    served = pl.pallas_call(
+    served, dense_hidden, down_near, scale_near, new_conv = pl.pallas_call(
         expert_body,
         name="experts",
-        out_shape=pltpu.HBM((count, block), BF),
-        in_specs=smem() + vmem(7),
-        out_specs=hbm(1)[0],
+        out_shape=(
+            jax.ShapeDtypeStruct((count, block), BF),
+            jax.ShapeDtypeStruct((seq_count, dense_gate.shape[1]), BF),
+            jax.ShapeDtypeStruct(dense_down.shape, BF),
+            jax.ShapeDtypeStruct((1, half), F32),
+            pltpu.HBM((3, seq_count, half), BF),
+        ),
+        in_specs=smem() + vmem(11) + hbm(3),
+        out_specs=tuple(vmem(4) + hbm(1)),
+        input_output_aliases={14: 4},
         scratch_shapes=[
-            pltpu.VMEM((count, block), BF),
             pieces,
             pieces,
             pltpu.VMEM((experts * SLOTS, features), BF),
-            pltpu.SemaphoreType.DMA((CHUNKS + 1,)),
+            pltpu.SemaphoreType.DMA((3,)),
         ],
-        compiler_params=pltpu.CompilerParams(vmem_limit_bytes=24 * MIB),
+        compiler_params=pltpu.CompilerParams(vmem_limit_bytes=20 * MIB),
     )(
         core_arr,
         incoming,
@@ -605,48 +590,51 @@
         other_up,
         own_down,
         other_down,
-    )
-
+        normed_two,
+        dense_gate,
+        dense_up,
+        old_conv,
+        in_hbm(dense_down),
+        in_hbm(dense_scale.reshape(1, half)),
+        in_hbm(conv_begun),
+    )
+    dense_other = swapped(dense_hidden)
     returned = lax.all_to_all(
         served.reshape(experts, MAIN, block), "ep", split_axis=0, concat_axis=0, tiled=True
     )
-    returned, base, new_conv, new_state, table, last = lax.optimization_barrier(
-        (returned, base, new_conv, new_state, table, last)
-    )
     returned = returned.reshape(count, block)
-    sum_other, table, last = pl.pallas_call(
+    halves = [pieces, pltpu.VMEM((experts, half), BF)]
+    sum_other = pl.pallas_call(
         combine_body,
         name="combine",
-        out_shape=(
-            jax.ShapeDtypeStruct((seq_count, half), BF),
-            jax.ShapeDtypeStruct(table.shape, BF),
-            jax.ShapeDtypeStruct(last.shape, BF),
-        ),
-        in_specs=vmem(1) + hbm(2),
-        out_specs=tuple(vmem(3)),
-        scratch_shapes=[
-            pieces,
-            pltpu.VMEM((experts, half), BF),
-            pltpu.SemaphoreType.DMA((2,)),
-        ],
+        out_shape=jax.ShapeDtypeStruct((seq_count, half), BF),
+        in_specs=vmem(3),
+        out_specs=vmem(1)[0],
+        scratch_shapes=halves,
         compiler_params=pltpu.CompilerParams(vmem_limit_bytes=10 * MIB),
-    )(returned, in_hbm(table), in_hbm(last))
+    )(returned, table, last)
     sum_received = swapped(sum_other)
     sum_own = pl.pallas_call(
         finish_body,
         name="finish",
         out_shape=jax.ShapeDtypeStruct((seq_count, half), F32),
-        in_specs=vmem(3) + hbm(1),
+        in_specs=smem() + vmem(8),
         out_specs=vmem(1)[0],
-        scratch_shapes=[
-            pieces,
-            pltpu.VMEM((experts, half), BF),
-            pltpu.VMEM((seq_count, half), F32),
-            pltpu.SemaphoreType.DMA,
-        ],
+        scratch_shapes=halves,
         compiler_params=pltpu.CompilerParams(vmem_limit_bytes=10 * MIB),
-    )(returned, table, last, in_hbm(base))
+    )(
+        core_arr,
+        returned,
+        table,
+        last,
+        resid,
+        dense_hidden,
+        dense_other,
+        down_near,
+        scale_near,
+    )
     result = (sum_own + sum_received.astype(F32)).astype(BF)
+    new_conv = new_conv.transpose(1, 0, 2)
     return (result, new_state, new_conv)
 
 

time: 112 us -> 117 us (1.045)
  blocking collectives: 0 us -> 38.4 us
  waiting for transfers between devices: 58.2 us -> 33.9 us
  starting transfers between devices: 18.9 us -> 13.7 us
  matrix products: 4.26 us -> 0 us
  local copies, waits for them, and re-layouts: 7.47 us -> 11 us
  Pallas kernels: 18.8 us -> 16.5 us
    all_to_all x0 -> x1, blocking collectives: none -> 38.4 us  [per_device(): lax.all_to_all(served.reshape(experts, MAIN, block), 'ep', split_axis=0,...]
    all_to_all x1 -> x0, waiting for transfers between devices: 24.6 us -> none  [per_device(): lax.all_to_all(served.reshape(experts, MAIN, block), 'ep', split_axis=0,...]
    all_to_all x1 -> x0, starting transfers between devices: 5.81 us -> none  [per_device(): lax.all_to_all(served.reshape(experts, MAIN, block), 'ep', split_axis=0,...]
    unnamed x38 -> x46, local copies, waits for them, and re-layouts: 6.41 us -> 11 us
    dot_general x3 -> x0, matrix products: 4.26 us -> none  [the longest x1 1.62 us: per_device(): jnp.dot(whole_two, dense_gate, preferred_element_type=F32)]
    pallas_call x4 -> x3, Pallas kernels: 11.6 us -> 9.82 us  [the longest x1 6.14 us: per_device(): pl.pallas_call(expert_body, name='experts', out_shape=(jax.ShapeDtypeStru...]
  transfers between devices with their start and end apart: 10 -> 9, of which waited for: 4 -> 2; matrix products, arithmetic and copies ran while one was open for 6% -> 0% of each run, Pallas kernels for 6% -> 4%
where the time goes in v5:
time: 117 us; the launch traced here: 115 us
  blocking collectives  38.4 us (33%)
  waiting for transfers between devices  33.9 us (29%)
  Pallas kernels  16.5 us (14%)
  starting transfers between devices  13.7 us (12%)
  local copies, waits for them, and re-layouts  11 us (9%)
    all_to_all x1, blocking collectives, per_device(): lax.all_to_all(served.reshape(experts, MAIN, block), 'ep', split_axis=0,...  38.4 us
    all_to_all x1, waiting for transfers between devices, per_device(): lax.all_to_all(payload.reshape(experts, MAIN, block), 'ep', split_axis=0,...  33 us
    all_to_all x1, starting transfers between devices, per_device(): lax.all_to_all(payload.reshape(experts, MAIN, block), 'ep', split_axis=0,...  11.7 us
    unnamed x46, local copies, waits for them, and re-layouts  11 us
    pallas_call x1, Pallas kernels, per_device(): pl.pallas_call(expert_body, name='experts', out_shape=(jax.ShapeDtypeStru...  6.14 us
    pallas_call x1, Pallas kernels, per_device(): pl.pallas_call(mixer_body, name='mixer', out_shape=(pltpu.HBM((3, seq_cou...  3.27 us
    pallas_call x1, Pallas kernels, per_device(): pl.pallas_call(warm_body, name='warm', out_shape=(jax.ShapeDtypeStruct((f...  2.5 us
  transfers between devices with their start and end apart: 9, of which 2 were waited for; matrix products, arithmetic and copies ran while one was open for 0% of the time, Pallas kernels for 4%

profile of v5, /device:TPU:0, one launch (start us, length us, event | category | flops | bytes accessed | tf_op | source)
XLA Modules:
  0.0 115.1 jit_solution(8745162094338160952)
XLA Ops:
  0.6 0.0 copy-start.6
  0.7 0.1 collective-permute-start
  0.8 2.5 %warm.1 = (bf16[2048,1024]{1,0:T(8,128)(2,1)S(1)}, f32[64,1024]{1,0:T(8,128)S(1)}, f32[1,1024]{1,0:T(1,128)S(1)}, bf16[3,64,1024]{2,1,0:T(8,128)(2,1)S(1)}) custom-call(bf16[2048,1024]{1,0:T(8,128)(2,1)} %weight_hbm.2, bf16[3,64,1024]{2,1,0:T(8,128)(2,1)} %bitcast.32, f32[4,1024]{1,0:T(4,128)} %taps_ref.1, f32[1,1024]{1,0:T(1,128)} %bitcast.34), custom_call_target="tpu_custom_call" | custom-call | tf_op jit(solution)/shard_map/warm/pallas_call | solution.py:436
  3.3 0.8 copy-done.9
  4.1 0.0 collective-permute-done.other_ref
  4.1 3.3 %mixer.1 = (bf16[3,64,1024]{2,1,0:T(8,128)(2,1)}, f32[64,1024]{1,0:T(8,128)}, bf16[64,1024]{1,0:T(8,128)(2,1)S(1)}, bf16[1024,1024]{1,0:T(8,128)(2,1)S(1)}) custom-call(s32[1]{0:T(128)} %bitcast.core_ref, bf16[64,1024]{1,0:T(8,128)(2,1)S(1)} %copy-done.6, bf16[64,1024]{1,0:T(8,128)(2,1)S(1)} %collective-permute-done.other_ref, f32[1,2048]{1,0:T(1,128)S(1)} %bitcast.28, ...), custom_call_target="tpu_custom_call" | custom-call | flops 536870912 | bytes 8388608 | tf_op jit(solution)/shard_map/mixer/pallas_call | solution.py:464
  7.4 0.5 collective-permute-start.1
  7.9 1.6 %near.1 = (f32[64,1024]{1,0:T(8,128)S(1)}, bf16[1024,1024]{1,0:T(8,128)(2,1)S(1)}) custom-call(s32[1]{0:T(128)} %bitcast.core_ref, bf16[64,1024]{1,0:T(8,128)(2,1)S(1)} %get-tuple-element.34.mixed_ref, bf16[1024,1024]{1,0:T(8,128)(2,1)S(1)} %get-tuple-element.35.weight_ref, bf16[2048,1024]{1,0:T(8,128)(2,1)} %weight_hbm.3), custom_call_target="tpu_custom_call" | custom-call | tf_op jit(solution)/shard_map/near/pallas_call | solution.py:507
  9.5 0.0 copy-start.21
  9.5 0.0 copy-start.22
  9.5 0.0 copy-start.19
  9.5 0.0 collective-permute-done.1.mixed_ref
  9.5 0.5 resid.1.own_ref.resid_ref
  10.0 0.2 collective-permute-start.2
  10.2 0.5 route.1
  10.7 0.0 copy-start.7
  10.7 0.6 copy-done.7
  11.4 0.6 copy-done.16
  12.0 0.0 collective-permute-done.2.other_ref
  12.0 0.0 copy-done.19
  12.0 1.0 pack.1
  13.0 1.4 %copy-done = bf16[512,2304]{1,0:T(8,128)(2,1)} copy-done((bf16[512,2304]{1,0:T(8,128)(2,1)}, bf16[512,2304]{1,0:T(8,128)(2,1)S(1)}, u32[]{:S(2)}) %copy-start) | copy-done | bytes 2359320
  14.4 0.7 copy-done.14
  15.1 11.7 %all-to-all-start = ((bf16[64,8,2304]{2,1,0:T(8,128)(2,1)}), bf16[64,8,2304]{2,1,0:T(8,128)(2,1)S(1)}, u32[]{:S(2)}, u32[]{:S(2)}) async-start(bf16[64,8,2304]{2,1,0:T(8,128)(2,1)} %bitcast.19), calls=%async_computation | async-start | bytes 4718592 | tf_op jit(solution)/shard_map/all_to_all | solution.py:559
  26.8 0.2 collective-permute-start.3
  27.0 0.4 collective-permute-start.4
  27.4 0.1 collective-permute-start.5
  27.5 33.0 %all-to-all-done = bf16[64,8,2304]{2,1,0:T(8,128)(2,1)S(1)} async-done(((bf16[64,8,2304]{2,1,0:T(8,128)(2,1)}), bf16[64,8,2304]{2,1,0:T(8,128)(2,1)S(1)}, u32[]{:S(2)}, u32[]{:S(2)}) %all-to-all-start) | async-done | bytes 2359328 | tf_op jit(solution)/shard_map/all_to_all | solution.py:559
  60.5 0.0 collective-permute-done.3.gate2_ref
  60.5 0.0 collective-permute-done.4.up2_ref
  60.5 0.0 collective-permute-done.5.down2_ref
  60.5 0.0 copy-start.2
  60.5 1.2 %copy-done.2 = bf16[1,2048,256]{2,1,0:T(8,128)(2,1)S(1)} copy-done((bf16[1,2048,256]{2,1,0:T(8,128)(2,1)S(1)}, bf16[1,2048,256]{2,1,0:T(8,128)(2,1)}, u32[]{:S(2)}) %copy-start.2) | copy-done | bytes 1048600
  61.8 1.2 %copy-done.3 = bf16[1,512,1024]{2,1,0:T(8,128)(2,1)S(1)} copy-done((bf16[1,512,1024]{2,1,0:T(8,128)(2,1)S(1)}, bf16[1,512,1024]{2,1,0:T(8,128)(2,1)}, u32[]{:S(2)}) %copy-start.3) | copy-done | bytes 1048600
  63.0 1.2 %copy-done.4 = bf16[2048,256]{1,0:T(8,128)(2,1)S(1)} copy-done((bf16[2048,256]{1,0:T(8,128)(2,1)S(1)}, bf16[2048,256]{1,0:T(8,128)(2,1)}, u32[]{:S(2)}) %copy-start.4) | copy-done | bytes 1048600
  64.2 1.2 %copy-done.5 = bf16[2048,256]{1,0:T(8,128)(2,1)S(1)} copy-done((bf16[2048,256]{1,0:T(8,128)(2,1)S(1)}, bf16[2048,256]{1,0:T(8,128)(2,1)}, u32[]{:S(2)}) %copy-start.5) | copy-done | bytes 1048600
  65.4 1.0 copy-done.10
  66.4 0.9 copy-done.15
  67.4 6.1 %experts.1 = (bf16[512,2304]{1,0:T(8,128)(2,1)S(1)}, bf16[64,256]{1,0:T(8,128)(2,1)S(1)}, bf16[512,1024]{1,0:T(8,128)(2,1)S(1)}, f32[1,1024]{1,0:T(1,128)S(1)}, bf16[3,64,1024]{2,1,0:T(8,128)(2,1)}) custom-call(s32[1]{0:T(128)} %bitcast.core_ref, bf16[512,2304]{1,0:T(8,128)(2,1)S(1)} %bitcast.18, ...), custom_call_target="tpu_custom_call", output_to_operand_aliasing={{4}: (14, {})} | custom-call | tf_op jit(solution)/shard_map/experts/pallas_call | solution.py:564
  73.5 0.0 copy-start.8
  73.5 38.4 %all_to_all.10 = bf16[64,8,2304]{2,1,0:T(8,128)(2,1)S(1)} all-to-all(bf16[64,8,2304]{2,1,0:T(8,128)(2,1)S(1)} %bitcast.20), channel_id=1, replica_groups=mesh['ep'=64,'tp'=2] {'ep'}, dimensions={0} | all-to-all | bytes 4718592 | tf_op jit(solution)/shard_map/all_to_all | solution.py:602
  111.9 0.4 combine.1
  112.3 0.1 collective-permute-start.7
  112.4 0.5 collective-permute-start.6
  112.9 0.9 collective-permute-done.6.other_hid_ref
  113.8 0.5 finish.1
  114.4 0.0 collective-permute-done.7
  114.4 0.7 add_convert_fusion
  (27 shorter events, 0.1 us)
Async XLA Ops:
  0.6 3.4 %copy-start.6 = (bf16[64,1024]{1,0:T(8,128)(2,1)S(1)}, bf16[64,1024]{1,0:T(8,128)(2,1)}, u32[]{:S(2)}) copy-start(bf16[64,1024]{1,0:T(8,128)(2,1)} %stream_ref.1) | copy-start | bytes 393220
  0.6 3.4 %copy-start.18 = (f32[4,1024]{1,0:T(4,128)S(1)}, f32[4,1024]{1,0:T(4,128)}, u32[]{:S(2)}) copy-start(f32[4,1024]{1,0:T(4,128)} %taps_ref.1) | copy-start | bytes 49156
  0.7 3.4 %copy-start.12 = (bf16[8,128,128]{2,1,0:T(8,128)(2,1)S(1)}, bf16[8,128,128]{2,1,0:T(8,128)(2,1)}, u32[]{:S(2)}) copy-start(bf16[8,128,128]{2,1,0:T(8,128)(2,1)} %input_ref.1) | copy-start | bytes 786436
  0.7 3.4 %copy-start.11 = (bf16[8,128,128]{2,1,0:T(8,128)(2,1)S(1)}, bf16[8,128,128]{2,1,0:T(8,128)(2,1)}, u32[]{:S(2)}) copy-start(bf16[8,128,128]{2,1,0:T(8,128)(2,1)} %recur_ref.1) | copy-start | bytes 786436
  0.7 3.4 %copy-start.20 = (f32[2048]{0:T(1024)S(1)}, f32[2048]{0:T(1024)}, u32[]{:S(2)}) copy-start(f32[2048]{0:T(1024)} %param.24) | copy-start | bytes 24580
  0.7 3.4 %copy-start.13 = (f32[64,1024]{1,0:T(8,128)S(1)}, f32[64,1024]{1,0:T(8,128)}, u32[]{:S(2)}) copy-start(f32[64,1024]{1,0:T(8,128)} %state_ref.1) | copy-start | bytes 786436
  0.7 3.4 %collective-permute-start = (bf16[64,1024]{1,0:T(8,128)(2,1)}, bf16[64,1024]{1,0:T(8,128)(2,1)S(1)}, u32[]{:S(2)}, u32[]{:S(2)}) collective-permute-start(bf16[64,1024]{1,0:T(8,128)(2,1)} %stream_ref.1), channel_id=1, source_target_pairs={{0,1},{1,0},{2,3},{3,2},{4,5},{5,4},{6,7},{7,6},{8,9},{9,8},{10,11... | collective-permute-start | bytes 393224 | tf_op jit(solution)/shard_map/ppermute | solution.py:21
  3.3 0.8 copy-start.9
  7.4 2.1 %collective-permute-start.1 = (bf16[64,1024]{1,0:T(8,128)(2,1)S(1)}, bf16[64,1024]{1,0:T(8,128)(2,1)S(1)}, u32[]{:S(2)}, u32[]{:S(2)}) collective-permute-start(bf16[64,1024]{1,0:T(8,128)(2,1)S(1)} %get-tuple-element.34.mixed_ref), channel_id=1, source_target_pairs={{0,1},{1,0},{2,3},{3,2},{4,5},{5,4},{6,7},{7,6},{8,9},{9,8},{10,11... | collective-permute-start | bytes 393224 | tf_op jit(solution)/shard_map/ppermute | solution.py:21
  9.5 0.8 copy-start.21
  9.5 0.8 copy-start.22
  9.5 2.5 %copy-start.19 = (f32[2048]{0:T(1024)S(1)}, f32[2048]{0:T(1024)}, u32[]{:S(2)}) copy-start(f32[2048]{0:T(1024)} %param.32) | copy-start | bytes 24580
  10.0 2.0 %collective-permute-start.2 = (bf16[64,1024]{1,0:T(8,128)(2,1)S(1)}, bf16[64,1024]{1,0:T(8,128)(2,1)S(1)}, u32[]{:S(2)}, u32[]{:S(2)}) collective-permute-start(bf16[64,1024]{1,0:T(8,128)(2,1)S(1)} %resid.1.own_ref.resid_ref), channel_id=1, source_target_pairs={{0,1},{1,0},{2,3},{3,2},{4,5},{5,4},{6,7},{7,6},{8,9},{9,8},{10,11... | collective-permute-start | bytes 393224 | tf_op jit(solution)/shard_map/ppermute | solution.py:21
  10.7 0.7 copy-start.7
  11.4 0.6 copy-start.16
  13.0 1.4 %copy-start = (bf16[512,2304]{1,0:T(8,128)(2,1)}, bf16[512,2304]{1,0:T(8,128)(2,1)S(1)}, u32[]{:S(2)}) copy-start(bf16[512,2304]{1,0:T(8,128)(2,1)S(1)} %get-tuple-element.40) | copy-start | bytes 7077892
  14.4 0.7 copy-start.14
  15.1 11.7 %copy-start.1 = (bf16[1,2048,256]{2,1,0:T(8,128)(2,1)S(1)}, bf16[1,2048,256]{2,1,0:T(8,128)(2,1)}, u32[]{:S(2)}) copy-start(bf16[1,2048,256]{2,1,0:T(8,128)(2,1)} %param.35) | copy-start | bytes 3145732
  15.1 45.4 %all-to-all-start = ((bf16[64,8,2304]{2,1,0:T(8,128)(2,1)}), bf16[64,8,2304]{2,1,0:T(8,128)(2,1)S(1)}, u32[]{:S(2)}, u32[]{:S(2)}) async-start(bf16[64,8,2304]{2,1,0:T(8,128)(2,1)} %bitcast.19), calls=%async_computation | async-start | bytes 4718592 | tf_op jit(solution)/shard_map/all_to_all | solution.py:559
  26.8 33.7 %collective-permute-start.3 = (bf16[2048,256]{1,0:T(8,128)(2,1)S(1)}, bf16[2048,256]{1,0:T(8,128)(2,1)}, u32[]{:S(2)}, u32[]{:S(2)}) collective-permute-start(bf16[2048,256]{1,0:T(8,128)(2,1)S(1)} %bitcast.21), channel_id=1, source_target_pairs={{0,1},{1,0},{2,3},{3,2},{4,5},{5,4},{6,7},{7,6},{8,9},{9,8},{10,11... | collective-permute-start | bytes 3145736 | tf_op jit(solution)/shard_map/ppermute | solution.py:21
  27.0 33.5 %collective-permute-start.4 = (bf16[2048,256]{1,0:T(8,128)(2,1)}, bf16[2048,256]{1,0:T(8,128)(2,1)}, u32[]{:S(2)}, u32[]{:S(2)}) collective-permute-start(bf16[2048,256]{1,0:T(8,128)(2,1)} %bitcast.23), channel_id=1, source_target_pairs={{0,1},{1,0},{2,3},{3,2},{4,5},{5,4},{6,7},{7,6},{8,9},{9,8},{10,11... | collective-permute-start | bytes 3145736 | tf_op jit(solution)/shard_map/ppermute | solution.py:21
  27.4 33.1 %collective-permute-start.5 = (bf16[512,1024]{1,0:T(8,128)(2,1)}, bf16[512,1024]{1,0:T(8,128)(2,1)}, u32[]{:S(2)}, u32[]{:S(2)}) collective-permute-start(bf16[512,1024]{1,0:T(8,128)(2,1)} %bitcast.25), channel_id=1, source_target_pairs={{0,1},{1,0},{2,3},{3,2},{4,5},{5,4},{6,7},{7,6},{8,9},{9,8},{10,11... | collective-permute-start | bytes 3145736 | tf_op jit(solution)/shard_map/ppermute | solution.py:21
  60.5 1.2 %copy-start.2 = (bf16[1,2048,256]{2,1,0:T(8,128)(2,1)S(1)}, bf16[1,2048,256]{2,1,0:T(8,128)(2,1)}, u32[]{:S(2)}) copy-start(bf16[1,2048,256]{2,1,0:T(8,128)(2,1)} %param.36) | copy-start | bytes 3145732
  61.8 1.2 %copy-start.3 = (bf16[1,512,1024]{2,1,0:T(8,128)(2,1)S(1)}, bf16[1,512,1024]{2,1,0:T(8,128)(2,1)}, u32[]{:S(2)}) copy-start(bf16[1,512,1024]{2,1,0:T(8,128)(2,1)} %param.37) | copy-start | bytes 3145732
  63.0 1.2 %copy-start.4 = (bf16[2048,256]{1,0:T(8,128)(2,1)S(1)}, bf16[2048,256]{1,0:T(8,128)(2,1)}, u32[]{:S(2)}) copy-start(bf16[2048,256]{1,0:T(8,128)(2,1)} %dense_gate_ref.1) | copy-start | bytes 3145732
  64.2 1.2 %copy-start.5 = (bf16[2048,256]{1,0:T(8,128)(2,1)S(1)}, bf16[2048,256]{1,0:T(8,128)(2,1)}, u32[]{:S(2)}) copy-start(bf16[2048,256]{1,0:T(8,128)(2,1)} %dense_up_ref.1) | copy-start | bytes 3145732
  65.4 1.0 copy-start.10
  66.4 0.9 copy-start.15
  73.5 38.4 %copy-start.8 = (bf16[128,512]{1,0:T(8,128)(2,1)S(1)}, bf16[128,512]{1,0:T(8,128)(2,1)}, u32[]{:S(2)}) copy-start(bf16[128,512]{1,0:T(8,128)(2,1)} %copy-done.7) | copy-start | bytes 393220
  73.5 38.4 %copy-start.17 = (bf16[128,64]{1,0:T(8,128)(2,1)S(1)}, bf16[128,64]{1,0:T(8,128)(2,1)}, u32[]{:S(2)}) copy-start(bf16[128,64]{1,0:T(8,128)(2,1)} %copy-done.16) | copy-start | bytes 49156
  112.3 2.0 %collective-permute-start.7 = (bf16[64,1024]{1,0:T(8,128)(2,1)S(1)}, bf16[64,1024]{1,0:T(8,128)(2,1)S(1)}, u32[]{:S(2)}, u32[]{:S(2)}) collective-permute-start(bf16[64,1024]{1,0:T(8,128)(2,1)S(1)} %combine.1), channel_id=1, source_target_pairs={{0,1},{1,0},{2,3},{3,2},{4,5},{5,4},{6,7},{7,6},{8,9},{9,8},{10,11... | collective-permute-start | bytes 393224 | tf_op jit(solution)/shard_map/ppermute | solution.py:21
  112.4 1.4 %collective-permute-start.6 = (bf16[64,256]{1,0:T(8,128)(2,1)S(1)}, bf16[64,256]{1,0:T(8,128)(2,1)S(1)}, u32[]{:S(2)}, u32[]{:S(2)}) collective-permute-start(bf16[64,256]{1,0:T(8,128)(2,1)S(1)} %get-tuple-element.52.own_hid_ref), channel_id=1, source_target_pairs={{0,1},{1,0},{2,3},{3,2},{4,5},{5,4},{6,7},{7,6},{8,9},{9,8},{10,11... | collective-permute-start | bytes 98312 | tf_op jit(solution)/shard_map/ppermute | solution.py:21

commit v6 on v5

--- a/solution.py
+++ b/solution.py
@@ -216,13 +216,9 @@
     features = 2 * half
     first = pl.ds(pl.multiple_of(core * half, half), half)
     second = pl.ds(pl.multiple_of((1 - core) * half, half), half)
-    copies = start_all(
-        (
-            (gate_hbm, gate_ref),
-            (out_hbm.at[first, :], weight_ref),
-        ),
-        sems,
-    )
+    gate_copy = pltpu.make_async_copy(gate_hbm, gate_ref, sems.at[0])
+    gate_copy.start()
+    out_copy = pltpu.make_async_copy(out_hbm.at[first, :], weight_ref, sems.at[1])
     own = own_ref[...].astype(F32)
     other = other_ref[...].astype(F32)
     mean = (jnp.sum(own, 1, keepdims=True) + jnp.sum(other, 1, keepdims=True)) / features
@@ -241,6 +237,7 @@
         ).astype(BF)
 
     branch = product(branch_ref)
+    out_copy.start()
     branch_out_ref[...] = branch
     conv = (conv_ref[...] + branch.astype(F32) * taps_ref[3:4, :]).astype(BF)
     width = recur_ref.shape[1]
@@ -266,9 +263,9 @@
     branch_copy.start()
     state_copy = pltpu.make_async_copy(state_out_ref, new_state_hbm, sems.at[3])
     state_copy.start()
-    wait_all(copies[:1])
+    gate_copy.wait()
     mixed_ref[...] = (jax.nn.gelu(product(gate_ref).astype(F32)) * state).astype(BF)
-    wait_all([*copies[1:], branch_copy, state_copy])
+    wait_all([out_copy, branch_copy, state_copy])
 
 
 def expert_body(

time: 117 us -> 117 us (level)
  no operation moved by 1% of the time
where the time goes in v6:
time: 117 us; the launch traced here: 115 us
  blocking collectives  38.4 us (33%)
  waiting for transfers between devices  33.9 us (29%)
  Pallas kernels  16.5 us (14%)
  starting transfers between devices  13.7 us (12%)
  local copies, waits for them, and re-layouts  11 us (9%)
    all_to_all x1, blocking collectives, per_device(): lax.all_to_all(served.reshape(experts, MAIN, block), 'ep', split_axis=0,...  38.4 us
    all_to_all x1, waiting for transfers between devices, per_device(): lax.all_to_all(payload.reshape(experts, MAIN, block), 'ep', split_axis=0,...  33 us
    all_to_all x1, starting transfers between devices, per_device(): lax.all_to_all(payload.reshape(experts, MAIN, block), 'ep', split_axis=0,...  11.7 us
    unnamed x46, local copies, waits for them, and re-layouts  11 us
    pallas_call x1, Pallas kernels, per_device(): pl.pallas_call(expert_body, name='experts', out_shape=(jax.ShapeDtypeStru...  6.14 us
    pallas_call x1, Pallas kernels, per_device(): pl.pallas_call(mixer_body, name='mixer', out_shape=(pltpu.HBM((3, seq_cou...  3.27 us
    pallas_call x1, Pallas kernels, per_device(): pl.pallas_call(warm_body, name='warm', out_shape=(jax.ShapeDtypeStruct((f...  2.5 us
  transfers between devices with their start and end apart: 9, of which 2 were waited for; matrix products, arithmetic and copies ran while one was open for 0% of the time, Pallas kernels for 4%

profile of v6, /device:TPU:0, one launch (start us, length us, event | category | flops | bytes accessed | tf_op | source)
XLA Modules:
  0.0 115.1 jit_solution(8745162094338160952)
XLA Ops:
  0.6 0.0 copy-start.6
  0.7 0.1 collective-permute-start
  0.8 2.5 %warm.1 = (bf16[2048,1024]{1,0:T(8,128)(2,1)S(1)}, f32[64,1024]{1,0:T(8,128)S(1)}, f32[1,1024]{1,0:T(1,128)S(1)}, bf16[3,64,1024]{2,1,0:T(8,128)(2,1)S(1)}) custom-call(bf16[2048,1024]{1,0:T(8,128)(2,1)} %weight_hbm.2, bf16[3,64,1024]{2,1,0:T(8,128)(2,1)} %bitcast.32, f32[4,1024]{1,0:T(4,128)} %taps_ref.1, f32[1,1024]{1,0:T(1,128)} %bitcast.34), custom_call_target="tpu_custom_call" | custom-call | tf_op jit(solution)/shard_map/warm/pallas_call | solution.py:433
  3.3 0.8 copy-done.9
  4.1 0.0 collective-permute-done.other_ref
  4.1 3.3 %mixer.1 = (bf16[3,64,1024]{2,1,0:T(8,128)(2,1)}, f32[64,1024]{1,0:T(8,128)}, bf16[64,1024]{1,0:T(8,128)(2,1)S(1)}, bf16[1024,1024]{1,0:T(8,128)(2,1)S(1)}) custom-call(s32[1]{0:T(128)} %bitcast.core_ref, bf16[64,1024]{1,0:T(8,128)(2,1)S(1)} %copy-done.6, bf16[64,1024]{1,0:T(8,128)(2,1)S(1)} %collective-permute-done.other_ref, f32[1,2048]{1,0:T(1,128)S(1)} %bitcast.28, ...), custom_call_target="tpu_custom_call" | custom-call | flops 536870912 | bytes 8388608 | tf_op jit(solution)/shard_map/mixer/pallas_call | solution.py:461
  7.4 0.5 collective-permute-start.1
  7.9 1.6 %near.1 = (f32[64,1024]{1,0:T(8,128)S(1)}, bf16[1024,1024]{1,0:T(8,128)(2,1)S(1)}) custom-call(s32[1]{0:T(128)} %bitcast.core_ref, bf16[64,1024]{1,0:T(8,128)(2,1)S(1)} %get-tuple-element.34.mixed_ref, bf16[1024,1024]{1,0:T(8,128)(2,1)S(1)} %get-tuple-element.35.weight_ref, bf16[2048,1024]{1,0:T(8,128)(2,1)} %weight_hbm.3), custom_call_target="tpu_custom_call" | custom-call | tf_op jit(solution)/shard_map/near/pallas_call | solution.py:504
  9.5 0.0 copy-start.21
  9.5 0.0 copy-start.22
  9.5 0.0 copy-start.19
  9.5 0.0 collective-permute-done.1.mixed_ref
  9.5 0.5 resid.1.own_ref.resid_ref
  10.0 0.2 collective-permute-start.2
  10.2 0.5 route.1
  10.7 0.0 copy-start.7
  10.7 0.6 copy-done.7
  11.4 0.6 copy-done.16
  12.0 0.0 collective-permute-done.2.other_ref
  12.0 0.0 copy-done.19
  12.0 1.0 pack.1
  13.0 1.4 %copy-done = bf16[512,2304]{1,0:T(8,128)(2,1)} copy-done((bf16[512,2304]{1,0:T(8,128)(2,1)}, bf16[512,2304]{1,0:T(8,128)(2,1)S(1)}, u32[]{:S(2)}) %copy-start) | copy-done | bytes 2359320
  14.4 0.7 copy-done.14
  15.1 11.7 %all-to-all-start = ((bf16[64,8,2304]{2,1,0:T(8,128)(2,1)}), bf16[64,8,2304]{2,1,0:T(8,128)(2,1)S(1)}, u32[]{:S(2)}, u32[]{:S(2)}) async-start(bf16[64,8,2304]{2,1,0:T(8,128)(2,1)} %bitcast.19), calls=%async_computation | async-start | bytes 4718592 | tf_op jit(solution)/shard_map/all_to_all | solution.py:556
  26.8 0.2 collective-permute-start.3
  27.0 0.4 collective-permute-start.4
  27.4 0.1 collective-permute-start.5
  27.5 33.0 %all-to-all-done = bf16[64,8,2304]{2,1,0:T(8,128)(2,1)S(1)} async-done(((bf16[64,8,2304]{2,1,0:T(8,128)(2,1)}), bf16[64,8,2304]{2,1,0:T(8,128)(2,1)S(1)}, u32[]{:S(2)}, u32[]{:S(2)}) %all-to-all-start) | async-done | bytes 2359328 | tf_op jit(solution)/shard_map/all_to_all | solution.py:556
  60.5 0.0 collective-permute-done.3.gate2_ref
  60.5 0.0 collective-permute-done.4.up2_ref
  60.5 0.0 collective-permute-done.5.down2_ref
  60.5 0.0 copy-start.2
  60.5 1.2 %copy-done.2 = bf16[1,2048,256]{2,1,0:T(8,128)(2,1)S(1)} copy-done((bf16[1,2048,256]{2,1,0:T(8,128)(2,1)S(1)}, bf16[1,2048,256]{2,1,0:T(8,128)(2,1)}, u32[]{:S(2)}) %copy-start.2) | copy-done | bytes 1048600
  61.8 1.2 %copy-done.3 = bf16[1,512,1024]{2,1,0:T(8,128)(2,1)S(1)} copy-done((bf16[1,512,1024]{2,1,0:T(8,128)(2,1)S(1)}, bf16[1,512,1024]{2,1,0:T(8,128)(2,1)}, u32[]{:S(2)}) %copy-start.3) | copy-done | bytes 1048600
  63.0 1.2 %copy-done.4 = bf16[2048,256]{1,0:T(8,128)(2,1)S(1)} copy-done((bf16[2048,256]{1,0:T(8,128)(2,1)S(1)}, bf16[2048,256]{1,0:T(8,128)(2,1)}, u32[]{:S(2)}) %copy-start.4) | copy-done | bytes 1048600
  64.2 1.2 %copy-done.5 = bf16[2048,256]{1,0:T(8,128)(2,1)S(1)} copy-done((bf16[2048,256]{1,0:T(8,128)(2,1)S(1)}, bf16[2048,256]{1,0:T(8,128)(2,1)}, u32[]{:S(2)}) %copy-start.5) | copy-done | bytes 1048600
  65.4 1.0 copy-done.10
  66.4 0.9 copy-done.15
  67.4 6.1 %experts.1 = (bf16[512,2304]{1,0:T(8,128)(2,1)S(1)}, bf16[64,256]{1,0:T(8,128)(2,1)S(1)}, bf16[512,1024]{1,0:T(8,128)(2,1)S(1)}, f32[1,1024]{1,0:T(1,128)S(1)}, bf16[3,64,1024]{2,1,0:T(8,128)(2,1)}) custom-call(s32[1]{0:T(128)} %bitcast.core_ref, bf16[512,2304]{1,0:T(8,128)(2,1)S(1)} %bitcast.18, ...), custom_call_target="tpu_custom_call", output_to_operand_aliasing={{4}: (14, {})} | custom-call | tf_op jit(solution)/shard_map/experts/pallas_call | solution.py:561
  73.5 0.0 copy-start.8
  73.5 38.4 %all_to_all.10 = bf16[64,8,2304]{2,1,0:T(8,128)(2,1)S(1)} all-to-all(bf16[64,8,2304]{2,1,0:T(8,128)(2,1)S(1)} %bitcast.20), channel_id=1, replica_groups=mesh['ep'=64,'tp'=2] {'ep'}, dimensions={0} | all-to-all | bytes 4718592 | tf_op jit(solution)/shard_map/all_to_all | solution.py:599
  111.9 0.4 combine.1
  112.3 0.1 collective-permute-start.7
  112.4 0.5 collective-permute-start.6
  112.9 0.9 collective-permute-done.6.other_hid_ref
  113.8 0.5 finish.1
  114.4 0.0 collective-permute-done.7
  114.4 0.7 add_convert_fusion
  (27 shorter events, 0.1 us)
Async XLA Ops:
  0.6 3.4 %copy-start.6 = (bf16[64,1024]{1,0:T(8,128)(2,1)S(1)}, bf16[64,1024]{1,0:T(8,128)(2,1)}, u32[]{:S(2)}) copy-start(bf16[64,1024]{1,0:T(8,128)(2,1)} %stream_ref.1) | copy-start | bytes 393220
  0.6 3.4 %copy-start.18 = (f32[4,1024]{1,0:T(4,128)S(1)}, f32[4,1024]{1,0:T(4,128)}, u32[]{:S(2)}) copy-start(f32[4,1024]{1,0:T(4,128)} %taps_ref.1) | copy-start | bytes 49156
  0.7 3.4 %copy-start.12 = (bf16[8,128,128]{2,1,0:T(8,128)(2,1)S(1)}, bf16[8,128,128]{2,1,0:T(8,128)(2,1)}, u32[]{:S(2)}) copy-start(bf16[8,128,128]{2,1,0:T(8,128)(2,1)} %input_ref.1) | copy-start | bytes 786436
  0.7 3.4 %copy-start.11 = (bf16[8,128,128]{2,1,0:T(8,128)(2,1)S(1)}, bf16[8,128,128]{2,1,0:T(8,128)(2,1)}, u32[]{:S(2)}) copy-start(bf16[8,128,128]{2,1,0:T(8,128)(2,1)} %recur_ref.1) | copy-start | bytes 786436
  0.7 3.4 %copy-start.20 = (f32[2048]{0:T(1024)S(1)}, f32[2048]{0:T(1024)}, u32[]{:S(2)}) copy-start(f32[2048]{0:T(1024)} %param.24) | copy-start | bytes 24580
  0.7 3.4 %copy-start.13 = (f32[64,1024]{1,0:T(8,128)S(1)}, f32[64,1024]{1,0:T(8,128)}, u32[]{:S(2)}) copy-start(f32[64,1024]{1,0:T(8,128)} %state_ref.1) | copy-start | bytes 786436
  0.7 3.4 %collective-permute-start = (bf16[64,1024]{1,0:T(8,128)(2,1)}, bf16[64,1024]{1,0:T(8,128)(2,1)S(1)}, u32[]{:S(2)}, u32[]{:S(2)}) collective-permute-start(bf16[64,1024]{1,0:T(8,128)(2,1)} %stream_ref.1), channel_id=1, source_target_pairs={{0,1},{1,0},{2,3},{3,2},{4,5},{5,4},{6,7},{7,6},{8,9},{9,8},{10,11... | collective-permute-start | bytes 393224 | tf_op jit(solution)/shard_map/ppermute | solution.py:21
  3.3 0.8 copy-start.9
  7.4 2.1 %collective-permute-start.1 = (bf16[64,1024]{1,0:T(8,128)(2,1)S(1)}, bf16[64,1024]{1,0:T(8,128)(2,1)S(1)}, u32[]{:S(2)}, u32[]{:S(2)}) collective-permute-start(bf16[64,1024]{1,0:T(8,128)(2,1)S(1)} %get-tuple-element.34.mixed_ref), channel_id=1, source_target_pairs={{0,1},{1,0},{2,3},{3,2},{4,5},{5,4},{6,7},{7,6},{8,9},{9,8},{10,11... | collective-permute-start | bytes 393224 | tf_op jit(solution)/shard_map/ppermute | solution.py:21
  9.5 0.8 copy-start.21
  9.5 0.8 copy-start.22
  9.5 2.5 %copy-start.19 = (f32[2048]{0:T(1024)S(1)}, f32[2048]{0:T(1024)}, u32[]{:S(2)}) copy-start(f32[2048]{0:T(1024)} %param.32) | copy-start | bytes 24580
  10.0 2.0 %collective-permute-start.2 = (bf16[64,1024]{1,0:T(8,128)(2,1)S(1)}, bf16[64,1024]{1,0:T(8,128)(2,1)S(1)}, u32[]{:S(2)}, u32[]{:S(2)}) collective-permute-start(bf16[64,1024]{1,0:T(8,128)(2,1)S(1)} %resid.1.own_ref.resid_ref), channel_id=1, source_target_pairs={{0,1},{1,0},{2,3},{3,2},{4,5},{5,4},{6,7},{7,6},{8,9},{9,8},{10,11... | collective-permute-start | bytes 393224 | tf_op jit(solution)/shard_map/ppermute | solution.py:21
  10.7 0.7 copy-start.7
  11.4 0.6 copy-start.16
  13.0 1.4 %copy-start = (bf16[512,2304]{1,0:T(8,128)(2,1)}, bf16[512,2304]{1,0:T(8,128)(2,1)S(1)}, u32[]{:S(2)}) copy-start(bf16[512,2304]{1,0:T(8,128)(2,1)S(1)} %get-tuple-element.40) | copy-start | bytes 7077892
  14.4 0.7 copy-start.14
  15.1 11.7 %copy-start.1 = (bf16[1,2048,256]{2,1,0:T(8,128)(2,1)S(1)}, bf16[1,2048,256]{2,1,0:T(8,128)(2,1)}, u32[]{:S(2)}) copy-start(bf16[1,2048,256]{2,1,0:T(8,128)(2,1)} %param.35) | copy-start | bytes 3145732
  15.1 45.4 %all-to-all-start = ((bf16[64,8,2304]{2,1,0:T(8,128)(2,1)}), bf16[64,8,2304]{2,1,0:T(8,128)(2,1)S(1)}, u32[]{:S(2)}, u32[]{:S(2)}) async-start(bf16[64,8,2304]{2,1,0:T(8,128)(2,1)} %bitcast.19), calls=%async_computation | async-start | bytes 4718592 | tf_op jit(solution)/shard_map/all_to_all | solution.py:556
  26.8 33.7 %collective-permute-start.3 = (bf16[2048,256]{1,0:T(8,128)(2,1)S(1)}, bf16[2048,256]{1,0:T(8,128)(2,1)}, u32[]{:S(2)}, u32[]{:S(2)}) collective-permute-start(bf16[2048,256]{1,0:T(8,128)(2,1)S(1)} %bitcast.21), channel_id=1, source_target_pairs={{0,1},{1,0},{2,3},{3,2},{4,5},{5,4},{6,7},{7,6},{8,9},{9,8},{10,11... | collective-permute-start | bytes 3145736 | tf_op jit(solution)/shard_map/ppermute | solution.py:21
  27.0 33.5 %collective-permute-start.4 = (bf16[2048,256]{1,0:T(8,128)(2,1)}, bf16[2048,256]{1,0:T(8,128)(2,1)}, u32[]{:S(2)}, u32[]{:S(2)}) collective-permute-start(bf16[2048,256]{1,0:T(8,128)(2,1)} %bitcast.23), channel_id=1, source_target_pairs={{0,1},{1,0},{2,3},{3,2},{4,5},{5,4},{6,7},{7,6},{8,9},{9,8},{10,11... | collective-permute-start | bytes 3145736 | tf_op jit(solution)/shard_map/ppermute | solution.py:21
  27.4 33.1 %collective-permute-start.5 = (bf16[512,1024]{1,0:T(8,128)(2,1)}, bf16[512,1024]{1,0:T(8,128)(2,1)}, u32[]{:S(2)}, u32[]{:S(2)}) collective-permute-start(bf16[512,1024]{1,0:T(8,128)(2,1)} %bitcast.25), channel_id=1, source_target_pairs={{0,1},{1,0},{2,3},{3,2},{4,5},{5,4},{6,7},{7,6},{8,9},{9,8},{10,11... | collective-permute-start | bytes 3145736 | tf_op jit(solution)/shard_map/ppermute | solution.py:21
  60.5 1.2 %copy-start.2 = (bf16[1,2048,256]{2,1,0:T(8,128)(2,1)S(1)}, bf16[1,2048,256]{2,1,0:T(8,128)(2,1)}, u32[]{:S(2)}) copy-start(bf16[1,2048,256]{2,1,0:T(8,128)(2,1)} %param.36) | copy-start | bytes 3145732
  61.8 1.2 %copy-start.3 = (bf16[1,512,1024]{2,1,0:T(8,128)(2,1)S(1)}, bf16[1,512,1024]{2,1,0:T(8,128)(2,1)}, u32[]{:S(2)}) copy-start(bf16[1,512,1024]{2,1,0:T(8,128)(2,1)} %param.37) | copy-start | bytes 3145732
  63.0 1.2 %copy-start.4 = (bf16[2048,256]{1,0:T(8,128)(2,1)S(1)}, bf16[2048,256]{1,0:T(8,128)(2,1)}, u32[]{:S(2)}) copy-start(bf16[2048,256]{1,0:T(8,128)(2,1)} %dense_gate_ref.1) | copy-start | bytes 3145732
  64.2 1.2 %copy-start.5 = (bf16[2048,256]{1,0:T(8,128)(2,1)S(1)}, bf16[2048,256]{1,0:T(8,128)(2,1)}, u32[]{:S(2)}) copy-start(bf16[2048,256]{1,0:T(8,128)(2,1)} %dense_up_ref.1) | copy-start | bytes 3145732
  65.4 1.0 copy-start.10
  66.4 0.9 copy-start.15
  73.5 38.4 %copy-start.8 = (bf16[128,512]{1,0:T(8,128)(2,1)S(1)}, bf16[128,512]{1,0:T(8,128)(2,1)}, u32[]{:S(2)}) copy-start(bf16[128,512]{1,0:T(8,128)(2,1)} %copy-done.7) | copy-start | bytes 393220
  73.5 38.4 %copy-start.17 = (bf16[128,64]{1,0:T(8,128)(2,1)S(1)}, bf16[128,64]{1,0:T(8,128)(2,1)}, u32[]{:S(2)}) copy-start(bf16[128,64]{1,0:T(8,128)(2,1)} %copy-done.16) | copy-start | bytes 49156
  112.3 2.0 %collective-permute-start.7 = (bf16[64,1024]{1,0:T(8,128)(2,1)S(1)}, bf16[64,1024]{1,0:T(8,128)(2,1)S(1)}, u32[]{:S(2)}, u32[]{:S(2)}) collective-permute-start(bf16[64,1024]{1,0:T(8,128)(2,1)S(1)} %combine.1), channel_id=1, source_target_pairs={{0,1},{1,0},{2,3},{3,2},{4,5},{5,4},{6,7},{7,6},{8,9},{9,8},{10,11... | collective-permute-start | bytes 393224 | tf_op jit(solution)/shard_map/ppermute | solution.py:21
  112.4 1.4 %collective-permute-start.6 = (bf16[64,256]{1,0:T(8,128)(2,1)S(1)}, bf16[64,256]{1,0:T(8,128)(2,1)S(1)}, u32[]{:S(2)}, u32[]{:S(2)}) collective-permute-start(bf16[64,256]{1,0:T(8,128)(2,1)S(1)} %get-tuple-element.52.own_hid_ref), channel_id=1, source_target_pairs={{0,1},{1,0},{2,3},{3,2},{4,5},{5,4},{6,7},{7,6},{8,9},{9,8},{10,11... | collective-permute-start | bytes 98312 | tf_op jit(solution)/shard_map/ppermute | solution.py:21
